TPU v7x, 32 devices: a whole 2x2x4 slice. The times are simulated.
32 devices in a mesh: ep: 8 (over z, y), tp: 4 (over x, core).
Axes of the slice: x: 2, y: 2, z: 4, core: 2. Of those that a mesh axis runs over, the one named last changes fastest.
Arguments:
- mixer_in: bfloat16 [3072, 2048], P(('ep', 'tp')), may hold values from -6 to 6
- expert_in: bfloat16 [3072, 2048], P(('ep', 'tp')), may hold values from -6 to 6
- mixer_gain: float32 [2048], replicated, may hold values from 0.1 to 1.9
- in_gate_weight: bfloat16 [2048, 2048], P(None, 'tp'), may hold values from -0.125 to 0.125
- out_gate_weight: bfloat16 [2048, 2048], P(None, 'tp'), may hold values from -0.125 to 0.125
- value_weight: bfloat16 [2048, 2048], P(None, 'tp'), may hold values from -0.125 to 0.125
- conv_taps: float32 [3, 2048], replicated, may hold values from -3 to 3
- mixer_proj: bfloat16 [2048, 2048], P(None, 'tp'), may hold values from -0.125 to 0.125
- expert_gain: float32 [2048], replicated, may hold values from 0.1 to 1.9
- route_ids: int32 [3072, 2], P('ep'), may hold values from 0 to 7, all different within a row; in each aligned block of 96 rows (0 to 95, 96 to 191, ...) at most 48 rows name the same one
- route_weights: float32 [3072, 2], P('ep'), may hold values from 0.1 to 1
- gate_weight: bfloat16 [8, 2048, 1024], P('ep', None, 'tp'), may hold values from -0.125 to 0.125
- up_weight: bfloat16 [8, 2048, 1024], P('ep', None, 'tp'), may hold values from -0.125 to 0.125
- down_weight: bfloat16 [8, 1024, 2048], P('ep', None, 'tp'), may hold values from -0.1875 to 0.1875
Outputs:
- mixer_out: bfloat16 [3072, 2048], P('ep', 'tp')
- expert_out: bfloat16 [3072, 2048], P('ep', 'tp')
Inputs may be any that keep to these rules, and one draw needn't show every extreme that they name: `route_ids`: each row names 2 different experts. In each aligned block of 96 rows no expert is named by more than 48 rows, a bound that some block reaches.
All inputs are finite; a program needn't handle non-finite values.
Results may differ from a plain program's by a relative error of at most 0.0076.
Values may be sent and summed in bfloat16 or wider, within the bound.
No kernel may reach another device: no remote copies, remote signals or barrier semaphores. Data moves between devices by JAX's collectives and lax.ppermute only.
A program may use at most 64 MiB of HBM per device.

v0:
```python
import functools

import jax
import jax.numpy as jnp
from jax import lax
from jax.experimental import pallas as pl
from jax.experimental.pallas import tpu as pltpu
from jax.sharding import PartitionSpec as P


norm_eps = 1e-06


def rms_rows(values, gain_row):
    wide = values.astype(jnp.float32)
    scale = lax.rsqrt(jnp.mean(wide * wide, axis=-1, keepdims=True) + norm_eps)
    return (wide * scale * gain_row).astype(jnp.bfloat16)


def swapped(value, axis, mask):
    count = lax.axis_size(axis)
    return lax.ppermute(value, axis, [(source, source ^ mask) for source in range(count)])


def after(value, *earlier):
    return lax.optimization_barrier((value,) + earlier)[0]


def slot_masks(block_ids, labels, slot_cap):
    rows = block_ids.shape[1]
    hits = block_ids[:, None, :] == labels[None, :, None]
    member = jnp.any(hits, axis=0)
    order = jnp.arange(rows, dtype=jnp.int32)
    before = (order[:, None] < order[None, :]).astype(jnp.bfloat16)
    rank = jnp.dot(member.astype(jnp.bfloat16), before, preferred_element_type=jnp.float32)
    rank = jnp.where(member, rank, -1.0)
    slots = jnp.arange(slot_cap, dtype=jnp.int32).astype(jnp.float32)
    return hits, rank[:, None, :] == slots[None, :, None]


def swaps_direct(count):
    return count <= 16 and count & (count - 1) == 0


def far_first(count):
    return sorted(range(1, count), key=lambda k: (-k.bit_length(), k))


def exchange(chunks, axis, direct):
    if direct:
        moved = {0: chunks[0]}
        for k in far_first(len(chunks)):
            moved[k] = swapped(chunks[k], axis, k)
        return [moved[k] for k in range(len(chunks))]
    (rows,) = chunks
    split = rows.reshape(lax.axis_size(axis), -1, rows.shape[1])
    moved = lax.all_to_all(split, axis, split_axis=0, concat_axis=0, tiled=True)
    return [moved.reshape(rows.shape)]


MIB = 1 << 20
HBM = pl.BlockSpec(memory_space=pltpu.HBM)
VMEM = pl.BlockSpec(memory_space=pltpu.VMEM)
SMEM = pl.BlockSpec(memory_space=pltpu.SMEM)


def dispatch_kernel(direct, slot_cap, place_ref, ids_ref, source_ref, gain_ref, *refs):
    out_refs, (rows_ref, sem) = refs[:-2], refs[-2:]
    load = pltpu.make_async_copy(source_ref, rows_ref, sem)
    load.start()
    tok, width = rows_ref.shape
    total = ids_ref.shape[1]
    slots = sum(ref.shape[0] for ref in out_refs)
    experts = slots // slot_cap
    lanes = min(total, -(-tok // 128) * 128)
    tp_index, ep_index = place_ref[0], place_ref[1]
    ids = pltpu.roll(ids_ref[...], lax.rem(total - tp_index * tok, total), 1)[:, :lanes]
    labels = lax.broadcasted_iota(jnp.int32, (experts, lanes), 0)
    if direct:
        labels = labels ^ ep_index
    member = ids[0:1] == labels
    for pick in range(1, ids_ref.shape[0]):
        member = member | (ids[pick : pick + 1] == labels)
    first = lax.broadcasted_iota(jnp.int32, (lanes, lanes), 0)
    second = lax.broadcasted_iota(jnp.int32, (lanes, lanes), 1)
    before = jnp.where(first < second, 1.0, 0.0).astype(jnp.bfloat16)
    member = jnp.where(member, 1.0, 0.0)
    rank = jnp.dot(member.astype(jnp.bfloat16), before, preferred_element_type=jnp.float32)
    rank = jnp.where(member > 0.5, rank, -1.0).astype(jnp.bfloat16)
    slot = lax.broadcasted_iota(jnp.int32, (slots, experts), 0)
    start = lax.broadcasted_iota(jnp.int32, (slots, experts), 1) * slot_cap
    inside = (slot >= start) & (slot < start + slot_cap)
    spread = jnp.where(inside, 1.0, 0.0)
    rank_of = jnp.dot(spread.astype(jnp.bfloat16), rank, preferred_element_type=jnp.float32)
    offset = jnp.where(inside, (slot - start).astype(jnp.float32), 0.0)
    offset = jnp.sum(offset, axis=1, keepdims=True)
    mask = jnp.where(rank_of == offset, 1.0, 0.0)[:, :tok].astype(jnp.bfloat16)
    load.wait()
    wide = rows_ref[...].astype(jnp.float32)
    scale = lax.rsqrt(jnp.mean(wide * wide, axis=-1, keepdims=True) + norm_eps)
    normed = (wide * scale * gain_ref[...]).astype(jnp.bfloat16)
    step = min(width, 512)
    for col in range(0, width, step):
        part = jnp.dot(mask, normed[:, col : col + step], preferred_element_type=jnp.float32)
        part = part.astype(jnp.bfloat16)
        row = 0
        for ref in out_refs:
            ref[:, col : col + step] = part[row : row + ref.shape[0]]
            row += ref.shape[0]


def dispatched(place, ids, rows, gain, sizes, direct, slot_cap):
    width = rows.shape[1]
    return pl.pallas_call(
        functools.partial(dispatch_kernel, direct, slot_cap),
        out_shape=[jax.ShapeDtypeStruct((size, width), jnp.bfloat16) for size in sizes],
        in_specs=[SMEM, VMEM, HBM, VMEM],
        out_specs=[VMEM] * len(sizes),
        scratch_shapes=[pltpu.VMEM(rows.shape, rows.dtype), pltpu.SemaphoreType.DMA],
        compiler_params=pltpu.CompilerParams(vmem_limit_bytes=56 * MIB),
        cost_estimate=pl.CostEstimate(
            flops=2 * sum(sizes) * rows.shape[0] * width, bytes_accessed=2 * MIB, transcendentals=0
        ),
        name="dispatch",
    )(place, ids, rows, gain)


def hidden_kernel(row_count, *refs):
    row_refs, refs = refs[:row_count], refs[row_count:]
    weight_refs, (out_ref, rows, weights, row_sems, weight_sems) = refs[:-5], refs[-5:]
    copies, row = [], 0
    for index, ref in enumerate(row_refs):
        target = rows.at[pl.ds(row, ref.shape[0])]
        copies.append(pltpu.make_async_copy(ref, target, row_sems.at[index]))
        row += ref.shape[0]
    loads = []
    for index, ref in enumerate(weight_refs):
        width = ref.shape[1]
        target = weights.at[index % 2, :, pl.ds(index // 2 * width, width)]
        loads.append(pltpu.make_async_copy(ref, target, weight_sems.at[index]))
    for copy in copies + loads[0::2] + loads[1::2]:
        copy.start()
    for copy in copies + loads[0::2]:
        copy.wait()
    gate_pre = jnp.dot(rows[...], weights[0], preferred_element_type=jnp.float32)
    for load in loads[1::2]:
        load.wait()
    up_pre = jnp.dot(rows[...], weights[1], preferred_element_type=jnp.float32)
    out_ref[...] = (gate_pre / (1.0 + jnp.exp(-gate_pre)) * up_pre).astype(jnp.bfloat16)


def hidden_of(row_parts, pairs):
    rows = sum(part.shape[0] for part in row_parts)
    depth, width = pairs[0][0].shape
    weights = [weight for pair in pairs for weight in pair]
    return pl.pallas_call(
        functools.partial(hidden_kernel, len(row_parts)),
        out_shape=jax.ShapeDtypeStruct((rows, width * len(pairs)), jnp.bfloat16),
        in_specs=[HBM] * (len(row_parts) + len(weights)),
        out_specs=VMEM,
        scratch_shapes=[
            pltpu.VMEM((rows, depth), jnp.bfloat16),
            pltpu.VMEM((2, depth, width * len(pairs)), jnp.bfloat16),
            pltpu.SemaphoreType.DMA((len(row_parts),)),
            pltpu.SemaphoreType.DMA((len(weights),)),
        ],
        compiler_params=pltpu.CompilerParams(vmem_limit_bytes=56 * MIB),
        cost_estimate=pl.CostEstimate(
            flops=2 * rows * depth * width * len(weights),
            bytes_accessed=2 * (rows * depth + len(weights) * depth * width),
            transcendentals=rows * width * len(pairs),
        ),
        name="hidden",
    )(*row_parts, *weights)


def down_kernel(base, place_ref, first_ref, second_ref, own_ref, near_ref, *out_refs):
    half = first_ref.shape[1] // 2
    col = 0
    for weight_ref in (own_ref, near_ref):
        total = None
        for j in range(4):
            source = first_ref if j < 2 else second_ref
            block = source[:, (j % 2) * half : (j % 2 + 1) * half]
            start = pl.multiple_of((place_ref[0] ^ base ^ j) * half, half)
            term = jnp.dot(
                block, weight_ref[pl.ds(start, half), :], preferred_element_type=jnp.float32
            )
            total = term if total is None else total + term
        total = total.astype(jnp.bfloat16)
        row = 0
        for ref in out_refs:
            ref[:, col : col + total.shape[1]] = total[row : row + ref.shape[0]]
            row += ref.shape[0]
        col += total.shape[1]


def results_of(place, base, first, second, down_own, down_near, sizes):
    width = 2 * down_own.shape[1]
    return pl.pallas_call(
        functools.partial(down_kernel, base),
        out_shape=[jax.ShapeDtypeStruct((size, width), jnp.bfloat16) for size in sizes],
        in_specs=[SMEM, VMEM, VMEM, VMEM, VMEM],
        out_specs=[VMEM] * len(sizes),
        compiler_params=pltpu.CompilerParams(vmem_limit_bytes=12 * MIB),
        cost_estimate=pl.CostEstimate(
            flops=2 * sum(sizes) * down_own.shape[0] * width,
            bytes_accessed=4 * MIB,
            transcendentals=0,
        ),
        name="down",
    )(place, first, second, down_own, down_near)


def combine_rows(mask, hits, share_rows, returned):
    share_of = jnp.sum(jnp.where(hits, share_rows[:, None, :], 0.0), axis=0)
    mixed = jnp.where(mask, share_of[:, None, :], 0.0).reshape(-1, mask.shape[2])
    high = mixed.astype(jnp.bfloat16)
    low = (mixed - high.astype(jnp.float32)).astype(jnp.bfloat16)
    dims = (((0,), (0,)), ((), ()))
    total = lax.dot_general(high, returned, dims, preferred_element_type=jnp.float32)
    total = total + lax.dot_general(low, returned, dims, preferred_element_type=jnp.float32)
    return total.astype(jnp.bfloat16)


def on_device(
    mixer_in,
    expert_in,
    mixer_gain,
    in_gate_weight,
    out_gate_weight,
    value_weight,
    conv_taps,
    mixer_proj,
    expert_gain,
    route_ids,
    route_weights,
    gate_weight,
    up_weight,
    down_weight,
):
    tok_dev = mixer_in.shape[0]
    tp_count = lax.axis_size("tp")
    ep_count = lax.axis_size("ep")
    top_count = route_ids.shape[1]
    experts = ep_count * gate_weight.shape[0]
    slot_cap = max(2, 2 * tok_dev * top_count // experts)
    tp_index = lax.axis_index("tp")
    ep_index = lax.axis_index("ep")
    direct = swaps_direct(ep_count)
    near, far = 1, tp_count // 2

    gates, ups = {0: gate_weight[0]}, {0: up_weight[0]}
    gates[far] = swapped(gates[0], "tp", far)
    ups[far] = swapped(ups[0], "tp", far)
    gates[near] = swapped(gates[0], "tp", near)
    ups[near] = swapped(ups[0], "tp", near)
    down_own = down_weight[0]
    down_near = swapped(down_own, "tp", near)
    order = [0, near, far, far ^ near]

    def rows_of(weight, j, width):
        return lax.dynamic_slice_in_dim(weight, (tp_index ^ j) * width, width, 0)

    peers = jnp.arange(experts, dtype=jnp.int32)
    labels = (peers ^ ep_index) if direct else peers

    def block_of(values, j):
        return lax.dynamic_slice_in_dim(values, (tp_index ^ j) * tok_dev, tok_dev, 0)

    hits_own, mask_own = slot_masks(block_of(route_ids, 0).T, labels, slot_cap)
    hits_far, mask_far = slot_masks(block_of(route_ids, far).T, labels, slot_cap)
    place = jnp.where(jnp.arange(2) == 0, tp_index, ep_index).astype(jnp.int32)
    sizes = [slot_cap] * experts if direct else [experts * slot_cap]
    outgoing = dispatched(
        place, route_ids.T, expert_in, expert_gain[None, :], sizes, direct, slot_cap
    )
    slots_in = exchange(outgoing, "ep", direct)

    first = hidden_of(slots_in, [(gates[j], ups[j]) for j in (0, near)])
    gates[far ^ near] = swapped(after(gates[far], first), "tp", near)
    ups[far ^ near] = swapped(after(ups[far], first), "tp", near)
    second = hidden_of(slots_in, [(gates[j], ups[j]) for j in (far, far ^ near)])
    first_far = swapped(after(first, ups[far]), "tp", far)
    second_far = swapped(second, "tp", far)
    done_own = results_of(place, 0, first, second, down_own, down_near, sizes)
    back_own = exchange(done_own, "ep", direct)

    normed = {0: after(rms_rows(mixer_in, mixer_gain), ups[far], first)}
    normed[far] = swapped(normed[0], "tp", far)
    normed[near] = swapped(normed[0], "tp", near)
    normed = {j: after(normed[j], done_own[0]) for j in normed}
    normed[far ^ near] = swapped(normed[far], "tp", near)
    mixer_rows = jnp.zeros((tp_count * tok_dev, mixer_in.shape[1]), jnp.bfloat16)
    for j in order:
        mixer_rows = lax.dynamic_update_slice_in_dim(
            mixer_rows, normed[j], (tp_index ^ j) * tok_dev, 0
        )
    chan_width = in_gate_weight.shape[1]
    in_gate = jnp.dot(mixer_rows, in_gate_weight, preferred_element_type=jnp.float32)
    values = jnp.dot(mixer_rows, value_weight, preferred_element_type=jnp.float32)
    product = (in_gate * values).astype(jnp.bfloat16)
    out_gate = jnp.dot(mixer_rows, out_gate_weight, preferred_element_type=jnp.float32)
    tap_count = conv_taps.shape[0]
    row_count = product.shape[0]
    rim_rows = lax.ppermute(
        product[row_count - (tap_count - 1) :], "ep", [(i, i + 1) for i in range(ep_count - 1)]
    )
    extended = jnp.concatenate([rim_rows, product], axis=0).astype(jnp.float32)
    tap_rows = lax.dynamic_slice_in_dim(conv_taps, tp_index * chan_width, chan_width, 1)
    conv_sum = tap_rows[0] * extended[0:row_count]
    for tap_index in range(1, tap_count):
        conv_sum = conv_sum + tap_rows[tap_index] * extended[tap_index : tap_index + row_count]
    gated = {0: (out_gate * conv_sum).astype(jnp.bfloat16)}
    gated[far] = swapped(gated[0], "tp", far)
    gated[near] = swapped(gated[0], "tp", near)
    gated[far ^ near] = swapped(gated[far], "tp", near)
    mixer_sum = None
    for j in order:
        term = jnp.dot(
            gated[j], rows_of(mixer_proj, j, chan_width), preferred_element_type=jnp.float32
        )
        mixer_sum = term if mixer_sum is None else mixer_sum + term
    first_far = after(first_far, gated[0])
    done_far = results_of(place, far, first_far, second_far, down_own, down_near, sizes)
    back_far = exchange(done_far, "ep", direct)

    def returned(parts):
        return jnp.concatenate(parts, axis=0)

    shares = route_weights / jnp.sum(route_weights, axis=1, keepdims=True)
    mixed_own = combine_rows(mask_own, hits_own, block_of(shares, 0).T, returned(back_own))
    mixed_far = combine_rows(mask_far, hits_far, block_of(shares, far).T, returned(back_far))
    mixed = jnp.concatenate([mixed_own, mixed_far], axis=0)
    col_width = down_own.shape[1]
    mixed_near = swapped(mixed[:, col_width:], "tp", near)
    expert_out = jnp.zeros((tp_count * tok_dev, col_width), jnp.bfloat16)
    for j, block in (
        (0, mixed[:tok_dev, :col_width]),
        (far, mixed[tok_dev:, :col_width]),
        (near, mixed_near[:tok_dev]),
        (far ^ near, mixed_near[tok_dev:]),
    ):
        expert_out = lax.dynamic_update_slice_in_dim(
            expert_out, block, (tp_index ^ j) * tok_dev, 0
        )

    return (mixer_sum.astype(jnp.bfloat16), expert_out)


def solution(mesh):
    return jax.shard_map(
        on_device,
        mesh=mesh,
        in_specs=(
            P(("ep", "tp"), None),
            P(("ep", "tp"), None),
            P(),
            P(None, "tp"),
            P(None, "tp"),
            P(None, "tp"),
            P(),
            P(None, "tp"),
            P(),
            P("ep", None),
            P("ep", None),
            P("ep", None, "tp"),
            P("ep", None, "tp"),
            P("ep", None, "tp"),
        ),
        out_specs=(P("ep", "tp"), P("ep", "tp")),
        check_vma=False,
    )
```

profile of v0, /device:TPU:0, one launch (start us, length us, event | category | flops | bytes accessed | tf_op | source)
XLA Modules:
  0.0 156.1 jit_solution(13914997043355486673)
XLA Ops:
  1.2 3.6 %dispatch.1 = (bf16[48,2048]{1,0:T(8,128)(2,1)}, bf16[48,2048]{1,0:T(8,128)(2,1)}, bf16[48,2048]{1,0:T(8,128)(2,1)}, bf16[48,2048]{1,0:T(8,128)(2,1)}, bf16[48,2...) custom-call(s32[2]{0:T(128)} %compare_select_fusion.2.place_ref, ...), custom_call_target="tpu_custom_call" | custom-call | flops 150994944 | bytes 2097152 | tf_op jit(solution)/shard_map/dispatch/pallas_call | solution.py:114
  4.8 3.1 %collective-permute-start.1 = (bf16[48,2048]{1,0:T(8,128)(2,1)}, bf16[48,2048]{1,0:T(8,128)(2,1)S(1)}, u32[]{:S(2)}, u32[]{:S(2)}) collective-permute-start(bf16[48,2048]{1,0:T(8,128)(2,1)} %get-tuple-element.35), channel_id=1, source_target_pairs={{0,4},{4,0},{8,12},{12,8},{16,20},{20,16},{24,28},{28,24},{1,5},{5... | collective-permute-start | bytes 589832 | tf_op jit(solution)/shard_map/ppermute | solution.py:22
  7.8 1.6 %collective-permute-start.2 = (bf16[48,2048]{1,0:T(8,128)(2,1)}, bf16[48,2048]{1,0:T(8,128)(2,1)S(1)}, u32[]{:S(2)}, u32[]{:S(2)}) collective-permute-start(bf16[48,2048]{1,0:T(8,128)(2,1)} %get-tuple-element.36), channel_id=1, source_target_pairs={{0,8},{4,12},{8,0},{12,4},{16,24},{20,28},{24,16},{28,20},{1,9},{5... | collective-permute-start | bytes 589832 | tf_op jit(solution)/shard_map/ppermute | solution.py:22
  12.9 1.9 %collective-permute-start = (bf16[2048,256]{1,0:T(8,128)(2,1)}, bf16[2048,256]{1,0:T(8,128)(2,1)}, u32[]{:S(2)}, u32[]{:S(2)}) collective-permute-start(bf16[2048,256]{1,0:T(8,128)(2,1)} %bitcast.76), channel_id=1, source_target_pairs={{0,2},{1,3},{2,0},{3,1},{4,6},{5,7},{6,4},{7,5},{8,10},{9,11},{10,... | collective-permute-start | bytes 3145736 | tf_op jit(solution)/shard_map/ppermute | solution.py:22
  18.4 2.7 %collective-permute-start.4 = (bf16[48,2048]{1,0:T(8,128)(2,1)}, bf16[48,2048]{1,0:T(8,128)(2,1)S(1)}, u32[]{:S(2)}, u32[]{:S(2)}) collective-permute-start(bf16[48,2048]{1,0:T(8,128)(2,1)} %get-tuple-element.38), channel_id=1, source_target_pairs={{0,16},{4,20},{8,24},{12,28},{16,0},{20,4},{24,8},{28,12},{1,17},{... | collective-permute-start | bytes 589832 | tf_op jit(solution)/shard_map/ppermute | solution.py:22
  21.8 7.7 %collective-permute-done.4.refs_4_ = bf16[48,2048]{1,0:T(8,128)(2,1)S(1)} collective-permute-done((bf16[48,2048]{1,0:T(8,128)(2,1)}, bf16[48,2048]{1,0:T(8,128)(2,1)S(1)}, u32[]{:S(2)}, u32[]{:S(2)}) %collective-permute-start.4) | collective-permute-done | bytes 196640 | tf_op jit(solution)/shard_map/ppermute | solution.py:22
  30.1 11.6 %collective-permute-done.5.refs_5_ = bf16[48,2048]{1,0:T(8,128)(2,1)S(1)} collective-permute-done((bf16[48,2048]{1,0:T(8,128)(2,1)}, bf16[48,2048]{1,0:T(8,128)(2,1)S(1)}, u32[]{:S(2)}, u32[]{:S(2)}) %collective-permute-start.5) | collective-permute-done | bytes 196640 | tf_op jit(solution)/shard_map/ppermute | solution.py:22
  43.4 6.0 %collective-permute-done.6.refs_6_ = bf16[48,2048]{1,0:T(8,128)(2,1)S(1)} collective-permute-done((bf16[48,2048]{1,0:T(8,128)(2,1)}, bf16[48,2048]{1,0:T(8,128)(2,1)S(1)}, u32[]{:S(2)}, u32[]{:S(2)}) %collective-permute-start.6) | collective-permute-done | bytes 196640 | tf_op jit(solution)/shard_map/ppermute | solution.py:22
  49.4 1.9 %collective-permute-start.7 = (bf16[48,2048]{1,0:T(8,128)(2,1)}, bf16[48,2048]{1,0:T(8,128)(2,1)S(1)}, u32[]{:S(2)}, u32[]{:S(2)}) collective-permute-start(bf16[48,2048]{1,0:T(8,128)(2,1)} %get-tuple-element.41), channel_id=1, source_target_pairs={{0,28},{4,24},{8,20},{12,16},{16,12},{20,8},{24,4},{28,0},{1,29},{... | collective-permute-start | bytes 589832 | tf_op jit(solution)/shard_map/ppermute | solution.py:22
  52.0 6.1 %collective-permute-done.7.refs_7_ = bf16[48,2048]{1,0:T(8,128)(2,1)S(1)} collective-permute-done((bf16[48,2048]{1,0:T(8,128)(2,1)}, bf16[48,2048]{1,0:T(8,128)(2,1)S(1)}, u32[]{:S(2)}, u32[]{:S(2)}) %collective-permute-start.7) | collective-permute-done | bytes 196640 | tf_op jit(solution)/shard_map/ppermute | solution.py:22
  58.8 5.3 %hidden.2.first_ref = bf16[384,512]{1,0:T(8,128)(2,1)} custom-call(bf16[48,2048]{1,0:T(8,128)(2,1)} %get-tuple-element.34.refs_0_, bf16[48,2048]{1,0:T(8,128)(2,1)} %copy-done.6, bf16[48,2048]{1,0:T(8,128)(2,1)} %copy-done.7, bf16[48,2048]{1,0:T(8,128)(2,1)} %copy-done.8, bf16[48,2048]{1,0:T(8,128)(2,1)} %copy-done.9, bf16[48,2048]{1,0:T(8,128)(2,1)} %copy-done.10, ...), custom_call_target="tpu_custom_call" | custom-call | flops 1610612736 | bytes 5767168 | tf_op jit(solution)/shard_map/hidden/pallas_call | solution.py:156
  71.8 5.3 %hidden.3.second_ref = bf16[384,512]{1,0:T(8,128)(2,1)} custom-call(bf16[48,2048]{1,0:T(8,128)(2,1)} %get-tuple-element.34.refs_0_, bf16[48,2048]{1,0:T(8,128)(2,1)} %copy-done.6, bf16[48,2048]{1,0:T(8,128)(2,1)} %copy-done.7, bf16[48,2048]{1,0:T(8,128)(2,1)} %copy-done.8, bf16[48,2048]{1,0:T(8,128)(2,1)} %copy-done.9, bf16[48,2048]{1,0:T(8,128)(2,1)} %copy-done.10, ...), custom_call_target="tpu_custom_call" | custom-call | flops 1610612736 | bytes 5767168 | tf_op jit(solution)/shard_map/hidden/pallas_call | solution.py:156
  84.4 1.7 %collective-permute-start.21 = (bf16[48,1024]{1,0:T(8,128)(2,1)S(1)}, bf16[48,1024]{1,0:T(8,128)(2,1)S(1)}, u32[]{:S(2)}, u32[]{:S(2)}) collective-permute-start(bf16[48,1024]{1,0:T(8,128)(2,1)S(1)} %get-tuple-element.49), channel_id=1, source_target_pairs={{0,4},{4,0},{8,12},{12,8},{16,20},{20,16},{24,28},{28,24},{1,5},{5... | collective-permute-start | bytes 294920 | tf_op jit(solution)/shard_map/ppermute | solution.py:22
  86.1 1.7 %collective-permute-start.22 = (bf16[48,1024]{1,0:T(8,128)(2,1)S(1)}, bf16[48,1024]{1,0:T(8,128)(2,1)S(1)}, u32[]{:S(2)}, u32[]{:S(2)}) collective-permute-start(bf16[48,1024]{1,0:T(8,128)(2,1)S(1)} %get-tuple-element.50), channel_id=1, source_target_pairs={{0,8},{4,12},{8,0},{12,4},{16,24},{20,28},{24,16},{28,20},{1,9},{5... | collective-permute-start | bytes 294920 | tf_op jit(solution)/shard_map/ppermute | solution.py:22
  87.8 1.9 %collective-permute-done.21 = bf16[48,1024]{1,0:T(8,128)(2,1)S(1)} collective-permute-done((bf16[48,1024]{1,0:T(8,128)(2,1)S(1)}, bf16[48,1024]{1,0:T(8,128)(2,1)S(1)}, u32[]{:S(2)}, u32[]{:S(2)}) %collective-permute-start.21) | collective-permute-done | bytes 98336 | tf_op jit(solution)/shard_map/ppermute | solution.py:22
  89.7 2.7 %collective-permute-start.23 = (bf16[48,1024]{1,0:T(8,128)(2,1)S(1)}, bf16[48,1024]{1,0:T(8,128)(2,1)S(1)}, u32[]{:S(2)}, u32[]{:S(2)}) collective-permute-start(bf16[48,1024]{1,0:T(8,128)(2,1)S(1)} %get-tuple-element.51), channel_id=1, source_target_pairs={{0,12},{4,8},{8,4},{12,0},{16,28},{20,24},{24,20},{28,16},{1,13},{... | collective-permute-start | bytes 294920 | tf_op jit(solution)/shard_map/ppermute | solution.py:22
  93.5 1.8 %collective-permute-done.23 = bf16[48,1024]{1,0:T(8,128)(2,1)S(1)} collective-permute-done((bf16[48,1024]{1,0:T(8,128)(2,1)S(1)}, bf16[48,1024]{1,0:T(8,128)(2,1)S(1)}, u32[]{:S(2)}, u32[]{:S(2)}) %collective-permute-start.23) | collective-permute-done | bytes 98336 | tf_op jit(solution)/shard_map/ppermute | solution.py:22
  95.4 4.3 %collective-permute-start.25 = (bf16[48,1024]{1,0:T(8,128)(2,1)S(1)}, bf16[48,1024]{1,0:T(8,128)(2,1)S(1)}, u32[]{:S(2)}, u32[]{:S(2)}) collective-permute-start(bf16[48,1024]{1,0:T(8,128)(2,1)S(1)} %get-tuple-element.53), channel_id=1, source_target_pairs={{0,20},{4,16},{8,28},{12,24},{16,4},{20,0},{24,12},{28,8},{1,21},{... | collective-permute-start | bytes 294920 | tf_op jit(solution)/shard_map/ppermute | solution.py:22
  101.1 2.4 %collective-permute-start.26 = (bf16[48,1024]{1,0:T(8,128)(2,1)S(1)}, bf16[48,1024]{1,0:T(8,128)(2,1)S(1)}, u32[]{:S(2)}, u32[]{:S(2)}) collective-permute-start(bf16[48,1024]{1,0:T(8,128)(2,1)S(1)} %get-tuple-element.54), channel_id=1, source_target_pairs={{0,24},{4,28},{8,16},{12,20},{16,8},{20,12},{24,0},{28,4},{1,25},{... | collective-permute-start | bytes 294920 | tf_op jit(solution)/shard_map/ppermute | solution.py:22
  103.5 2.5 %collective-permute-done.25 = bf16[48,1024]{1,0:T(8,128)(2,1)S(1)} collective-permute-done((bf16[48,1024]{1,0:T(8,128)(2,1)S(1)}, bf16[48,1024]{1,0:T(8,128)(2,1)S(1)}, u32[]{:S(2)}, u32[]{:S(2)}) %collective-permute-start.25) | collective-permute-done | bytes 98336 | tf_op jit(solution)/shard_map/ppermute | solution.py:22
  106.1 2.6 %collective-permute-start.27 = (bf16[48,1024]{1,0:T(8,128)(2,1)S(1)}, bf16[48,1024]{1,0:T(8,128)(2,1)S(1)}, u32[]{:S(2)}, u32[]{:S(2)}) collective-permute-start(bf16[48,1024]{1,0:T(8,128)(2,1)S(1)} %get-tuple-element.55), channel_id=1, source_target_pairs={{0,28},{4,24},{8,20},{12,16},{16,12},{20,8},{24,4},{28,0},{1,29},{... | collective-permute-start | bytes 294920 | tf_op jit(solution)/shard_map/ppermute | solution.py:22
  108.7 4.7 %collective-permute-done.27 = bf16[48,1024]{1,0:T(8,128)(2,1)S(1)} collective-permute-done((bf16[48,1024]{1,0:T(8,128)(2,1)S(1)}, bf16[48,1024]{1,0:T(8,128)(2,1)S(1)}, u32[]{:S(2)}, u32[]{:S(2)}) %collective-permute-start.27) | collective-permute-done | bytes 98336 | tf_op jit(solution)/shard_map/ppermute | solution.py:22
  117.6 3.0 %collective-permute-start.17 = (bf16[2,512]{1,0:T(2,128)(2,1)S(1)}, bf16[2,512]{1,0:T(2,128)(2,1)S(1)}, u32[]{:S(2)}, u32[]{:S(2)}) collective-permute-start(bf16[2,512]{1,0:T(2,128)(2,1)S(1)} %slice.48), channel_id=1, source_target_pairs={{0,4},{4,8},{8,12},{12,16},{16,20},{20,24},{24,28},{1,5},{5,9},{9,... | collective-permute-start | bytes 6152 | tf_op jit(solution)/shard_map/ppermute | solution.py:306
  124.0 1.5 down.3
  125.6 2.3 %collective-permute-start.30 = (bf16[48,1024]{1,0:T(8,128)(2,1)S(1)}, bf16[48,1024]{1,0:T(8,128)(2,1)S(1)}, u32[]{:S(2)}, u32[]{:S(2)}) collective-permute-start(bf16[48,1024]{1,0:T(8,128)(2,1)S(1)} %get-tuple-element.59), channel_id=1, source_target_pairs={{0,4},{4,0},{8,12},{12,8},{16,20},{20,16},{24,28},{28,24},{1,5},{5... | collective-permute-start | bytes 294920 | tf_op jit(solution)/shard_map/ppermute | solution.py:22
  127.9 1.5 collective-permute-start.32
  133.5 2.1 %collective-permute-start.34 = (bf16[48,1024]{1,0:T(8,128)(2,1)S(1)}, bf16[48,1024]{1,0:T(8,128)(2,1)S(1)}, u32[]{:S(2)}, u32[]{:S(2)}) collective-permute-start(bf16[48,1024]{1,0:T(8,128)(2,1)S(1)} %get-tuple-element.63), channel_id=1, source_target_pairs={{0,20},{4,16},{8,28},{12,24},{16,4},{20,0},{24,12},{28,8},{1,21},{... | collective-permute-start | bytes 294920 | tf_op jit(solution)/shard_map/ppermute | solution.py:22
  135.7 2.7 %collective-permute-start.35 = (bf16[48,1024]{1,0:T(8,128)(2,1)S(1)}, bf16[48,1024]{1,0:T(8,128)(2,1)S(1)}, u32[]{:S(2)}, u32[]{:S(2)}) collective-permute-start(bf16[48,1024]{1,0:T(8,128)(2,1)S(1)} %get-tuple-element.64), channel_id=1, source_target_pairs={{0,24},{4,28},{8,16},{12,20},{16,8},{20,12},{24,0},{28,4},{1,25},{... | collective-permute-start | bytes 294920 | tf_op jit(solution)/shard_map/ppermute | solution.py:22
  138.3 5.2 %collective-permute-done.33 = bf16[48,1024]{1,0:T(8,128)(2,1)S(1)} collective-permute-done((bf16[48,1024]{1,0:T(8,128)(2,1)S(1)}, bf16[48,1024]{1,0:T(8,128)(2,1)S(1)}, u32[]{:S(2)}, u32[]{:S(2)}) %collective-permute-start.33) | collective-permute-done | bytes 98336 | tf_op jit(solution)/shard_map/ppermute | solution.py:22
  143.5 2.3 %collective-permute-start.36 = (bf16[48,1024]{1,0:T(8,128)(2,1)S(1)}, bf16[48,1024]{1,0:T(8,128)(2,1)S(1)}, u32[]{:S(2)}, u32[]{:S(2)}) collective-permute-start(bf16[48,1024]{1,0:T(8,128)(2,1)S(1)} %get-tuple-element.65), channel_id=1, source_target_pairs={{0,28},{4,24},{8,20},{12,16},{16,12},{20,8},{24,4},{28,0},{1,29},{... | collective-permute-start | bytes 294920 | tf_op jit(solution)/shard_map/ppermute | solution.py:22
  145.9 1.8 %collective-permute-done.34 = bf16[48,1024]{1,0:T(8,128)(2,1)S(1)} collective-permute-done((bf16[48,1024]{1,0:T(8,128)(2,1)S(1)}, bf16[48,1024]{1,0:T(8,128)(2,1)S(1)}, u32[]{:S(2)}, u32[]{:S(2)}) %collective-permute-start.34) | collective-permute-done | bytes 98336 | tf_op jit(solution)/shard_map/ppermute | solution.py:22
  147.7 3.2 %collective-permute-done.36 = bf16[48,1024]{1,0:T(8,128)(2,1)S(1)} collective-permute-done((bf16[48,1024]{1,0:T(8,128)(2,1)S(1)}, bf16[48,1024]{1,0:T(8,128)(2,1)S(1)}, u32[]{:S(2)}, u32[]{:S(2)}) %collective-permute-start.36) | collective-permute-done | bytes 98336 | tf_op jit(solution)/shard_map/ppermute | solution.py:22
  (152 shorter events, 46.2 us)
Async XLA Ops:
  4.8 8.2 %collective-permute-start.1 = (bf16[48,2048]{1,0:T(8,128)(2,1)}, bf16[48,2048]{1,0:T(8,128)(2,1)S(1)}, u32[]{:S(2)}, u32[]{:S(2)}) collective-permute-start(bf16[48,2048]{1,0:T(8,128)(2,1)} %get-tuple-element.35), channel_id=1, source_target_pairs={{0,4},{4,0},{8,12},{12,8},{16,20},{20,16},{24,28},{28,24},{1,5},{5... | collective-permute-start | bytes 589832 | tf_op jit(solution)/shard_map/ppermute | solution.py:22
  7.8 8.0 %collective-permute-start.2 = (bf16[48,2048]{1,0:T(8,128)(2,1)}, bf16[48,2048]{1,0:T(8,128)(2,1)S(1)}, u32[]{:S(2)}, u32[]{:S(2)}) collective-permute-start(bf16[48,2048]{1,0:T(8,128)(2,1)} %get-tuple-element.36), channel_id=1, source_target_pairs={{0,8},{4,12},{8,0},{12,4},{16,24},{20,28},{24,16},{28,20},{1,9},{5... | collective-permute-start | bytes 589832 | tf_op jit(solution)/shard_map/ppermute | solution.py:22
  9.4 9.0 %collective-permute-start.3 = (bf16[48,2048]{1,0:T(8,128)(2,1)}, bf16[48,2048]{1,0:T(8,128)(2,1)S(1)}, u32[]{:S(2)}, u32[]{:S(2)}) collective-permute-start(bf16[48,2048]{1,0:T(8,128)(2,1)} %get-tuple-element.37), channel_id=1, source_target_pairs={{0,12},{4,8},{8,4},{12,0},{16,28},{20,24},{24,20},{28,16},{1,13},{... | collective-permute-start | bytes 589832 | tf_op jit(solution)/shard_map/ppermute | solution.py:22
  9.4 48.7 %collective-permute-start.8 = (bf16[2048,256]{1,0:T(8,128)(2,1)}, bf16[2048,256]{1,0:T(8,128)(2,1)}, u32[]{:S(2)}, u32[]{:S(2)}) collective-permute-start(bf16[2048,256]{1,0:T(8,128)(2,1)} %bitcast.78), channel_id=1, source_target_pairs={{0,1},{1,0},{2,3},{3,2},{4,5},{5,4},{6,7},{7,6},{8,9},{9,8},{10,11... | collective-permute-start | bytes 3145736 | tf_op jit(solution)/shard_map/ppermute | solution.py:22
  9.4 48.7 %collective-permute-start.9 = (bf16[2048,256]{1,0:T(8,128)(2,1)}, bf16[2048,256]{1,0:T(8,128)(2,1)}, u32[]{:S(2)}, u32[]{:S(2)}) collective-permute-start(bf16[2048,256]{1,0:T(8,128)(2,1)} %bitcast.75), channel_id=1, source_target_pairs={{0,1},{1,0},{2,3},{3,2},{4,5},{5,4},{6,7},{7,6},{8,9},{9,8},{10,11... | collective-permute-start | bytes 3145736 | tf_op jit(solution)/shard_map/ppermute | solution.py:22
  12.9 51.1 %collective-permute-start = (bf16[2048,256]{1,0:T(8,128)(2,1)}, bf16[2048,256]{1,0:T(8,128)(2,1)}, u32[]{:S(2)}, u32[]{:S(2)}) collective-permute-start(bf16[2048,256]{1,0:T(8,128)(2,1)} %bitcast.76), channel_id=1, source_target_pairs={{0,2},{1,3},{2,0},{3,1},{4,6},{5,7},{6,4},{7,5},{8,10},{9,11},{10,... | collective-permute-start | bytes 3145736 | tf_op jit(solution)/shard_map/ppermute | solution.py:22
  15.8 48.4 %collective-permute-start.10 = (bf16[2048,256]{1,0:T(8,128)(2,1)}, bf16[2048,256]{1,0:T(8,128)(2,1)}, u32[]{:S(2)}, u32[]{:S(2)}) collective-permute-start(bf16[2048,256]{1,0:T(8,128)(2,1)} %bitcast.79), channel_id=1, source_target_pairs={{0,2},{1,3},{2,0},{3,1},{4,6},{5,7},{6,4},{7,5},{8,10},{9,11},{10,... | collective-permute-start | bytes 3145736 | tf_op jit(solution)/shard_map/ppermute | solution.py:22
  18.4 11.1 %collective-permute-start.4 = (bf16[48,2048]{1,0:T(8,128)(2,1)}, bf16[48,2048]{1,0:T(8,128)(2,1)S(1)}, u32[]{:S(2)}, u32[]{:S(2)}) collective-permute-start(bf16[48,2048]{1,0:T(8,128)(2,1)} %get-tuple-element.38), channel_id=1, source_target_pairs={{0,16},{4,20},{8,24},{12,28},{16,0},{20,4},{24,8},{28,12},{1,17},{... | collective-permute-start | bytes 589832 | tf_op jit(solution)/shard_map/ppermute | solution.py:22
  29.5 12.2 %collective-permute-start.5 = (bf16[48,2048]{1,0:T(8,128)(2,1)}, bf16[48,2048]{1,0:T(8,128)(2,1)S(1)}, u32[]{:S(2)}, u32[]{:S(2)}) collective-permute-start(bf16[48,2048]{1,0:T(8,128)(2,1)} %get-tuple-element.39), channel_id=1, source_target_pairs={{0,20},{4,16},{8,28},{12,24},{16,4},{20,0},{24,12},{28,8},{1,21},{... | collective-permute-start | bytes 589832 | tf_op jit(solution)/shard_map/ppermute | solution.py:22
  41.7 7.7 %collective-permute-start.6 = (bf16[48,2048]{1,0:T(8,128)(2,1)}, bf16[48,2048]{1,0:T(8,128)(2,1)S(1)}, u32[]{:S(2)}, u32[]{:S(2)}) collective-permute-start(bf16[48,2048]{1,0:T(8,128)(2,1)} %get-tuple-element.40), channel_id=1, source_target_pairs={{0,24},{4,28},{8,16},{12,20},{16,8},{20,12},{24,0},{28,4},{1,25},{... | collective-permute-start | bytes 589832 | tf_op jit(solution)/shard_map/ppermute | solution.py:22
  49.4 8.7 %collective-permute-start.7 = (bf16[48,2048]{1,0:T(8,128)(2,1)}, bf16[48,2048]{1,0:T(8,128)(2,1)S(1)}, u32[]{:S(2)}, u32[]{:S(2)}) collective-permute-start(bf16[48,2048]{1,0:T(8,128)(2,1)} %get-tuple-element.41), channel_id=1, source_target_pairs={{0,28},{4,24},{8,20},{12,16},{16,12},{20,8},{24,4},{28,0},{1,29},{... | collective-permute-start | bytes 589832 | tf_op jit(solution)/shard_map/ppermute | solution.py:22
  58.1 20.4 %collective-permute-start.13 = (bf16[1024,512]{1,0:T(8,128)(2,1)}, bf16[1024,512]{1,0:T(8,128)(2,1)S(1)}, u32[]{:S(2)}, u32[]{:S(2)}) collective-permute-start(bf16[1024,512]{1,0:T(8,128)(2,1)} %bitcast.72), channel_id=1, source_target_pairs={{0,1},{1,0},{2,3},{3,2},{4,5},{5,4},{6,7},{7,6},{8,9},{9,8},{10,11... | collective-permute-start | bytes 3145736 | tf_op jit(solution)/shard_map/ppermute | solution.py:22
  64.1 6.9 %collective-permute-start.12 = (bf16[2048,256]{1,0:T(8,128)(2,1)}, bf16[2048,256]{1,0:T(8,128)(2,1)}, u32[]{:S(2)}, u32[]{:S(2)}) collective-permute-start(bf16[2048,256]{1,0:T(8,128)(2,1)} %collective-permute-done.refs_9_), channel_id=1, source_target_pairs={{0,1},{1,0},{2,3},{3,2},{4,5},{5,4},{6,7},{7,6},{8,9},{9,8},{10,11... | collective-permute-start | bytes 3145736 | tf_op jit(solution)/shard_map/ppermute | solution.py:22
  64.2 7.6 %collective-permute-start.11 = (bf16[2048,256]{1,0:T(8,128)(2,1)}, bf16[2048,256]{1,0:T(8,128)(2,1)}, u32[]{:S(2)}, u32[]{:S(2)}) collective-permute-start(bf16[2048,256]{1,0:T(8,128)(2,1)} %collective-permute-done.10.refs_8_), channel_id=1, source_target_pairs={{0,1},{1,0},{2,3},{3,2},{4,5},{5,4},{6,7},{7,6},{8,9},{9,8},{10,11... | collective-permute-start | bytes 3145736 | tf_op jit(solution)/shard_map/ppermute | solution.py:22
  65.8 15.2 %collective-permute-start.15 = (bf16[96,2048]{1,0:T(8,128)(2,1)}, bf16[96,2048]{1,0:T(8,128)(2,1)}, u32[]{:S(2)}, u32[]{:S(2)}) collective-permute-start(bf16[96,2048]{1,0:T(8,128)(2,1)} %fusion.7), channel_id=1, source_target_pairs={{0,2},{1,3},{2,0},{3,1},{4,6},{5,7},{6,4},{7,5},{8,10},{9,11},{10,... | collective-permute-start | bytes 1179656 | tf_op jit(solution)/shard_map/ppermute | solution.py:22
  67.1 13.9 %collective-permute-start.14 = (bf16[96,2048]{1,0:T(8,128)(2,1)}, bf16[96,2048]{1,0:T(8,128)(2,1)}, u32[]{:S(2)}, u32[]{:S(2)}) collective-permute-start(bf16[96,2048]{1,0:T(8,128)(2,1)} %fusion.7), channel_id=1, source_target_pairs={{0,1},{1,0},{2,3},{3,2},{4,5},{5,4},{6,7},{7,6},{8,9},{9,8},{10,11... | collective-permute-start | bytes 1179656 | tf_op jit(solution)/shard_map/ppermute | solution.py:22
  71.0 53.0 %collective-permute-start.28 = (bf16[384,512]{1,0:T(8,128)(2,1)S(1)}, bf16[384,512]{1,0:T(8,128)(2,1)S(1)}, u32[]{:S(2)}, u32[]{:S(2)}) collective-permute-start(bf16[384,512]{1,0:T(8,128)(2,1)S(1)} %copy-done.1), channel_id=1, source_target_pairs={{0,2},{1,3},{2,0},{3,1},{4,6},{5,7},{6,4},{7,5},{8,10},{9,11},{10,... | collective-permute-start | bytes 1179656 | tf_op jit(solution)/shard_map/ppermute | solution.py:22
  77.1 47.0 %collective-permute-start.29 = (bf16[384,512]{1,0:T(8,128)(2,1)}, bf16[384,512]{1,0:T(8,128)(2,1)S(1)}, u32[]{:S(2)}, u32[]{:S(2)}) collective-permute-start(bf16[384,512]{1,0:T(8,128)(2,1)} %hidden.3.second_ref), channel_id=1, source_target_pairs={{0,2},{1,3},{2,0},{3,1},{4,6},{5,7},{6,4},{7,5},{8,10},{9,11},{10,... | collective-permute-start | bytes 1179656 | tf_op jit(solution)/shard_map/ppermute | solution.py:22
  81.0 33.0 %collective-permute-start.16 = (bf16[96,2048]{1,0:T(8,128)(2,1)}, bf16[96,2048]{1,0:T(8,128)(2,1)S(1)}, u32[]{:S(2)}, u32[]{:S(2)}) collective-permute-start(bf16[96,2048]{1,0:T(8,128)(2,1)} %collective-permute-done.15), channel_id=1, source_target_pairs={{0,1},{1,0},{2,3},{3,2},{4,5},{5,4},{6,7},{7,6},{8,9},{9,8},{10,11... | collective-permute-start | bytes 1179656 | tf_op jit(solution)/shard_map/ppermute | solution.py:22
  86.1 6.3 %collective-permute-start.22 = (bf16[48,1024]{1,0:T(8,128)(2,1)S(1)}, bf16[48,1024]{1,0:T(8,128)(2,1)S(1)}, u32[]{:S(2)}, u32[]{:S(2)}) collective-permute-start(bf16[48,1024]{1,0:T(8,128)(2,1)S(1)} %get-tuple-element.50), channel_id=1, source_target_pairs={{0,8},{4,12},{8,0},{12,4},{16,24},{20,28},{24,16},{28,20},{1,9},{5... | collective-permute-start | bytes 294920 | tf_op jit(solution)/shard_map/ppermute | solution.py:22
  89.7 5.7 %collective-permute-start.23 = (bf16[48,1024]{1,0:T(8,128)(2,1)S(1)}, bf16[48,1024]{1,0:T(8,128)(2,1)S(1)}, u32[]{:S(2)}, u32[]{:S(2)}) collective-permute-start(bf16[48,1024]{1,0:T(8,128)(2,1)S(1)} %get-tuple-element.51), channel_id=1, source_target_pairs={{0,12},{4,8},{8,4},{12,0},{16,28},{20,24},{24,20},{28,16},{1,13},{... | collective-permute-start | bytes 294920 | tf_op jit(solution)/shard_map/ppermute | solution.py:22
  92.4 8.7 %collective-permute-start.24 = (bf16[48,1024]{1,0:T(8,128)(2,1)S(1)}, bf16[48,1024]{1,0:T(8,128)(2,1)S(1)}, u32[]{:S(2)}, u32[]{:S(2)}) collective-permute-start(bf16[48,1024]{1,0:T(8,128)(2,1)S(1)} %get-tuple-element.52), channel_id=1, source_target_pairs={{0,16},{4,20},{8,24},{12,28},{16,0},{20,4},{24,8},{28,12},{1,17},{... | collective-permute-start | bytes 294920 | tf_op jit(solution)/shard_map/ppermute | solution.py:22
  95.4 10.7 %collective-permute-start.25 = (bf16[48,1024]{1,0:T(8,128)(2,1)S(1)}, bf16[48,1024]{1,0:T(8,128)(2,1)S(1)}, u32[]{:S(2)}, u32[]{:S(2)}) collective-permute-start(bf16[48,1024]{1,0:T(8,128)(2,1)S(1)} %get-tuple-element.53), channel_id=1, source_target_pairs={{0,20},{4,16},{8,28},{12,24},{16,4},{20,0},{24,12},{28,8},{1,21},{... | collective-permute-start | bytes 294920 | tf_op jit(solution)/shard_map/ppermute | solution.py:22
  101.1 7.5 %collective-permute-start.26 = (bf16[48,1024]{1,0:T(8,128)(2,1)S(1)}, bf16[48,1024]{1,0:T(8,128)(2,1)S(1)}, u32[]{:S(2)}, u32[]{:S(2)}) collective-permute-start(bf16[48,1024]{1,0:T(8,128)(2,1)S(1)} %get-tuple-element.54), channel_id=1, source_target_pairs={{0,24},{4,28},{8,16},{12,20},{16,8},{20,12},{24,0},{28,4},{1,25},{... | collective-permute-start | bytes 294920 | tf_op jit(solution)/shard_map/ppermute | solution.py:22
  106.1 7.3 %collective-permute-start.27 = (bf16[48,1024]{1,0:T(8,128)(2,1)S(1)}, bf16[48,1024]{1,0:T(8,128)(2,1)S(1)}, u32[]{:S(2)}, u32[]{:S(2)}) collective-permute-start(bf16[48,1024]{1,0:T(8,128)(2,1)S(1)} %get-tuple-element.55), channel_id=1, source_target_pairs={{0,28},{4,24},{8,20},{12,16},{16,12},{20,8},{24,4},{28,0},{1,29},{... | collective-permute-start | bytes 294920 | tf_op jit(solution)/shard_map/ppermute | solution.py:22
  122.9 30.5 %collective-permute-start.18 = (bf16[384,512]{1,0:T(8,128)(2,1)S(1)}, bf16[384,512]{1,0:T(8,128)(2,1)S(1)}, u32[]{:S(2)}, u32[]{:S(2)}) collective-permute-start(bf16[384,512]{1,0:T(8,128)(2,1)S(1)} %fusion), channel_id=1, source_target_pairs={{0,1},{1,0},{2,3},{3,2},{4,5},{5,4},{6,7},{7,6},{8,9},{9,8},{10,11... | collective-permute-start | bytes 1179656 | tf_op jit(solution)/shard_map/ppermute | solution.py:22
  123.0 30.2 %collective-permute-start.19 = (bf16[384,512]{1,0:T(8,128)(2,1)S(1)}, bf16[384,512]{1,0:T(8,128)(2,1)S(1)}, u32[]{:S(2)}, u32[]{:S(2)}) collective-permute-start(bf16[384,512]{1,0:T(8,128)(2,1)S(1)} %fusion), channel_id=1, source_target_pairs={{0,2},{1,3},{2,0},{3,1},{4,6},{5,7},{6,4},{7,5},{8,10},{9,11},{10,... | collective-permute-start | bytes 1179656 | tf_op jit(solution)/shard_map/ppermute | solution.py:22
  127.9 7.7 %collective-permute-start.32 = (bf16[48,1024]{1,0:T(8,128)(2,1)S(1)}, bf16[48,1024]{1,0:T(8,128)(2,1)S(1)}, u32[]{:S(2)}, u32[]{:S(2)}) collective-permute-start(bf16[48,1024]{1,0:T(8,128)(2,1)S(1)} %get-tuple-element.61), channel_id=1, source_target_pairs={{0,12},{4,8},{8,4},{12,0},{16,28},{20,24},{24,20},{28,16},{1,13},{... | collective-permute-start | bytes 294920 | tf_op jit(solution)/shard_map/ppermute | solution.py:22
  131.0 12.5 %collective-permute-start.33 = (bf16[48,1024]{1,0:T(8,128)(2,1)S(1)}, bf16[48,1024]{1,0:T(8,128)(2,1)S(1)}, u32[]{:S(2)}, u32[]{:S(2)}) collective-permute-start(bf16[48,1024]{1,0:T(8,128)(2,1)S(1)} %get-tuple-element.62), channel_id=1, source_target_pairs={{0,16},{4,20},{8,24},{12,28},{16,0},{20,4},{24,8},{28,12},{1,17},{... | collective-permute-start | bytes 294920 | tf_op jit(solution)/shard_map/ppermute | solution.py:22
  133.5 14.2 %collective-permute-start.34 = (bf16[48,1024]{1,0:T(8,128)(2,1)S(1)}, bf16[48,1024]{1,0:T(8,128)(2,1)S(1)}, u32[]{:S(2)}, u32[]{:S(2)}) collective-permute-start(bf16[48,1024]{1,0:T(8,128)(2,1)S(1)} %get-tuple-element.63), channel_id=1, source_target_pairs={{0,20},{4,16},{8,28},{12,24},{16,4},{20,0},{24,12},{28,8},{1,21},{... | collective-permute-start | bytes 294920 | tf_op jit(solution)/shard_map/ppermute | solution.py:22
  135.7 12.0 %collective-permute-start.35 = (bf16[48,1024]{1,0:T(8,128)(2,1)S(1)}, bf16[48,1024]{1,0:T(8,128)(2,1)S(1)}, u32[]{:S(2)}, u32[]{:S(2)}) collective-permute-start(bf16[48,1024]{1,0:T(8,128)(2,1)S(1)} %get-tuple-element.64), channel_id=1, source_target_pairs={{0,24},{4,28},{8,16},{12,20},{16,8},{20,12},{24,0},{28,4},{1,25},{... | collective-permute-start | bytes 294920 | tf_op jit(solution)/shard_map/ppermute | solution.py:22
  143.5 7.4 %collective-permute-start.36 = (bf16[48,1024]{1,0:T(8,128)(2,1)S(1)}, bf16[48,1024]{1,0:T(8,128)(2,1)S(1)}, u32[]{:S(2)}, u32[]{:S(2)}) collective-permute-start(bf16[48,1024]{1,0:T(8,128)(2,1)S(1)} %get-tuple-element.65), channel_id=1, source_target_pairs={{0,28},{4,24},{8,20},{12,16},{16,12},{20,8},{24,4},{28,0},{1,29},{... | collective-permute-start | bytes 294920 | tf_op jit(solution)/shard_map/ppermute | solution.py:22
  (28 other events, 483.2 us)
where the time goes:
time: 157 us; the launch traced here: 156 us
  waiting for transfers between devices  62.9 us (40%)
  starting transfers between devices  52.1 us (33%)
  Pallas kernels  17.1 us (11%)
  local copies, waits for them, and re-layouts  8.66 us (6%)
  matrix products  7.83 us (5%)
  other arithmetic  6.24 us (4%)
    ppermute x37, waiting for transfers between devices, swapped(): lax.ppermute(value, axis, [(source, source ^ mask) for source in range(co...  61.8 us
    ppermute x37, starting transfers between devices, swapped(): lax.ppermute(value, axis, [(source, source ^ mask) for source in range(co...  49.1 us
    pallas_call x2, Pallas kernels, hidden_of(): pl.pallas_call(functools.partial(hidden_kernel, len(row_parts)), out_shap...  10.5 us
    pallas_call x1, Pallas kernels, dispatched(): pl.pallas_call(functools.partial(dispatch_kernel, direct, slot_cap), out_...  3.56 us
    unnamed x58, local copies, waits for them, and re-layouts  3.35 us
    dynamic_update_slice x4, local copies, waits for them, and re-layouts, on_device(): lax.dynamic_update_slice_in_dim(mixer_rows, normed[j], (tp_index ^ j) * t...  3.15 us
  transfers between devices with their start and end apart: 38, of which 20 were waited for; matrix products, arithmetic and copies ran while one was open for 11% of the time, Pallas kernels for 9%

commit v1 on v0

--- a/solution.py
+++ b/solution.py
@@ -23,7 +23,7 @@
 
 
 def after(value, *earlier):
-    return lax.optimization_barrier((value,) + earlier)[0]
+    return lax.optimization_barrier((value, earlier))[0]
 
 
 def slot_masks(block_ids, labels, slot_cap):
@@ -48,18 +48,20 @@
 
 def exchange(chunks, axis, direct):
     if direct:
-        moved = {0: chunks[0]}
-        for k in far_first(len(chunks)):
-            moved[k] = swapped(chunks[k], axis, k)
-        return [moved[k] for k in range(len(chunks))]
-    (rows,) = chunks
+        moved = dict(chunks)
+        for k in far_first(lax.axis_size(axis)):
+            if k in chunks:
+                moved[k] = swapped(chunks[k], axis, k)
+        return moved
+    rows = chunks[0]
     split = rows.reshape(lax.axis_size(axis), -1, rows.shape[1])
     moved = lax.all_to_all(split, axis, split_axis=0, concat_axis=0, tiled=True)
-    return [moved.reshape(rows.shape)]
+    return {0: moved.reshape(rows.shape)}
 
 
 MIB = 1 << 20
-HBM = pl.BlockSpec(memory_space=pltpu.HBM)
+STREAMS = 4
+ANY = pl.BlockSpec(memory_space=pl.ANY)
 VMEM = pl.BlockSpec(memory_space=pltpu.VMEM)
 SMEM = pl.BlockSpec(memory_space=pltpu.SMEM)
 
@@ -114,7 +116,7 @@
     return pl.pallas_call(
         functools.partial(dispatch_kernel, direct, slot_cap),
         out_shape=[jax.ShapeDtypeStruct((size, width), jnp.bfloat16) for size in sizes],
-        in_specs=[SMEM, VMEM, HBM, VMEM],
+        in_specs=[SMEM, VMEM, ANY, VMEM],
         out_specs=[VMEM] * len(sizes),
         scratch_shapes=[pltpu.VMEM(rows.shape, rows.dtype), pltpu.SemaphoreType.DMA],
         compiler_params=pltpu.CompilerParams(vmem_limit_bytes=56 * MIB),
@@ -125,69 +127,114 @@
     )(place, ids, rows, gain)
 
 
-def hidden_kernel(row_count, *refs):
+def stream_hidden(row_refs, weight_refs, rows, weights, row_sems, weight_sems):
+    chunks = row_sems.shape[0]
+    depth = rows.shape[1] // chunks
+    plan = []
+    for chunk in range(chunks):
+        part = pl.ds(chunk * depth, depth)
+        copies, row = [], 0
+        for index, ref in enumerate(row_refs):
+            target = rows.at[pl.ds(row, ref.shape[0]), part]
+            sem = row_sems.at[chunk, index]
+            copies.append(pltpu.make_async_copy(ref.at[:, part], target, sem))
+            row += ref.shape[0]
+        for index, ref in enumerate(weight_refs):
+            width = ref.shape[1]
+            target = weights.at[index % 2, part, pl.ds(index // 2 * width, width)]
+            sem = weight_sems.at[chunk, index]
+            copies.append(pltpu.make_async_copy(ref.at[part, :], target, sem))
+        for copy in copies:
+            copy.start()
+        plan.append(copies)
+    gate_pre = up_pre = None
+    for chunk in range(chunks):
+        for copy in plan[chunk]:
+            copy.wait()
+        part = slice(chunk * depth, (chunk + 1) * depth)
+        here = rows[:, part]
+        gate_term = jnp.dot(here, weights[0, part, :], preferred_element_type=jnp.float32)
+        up_term = jnp.dot(here, weights[1, part, :], preferred_element_type=jnp.float32)
+        gate_pre = gate_term if gate_pre is None else gate_pre + gate_term
+        up_pre = up_term if up_pre is None else up_pre + up_term
+    return (gate_pre / (1.0 + jnp.exp(-gate_pre)) * up_pre).astype(jnp.bfloat16)
+
+
+def hidden_scratch(row_parts, weights):
+    rows = sum(part.shape[0] for part in row_parts)
+    depth, width = weights[0].shape
+    return [
+        pltpu.VMEM((rows, depth), jnp.bfloat16),
+        pltpu.VMEM((2, depth, width * len(weights) // 2), jnp.bfloat16),
+        pltpu.SemaphoreType.DMA((STREAMS, len(row_parts))),
+        pltpu.SemaphoreType.DMA((STREAMS, len(weights))),
+    ]
+
+
+def hidden_cost(row_parts, weights):
+    rows = sum(part.shape[0] for part in row_parts)
+    depth, width = weights[0].shape
+    return pl.CostEstimate(
+        flops=2 * rows * depth * width * len(weights),
+        bytes_accessed=2 * (rows * depth + len(weights) * depth * width),
+        transcendentals=rows * width * len(weights) // 2,
+    )
+
+
+def first_kernel(row_count, *refs):
     row_refs, refs = refs[:row_count], refs[row_count:]
-    weight_refs, (out_ref, rows, weights, row_sems, weight_sems) = refs[:-5], refs[-5:]
-    copies, row = [], 0
-    for index, ref in enumerate(row_refs):
-        target = rows.at[pl.ds(row, ref.shape[0])]
-        copies.append(pltpu.make_async_copy(ref, target, row_sems.at[index]))
-        row += ref.shape[0]
-    loads = []
-    for index, ref in enumerate(weight_refs):
-        width = ref.shape[1]
-        target = weights.at[index % 2, :, pl.ds(index // 2 * width, width)]
-        loads.append(pltpu.make_async_copy(ref, target, weight_sems.at[index]))
-    for copy in copies + loads[0::2] + loads[1::2]:
-        copy.start()
-    for copy in copies + loads[0::2]:
-        copy.wait()
-    gate_pre = jnp.dot(rows[...], weights[0], preferred_element_type=jnp.float32)
-    for load in loads[1::2]:
+    weight_refs, (out_ref, *scratch) = refs[:-5], refs[-5:]
+    out_ref[...] = stream_hidden(row_refs, weight_refs, *scratch)
+
+
+def first_hidden(row_parts, weights):
+    rows = sum(part.shape[0] for part in row_parts)
+    width = weights[0].shape[1] * len(weights) // 2
+    return pl.pallas_call(
+        functools.partial(first_kernel, len(row_parts)),
+        out_shape=jax.ShapeDtypeStruct((rows, width), jnp.bfloat16),
+        in_specs=[ANY] * (len(row_parts) + len(weights)),
+        out_specs=VMEM,
+        scratch_shapes=hidden_scratch(row_parts, weights),
+        compiler_params=pltpu.CompilerParams(vmem_limit_bytes=56 * MIB),
+        cost_estimate=hidden_cost(row_parts, weights),
+        name="first_hidden",
+    )(*row_parts, *weights)
+
+
+def down_rows(place, first, second, weight_ref):
+    half = first.shape[1] // 2
+    total = None
+    for j in range(4):
+        source = first if j < 2 else second
+        block = source[:, (j % 2) * half : (j % 2 + 1) * half]
+        start = pl.multiple_of((place ^ j) * half, half)
+        term = jnp.dot(block, weight_ref[pl.ds(start, half), :], preferred_element_type=jnp.float32)
+        total = term if total is None else total + term
+    return total.astype(jnp.bfloat16)
+
+
+def second_kernel(row_count, weight_count, early_rows, place_ref, first_ref, *refs):
+    row_refs, refs = refs[:row_count], refs[row_count:]
+    weight_refs, refs = refs[:weight_count], refs[weight_count:]
+    down_refs, (hidden_ref, *refs) = refs[:2], refs[2:]
+    out_refs, (first_rows, down_own, down_near, down_sems, *scratch) = refs[:-8], refs[-8:]
+    sources, targets = (first_ref, *down_refs), (first_rows, down_own, down_near)
+    loads = [
+        pltpu.make_async_copy(ref, target, down_sems.at[index])
+        for index, (ref, target) in enumerate(zip(sources, targets))
+    ]
+    hidden = stream_hidden(row_refs, weight_refs, *scratch)
+    for load in loads:
+        load.start()
+    hidden_ref[...] = hidden
+    loads[0].wait()
+    first = first_rows[early_rows:]
+    second = hidden_ref[early_rows:]
+    col = 0
+    for load, weight in zip(loads[1:], (down_own, down_near)):
         load.wait()
-    up_pre = jnp.dot(rows[...], weights[1], preferred_element_type=jnp.float32)
-    out_ref[...] = (gate_pre / (1.0 + jnp.exp(-gate_pre)) * up_pre).astype(jnp.bfloat16)
-
-
-def hidden_of(row_parts, pairs):
-    rows = sum(part.shape[0] for part in row_parts)
-    depth, width = pairs[0][0].shape
-    weights = [weight for pair in pairs for weight in pair]
-    return pl.pallas_call(
-        functools.partial(hidden_kernel, len(row_parts)),
-        out_shape=jax.ShapeDtypeStruct((rows, width * len(pairs)), jnp.bfloat16),
-        in_specs=[HBM] * (len(row_parts) + len(weights)),
-        out_specs=VMEM,
-        scratch_shapes=[
-            pltpu.VMEM((rows, depth), jnp.bfloat16),
-            pltpu.VMEM((2, depth, width * len(pairs)), jnp.bfloat16),
-            pltpu.SemaphoreType.DMA((len(row_parts),)),
-            pltpu.SemaphoreType.DMA((len(weights),)),
-        ],
-        compiler_params=pltpu.CompilerParams(vmem_limit_bytes=56 * MIB),
-        cost_estimate=pl.CostEstimate(
-            flops=2 * rows * depth * width * len(weights),
-            bytes_accessed=2 * (rows * depth + len(weights) * depth * width),
-            transcendentals=rows * width * len(pairs),
-        ),
-        name="hidden",
-    )(*row_parts, *weights)
-
-
-def down_kernel(base, place_ref, first_ref, second_ref, own_ref, near_ref, *out_refs):
-    half = first_ref.shape[1] // 2
-    col = 0
-    for weight_ref in (own_ref, near_ref):
-        total = None
-        for j in range(4):
-            source = first_ref if j < 2 else second_ref
-            block = source[:, (j % 2) * half : (j % 2 + 1) * half]
-            start = pl.multiple_of((place_ref[0] ^ base ^ j) * half, half)
-            term = jnp.dot(
-                block, weight_ref[pl.ds(start, half), :], preferred_element_type=jnp.float32
-            )
-            total = term if total is None else total + term
-        total = total.astype(jnp.bfloat16)
+        total = down_rows(place_ref[0], first, second, weight)
         row = 0
         for ref in out_refs:
             ref[:, col : col + total.shape[1]] = total[row : row + ref.shape[0]]
@@ -195,31 +242,145 @@
         col += total.shape[1]
 
 
-def results_of(place, base, first, second, down_own, down_near, sizes):
-    width = 2 * down_own.shape[1]
+def second_hidden(place, first, row_parts, weights, downs, sizes, early):
+    rows = sum(sizes)
+    width = weights[0].shape[1] * len(weights) // 2
+    out_width = 2 * downs[0].shape[1]
+    outs = [jax.ShapeDtypeStruct((rows, width), jnp.bfloat16)]
+    outs += [jax.ShapeDtypeStruct((sizes[k], out_width), jnp.bfloat16) for k in early]
+    hidden, *results = pl.pallas_call(
+        functools.partial(second_kernel, len(row_parts), len(weights), sum(sizes[: early[0]])),
+        out_shape=outs,
+        in_specs=[SMEM, ANY] + [ANY] * (len(row_parts) + len(weights) + 2),
+        out_specs=[VMEM] * len(outs),
+        scratch_shapes=[
+            pltpu.VMEM(first.shape, jnp.bfloat16),
+            pltpu.VMEM(downs[0].shape, jnp.bfloat16),
+            pltpu.VMEM(downs[1].shape, jnp.bfloat16),
+            pltpu.SemaphoreType.DMA((3,)),
+        ]
+        + hidden_scratch(row_parts, weights),
+        compiler_params=pltpu.CompilerParams(vmem_limit_bytes=56 * MIB),
+        cost_estimate=pl.CostEstimate(flops=MIB, bytes_accessed=MIB, transcendentals=0),
+        name="second_hidden",
+    )(place, first, *row_parts, *weights, *downs)
+    return hidden, dict(zip(early, results))
+
+
+def late_kernel(far, sizes, early, place_ref, *refs):
+    first_ref, second_ref, first_far_ref, second_far_ref, own_ref, near_ref, *refs = refs
+    out_refs, (down_own, down_near, sems) = refs[:-3], refs[-3:]
+    loads = [
+        pltpu.make_async_copy(own_ref, down_own, sems.at[0]),
+        pltpu.make_async_copy(near_ref, down_near, sems.at[1]),
+    ]
+    for load in loads:
+        load.start()
+    later = [k for k in range(len(sizes)) if k not in early]
+    own_rows = sum(sizes[k] for k in later)
+    col = 0
+    for load, weight_ref in zip(loads, (down_own, down_near)):
+        load.wait()
+        total = down_rows(place_ref[0] ^ far, first_far_ref[...], second_far_ref[...], weight_ref)
+        width = total.shape[1]
+        row = 0
+        for k, ref in enumerate(out_refs):
+            at = 0 if k in early else sizes[k]
+            ref[at:, col : col + width] = total[row : row + sizes[k]]
+            row += sizes[k]
+        if later:
+            total = down_rows(place_ref[0], first_ref[:own_rows], second_ref[:own_rows], weight_ref)
+            row = 0
+            for k in later:
+                out_refs[k][: sizes[k], col : col + width] = total[row : row + sizes[k]]
+                row += sizes[k]
+        col += width
+
+
+def late_results(place, far, hidden_parts, downs, sizes, early):
+    out_width = 2 * downs[0].shape[1]
+    rows = [sizes[k] if k in early else 2 * sizes[k] for k in range(len(sizes))]
     return pl.pallas_call(
-        functools.partial(down_kernel, base),
-        out_shape=[jax.ShapeDtypeStruct((size, width), jnp.bfloat16) for size in sizes],
-        in_specs=[SMEM, VMEM, VMEM, VMEM, VMEM],
-        out_specs=[VMEM] * len(sizes),
-        compiler_params=pltpu.CompilerParams(vmem_limit_bytes=12 * MIB),
+        functools.partial(late_kernel, far, tuple(sizes), tuple(early)),
+        out_shape=[jax.ShapeDtypeStruct((count, out_width), jnp.bfloat16) for count in rows],
+        in_specs=[SMEM] + [VMEM] * 4 + [ANY] * 2,
+        out_specs=[VMEM] * len(rows),
+        scratch_shapes=[
+            pltpu.VMEM(downs[0].shape, jnp.bfloat16),
+            pltpu.VMEM(downs[1].shape, jnp.bfloat16),
+            pltpu.SemaphoreType.DMA((2,)),
+        ],
+        compiler_params=pltpu.CompilerParams(vmem_limit_bytes=56 * MIB),
         cost_estimate=pl.CostEstimate(
-            flops=2 * sum(sizes) * down_own.shape[0] * width,
+            flops=2 * sum(rows) * downs[0].shape[0] * out_width,
             bytes_accessed=4 * MIB,
             transcendentals=0,
         ),
-        name="down",
-    )(place, first, second, down_own, down_near)
-
-
-def combine_rows(mask, hits, share_rows, returned):
+        name="late_down",
+    )(place, *hidden_parts, *downs)
+
+
+def front_kernel(place_ref, *refs):
+    part_refs, weight_refs, refs = refs[:4], refs[4:7], refs[7:]
+    product_ref, gate_ref, rows, weights, row_sems, weight_sems = refs
+    tok = part_refs[0].shape[0]
+    copies = []
+    for j, ref in enumerate(part_refs):
+        start = pl.multiple_of((place_ref[0] ^ j) * tok, tok)
+        copies.append(pltpu.make_async_copy(ref, rows.at[pl.ds(start, tok)], row_sems.at[j]))
+    loads = [
+        pltpu.make_async_copy(ref, weights.at[index], weight_sems.at[index])
+        for index, ref in enumerate(weight_refs)
+    ]
+    for copy in copies + loads:
+        copy.start()
+    for copy in copies:
+        copy.wait()
+    loads[0].wait()
+    in_gate = jnp.dot(rows[...], weights[0], preferred_element_type=jnp.float32)
+    loads[1].wait()
+    values = jnp.dot(rows[...], weights[1], preferred_element_type=jnp.float32)
+    product_ref[...] = (in_gate * values).astype(jnp.bfloat16)
+    loads[2].wait()
+    gate_ref[...] = jnp.dot(rows[...], weights[2], preferred_element_type=jnp.float32)
+
+
+def mixer_front(place, parts, weights):
+    rows = sum(part.shape[0] for part in parts)
+    depth, width = weights[0].shape
+    return pl.pallas_call(
+        front_kernel,
+        out_shape=[
+            jax.ShapeDtypeStruct((rows, width), jnp.bfloat16),
+            jax.ShapeDtypeStruct((rows, width), jnp.float32),
+        ],
+        in_specs=[SMEM] + [ANY] * 7,
+        out_specs=[VMEM, VMEM],
+        scratch_shapes=[
+            pltpu.VMEM((rows, depth), jnp.bfloat16),
+            pltpu.VMEM((3, depth, width), jnp.bfloat16),
+            pltpu.SemaphoreType.DMA((4,)),
+            pltpu.SemaphoreType.DMA((3,)),
+        ],
+        compiler_params=pltpu.CompilerParams(vmem_limit_bytes=40 * MIB),
+        cost_estimate=pl.CostEstimate(
+            flops=6 * rows * depth * width, bytes_accessed=8 * MIB, transcendentals=0
+        ),
+        name="mixer_front",
+    )(place, *parts, *weights)
+
+
+def share_masks(mask, hits, share_rows):
     share_of = jnp.sum(jnp.where(hits, share_rows[:, None, :], 0.0), axis=0)
     mixed = jnp.where(mask, share_of[:, None, :], 0.0).reshape(-1, mask.shape[2])
     high = mixed.astype(jnp.bfloat16)
-    low = (mixed - high.astype(jnp.float32)).astype(jnp.bfloat16)
+    return high, (mixed - high.astype(jnp.float32)).astype(jnp.bfloat16)
+
+
+def combine_rows(masks, returned):
     dims = (((0,), (0,)), ((), ()))
-    total = lax.dot_general(high, returned, dims, preferred_element_type=jnp.float32)
-    total = total + lax.dot_general(low, returned, dims, preferred_element_type=jnp.float32)
+    total = lax.dot_general(masks[0], returned, dims, preferred_element_type=jnp.float32)
+    total = total + lax.dot_general(masks[1], returned, dims, preferred_element_type=jnp.float32)
     return total.astype(jnp.bfloat16)
 
 
@@ -270,44 +431,56 @@
 
     hits_own, mask_own = slot_masks(block_of(route_ids, 0).T, labels, slot_cap)
     hits_far, mask_far = slot_masks(block_of(route_ids, far).T, labels, slot_cap)
+    shares = route_weights / jnp.sum(route_weights, axis=1, keepdims=True)
+    masks_own = share_masks(mask_own, hits_own, block_of(shares, 0).T)
+    masks_far = share_masks(mask_far, hits_far, block_of(shares, far).T)
+    chan_width = in_gate_weight.shape[1]
+    tap_count = conv_taps.shape[0]
+    tap_rows = lax.dynamic_slice_in_dim(conv_taps, tp_index * chan_width, chan_width, 1)
+    tap_rows = [tap_rows[tap_index] for tap_index in range(tap_count)]
+    mixer_normed = rms_rows(mixer_in, mixer_gain)
     place = jnp.where(jnp.arange(2) == 0, tp_index, ep_index).astype(jnp.int32)
     sizes = [slot_cap] * experts if direct else [experts * slot_cap]
+    early = list(range(len(sizes) // 2, len(sizes)))
     outgoing = dispatched(
         place, route_ids.T, expert_in, expert_gain[None, :], sizes, direct, slot_cap
     )
-    slots_in = exchange(outgoing, "ep", direct)
-
-    first = hidden_of(slots_in, [(gates[j], ups[j]) for j in (0, near)])
-    gates[far ^ near] = swapped(after(gates[far], first), "tp", near)
+    arrived = exchange(dict(enumerate(outgoing)), "ep", direct)
+    gates[far ^ near] = swapped(gates[far], "tp", near)
+    ready = (masks_own, masks_far, mixer_normed, gates[far ^ near])
+    ready += (gates[near], ups[near], down_near)
+    arrived[0] = after(arrived[0], *ready)
+    slots_in = [arrived[k] for k in range(len(sizes))]
+
+    first = first_hidden(slots_in, [half[j] for j in (0, near) for half in (gates, ups)])
     ups[far ^ near] = swapped(after(ups[far], first), "tp", near)
-    second = hidden_of(slots_in, [(gates[j], ups[j]) for j in (far, far ^ near)])
+    downs = (down_own, down_near)
+    second, done_own = second_hidden(
+        place,
+        first,
+        slots_in,
+        [half[j] for j in (far, far ^ near) for half in (gates, ups)],
+        downs,
+        sizes,
+        early,
+    )
     first_far = swapped(after(first, ups[far]), "tp", far)
     second_far = swapped(second, "tp", far)
-    done_own = results_of(place, 0, first, second, down_own, down_near, sizes)
     back_own = exchange(done_own, "ep", direct)
 
-    normed = {0: after(rms_rows(mixer_in, mixer_gain), ups[far], first)}
+    normed = {0: after(mixer_normed, ups[far], first)}
     normed[far] = swapped(normed[0], "tp", far)
     normed[near] = swapped(normed[0], "tp", near)
-    normed = {j: after(normed[j], done_own[0]) for j in normed}
+    normed = {j: after(normed[j], second) for j in normed}
     normed[far ^ near] = swapped(normed[far], "tp", near)
-    mixer_rows = jnp.zeros((tp_count * tok_dev, mixer_in.shape[1]), jnp.bfloat16)
-    for j in order:
-        mixer_rows = lax.dynamic_update_slice_in_dim(
-            mixer_rows, normed[j], (tp_index ^ j) * tok_dev, 0
-        )
-    chan_width = in_gate_weight.shape[1]
-    in_gate = jnp.dot(mixer_rows, in_gate_weight, preferred_element_type=jnp.float32)
-    values = jnp.dot(mixer_rows, value_weight, preferred_element_type=jnp.float32)
-    product = (in_gate * values).astype(jnp.bfloat16)
-    out_gate = jnp.dot(mixer_rows, out_gate_weight, preferred_element_type=jnp.float32)
-    tap_count = conv_taps.shape[0]
+    product, out_gate = mixer_front(
+        place, [normed[j] for j in order], [in_gate_weight, value_weight, out_gate_weight]
+    )
     row_count = product.shape[0]
     rim_rows = lax.ppermute(
         product[row_count - (tap_count - 1) :], "ep", [(i, i + 1) for i in range(ep_count - 1)]
     )
     extended = jnp.concatenate([rim_rows, product], axis=0).astype(jnp.float32)
-    tap_rows = lax.dynamic_slice_in_dim(conv_taps, tp_index * chan_width, chan_width, 1)
     conv_sum = tap_rows[0] * extended[0:row_count]
     for tap_index in range(1, tap_count):
         conv_sum = conv_sum + tap_rows[tap_index] * extended[tap_index : tap_index + row_count]
@@ -322,15 +495,13 @@
         )
         mixer_sum = term if mixer_sum is None else mixer_sum + term
     first_far = after(first_far, gated[0])
-    done_far = results_of(place, far, first_far, second_far, down_own, down_near, sizes)
-    back_far = exchange(done_far, "ep", direct)
-
-    def returned(parts):
-        return jnp.concatenate(parts, axis=0)
-
-    shares = route_weights / jnp.sum(route_weights, axis=1, keepdims=True)
-    mixed_own = combine_rows(mask_own, hits_own, block_of(shares, 0).T, returned(back_own))
-    mixed_far = combine_rows(mask_far, hits_far, block_of(shares, far).T, returned(back_far))
+    late = late_results(place, far, (first, second, first_far, second_far), downs, sizes, early)
+    back_late = exchange(dict(enumerate(late)), "ep", direct)
+    back_late[0] = after(back_late[0], mixer_sum)
+    own_rows = [back_own[k] if k in early else back_late[k][: sizes[k]] for k in range(len(sizes))]
+    far_rows = [back_late[k][-sizes[k] :] for k in range(len(sizes))]
+    mixed_own = combine_rows(masks_own, jnp.concatenate(own_rows, axis=0))
+    mixed_far = combine_rows(masks_far, jnp.concatenate(far_rows, axis=0))
     mixed = jnp.concatenate([mixed_own, mixed_far], axis=0)
     col_width = down_own.shape[1]
     mixed_near = swapped(mixed[:, col_width:], "tp", near)

time: 157 us -> 179 us (1.14)
  waiting for transfers between devices: 62.9 us -> 75.5 us
  Pallas kernels: 17.1 us -> 26 us
  matrix products: 7.83 us -> 3.66 us
  starting transfers between devices: 52.1 us -> 55.8 us
    ppermute x37 -> x34, waiting for transfers between devices: 61.8 us -> 75.5 us  [swapped(): lax.ppermute(value, axis, [(source, source ^ mask) for source in range(co...]
    pallas_call x4, Pallas kernels: 13.6 us -> 22.5 us  [the longest x1 7.28 us: second_hidden(): pl.pallas_call(functools.partial(second_kernel, len(row_parts), len(weigh...]
    unnamed x58 -> x76, local copies, waits for them, and re-layouts: 3.35 us -> 8.03 us
    dynamic_update_slice x4 -> x0, local copies, waits for them, and re-layouts: 3.15 us -> none  [on_device(): lax.dynamic_update_slice_in_dim(mixer_rows, normed[j], (tp_index ^ j) * t...]
    ppermute x37 -> x34, starting transfers between devices: 49.1 us -> 52.2 us  [swapped(): lax.ppermute(value, axis, [(source, source ^ mask) for source in range(co...]
    dot_general x7 -> x4, matrix products: 4.18 us -> 1.16 us  [the longest x2 0.58 us: combine_rows(): lax.dot_general(masks[0], returned, dims, preferred_element_type=jnp.floa...]
  transfers between devices with their start and end apart: 38 -> 35, of which waited for: 20 -> 19; matrix products, arithmetic and copies ran while one was open for 11% -> 6% of each run, Pallas kernels for 9% -> 12%
where the time goes in v1:
time: 179 us
  waiting for transfers between devices  75.5 us (42%)
  starting transfers between devices  55.8 us (31%)
  Pallas kernels  26 us (15%)
  local copies, waits for them, and re-layouts  10 us (6%)
  other arithmetic  6.42 us (4%)
  matrix products  3.66 us (2%)
    ppermute x34, waiting for transfers between devices, swapped(): lax.ppermute(value, axis, [(source, source ^ mask) for source in range(co...  75.5 us
    ppermute x34, starting transfers between devices, swapped(): lax.ppermute(value, axis, [(source, source ^ mask) for source in range(co...  52.2 us
    unnamed x76, local copies, waits for them, and re-layouts  8.03 us
    pallas_call x1, Pallas kernels, second_hidden(): pl.pallas_call(functools.partial(second_kernel, len(row_parts), len(weigh...  7.28 us
    pallas_call x1, Pallas kernels, first_hidden(): pl.pallas_call(functools.partial(first_kernel, len(row_parts)), out_shape...  5.12 us
    pallas_call x1, Pallas kernels, mixer_front(): pl.pallas_call(front_kernel, out_shape=[jax.ShapeDtypeStruct((rows, width...  5.1 us
    pallas_call x1, Pallas kernels, late_results(): pl.pallas_call(functools.partial(late_kernel, far, tuple(sizes), tuple(ea...  5.04 us
    ppermute x1, starting transfers between devices, on_device(): lax.ppermute(product[row_count - (tap_count - 1):], 'ep', [(i, i + 1) for...  3.61 us
  transfers between devices with their start and end apart: 35, of which 19 were waited for; matrix products, arithmetic and copies ran while one was open for 6% of the time, Pallas kernels for 12%

profile of v1, /device:TPU:0, one launch (start us, length us, event | category | flops | bytes accessed | tf_op | source)
XLA Modules:
  0.0 178.7 jit_solution(12784756581104336135)
XLA Ops:
  0.6 3.0 %collective-permute-start.1 = (bf16[2048,256]{1,0:T(8,128)(2,1)}, bf16[2048,256]{1,0:T(8,128)(2,1)}, u32[]{:S(2)}, u32[]{:S(2)}) collective-permute-start(bf16[2048,256]{1,0:T(8,128)(2,1)} %bitcast.66), channel_id=1, source_target_pairs={{0,2},{1,3},{2,0},{3,1},{4,6},{5,7},{6,4},{7,5},{8,10},{9,11},{10,... | collective-permute-start | bytes 3145736 | tf_op jit(solution)/shard_map/ppermute | solution.py:22
  4.7 3.5 %dispatch.1 = (bf16[48,2048]{1,0:T(8,128)(2,1)}, bf16[48,2048]{1,0:T(8,128)(2,1)}, bf16[48,2048]{1,0:T(8,128)(2,1)}, bf16[48,2048]{1,0:T(8,128)(2,1)}, bf16[48,2...) custom-call(s32[2]{0:T(128)} %compare_select_fusion.2.place_ref, ...), custom_call_target="tpu_custom_call" | custom-call | flops 150994944 | bytes 2097152 | tf_op jit(solution)/shard_map/dispatch/pallas_call | solution.py:116
  8.2 3.6 %collective-permute-start.10 = (bf16[48,2048]{1,0:T(8,128)(2,1)}, bf16[48,2048]{1,0:T(8,128)(2,1)S(1)}, u32[]{:S(2)}, u32[]{:S(2)}) collective-permute-start(bf16[48,2048]{1,0:T(8,128)(2,1)} %get-tuple-element.40), channel_id=1, source_target_pairs={{0,20},{4,16},{8,28},{12,24},{16,4},{20,0},{24,12},{28,8},{1,21},{... | collective-permute-start | bytes 589832 | tf_op jit(solution)/shard_map/ppermute | solution.py:22
  15.7 10.8 %collective-permute-done.10.refs_5_ = bf16[48,2048]{1,0:T(8,128)(2,1)S(1)} collective-permute-done((bf16[48,2048]{1,0:T(8,128)(2,1)}, bf16[48,2048]{1,0:T(8,128)(2,1)S(1)}, u32[]{:S(2)}, u32[]{:S(2)}) %collective-permute-start.10) | collective-permute-done | bytes 196640 | tf_op jit(solution)/shard_map/ppermute | solution.py:22
  28.4 4.9 %collective-permute-start.12 = (bf16[48,2048]{1,0:T(8,128)(2,1)}, bf16[48,2048]{1,0:T(8,128)(2,1)S(1)}, u32[]{:S(2)}, u32[]{:S(2)}) collective-permute-start(bf16[48,2048]{1,0:T(8,128)(2,1)} %get-tuple-element.42), channel_id=1, source_target_pairs={{0,28},{4,24},{8,20},{12,16},{16,12},{20,8},{24,4},{28,0},{1,29},{... | collective-permute-start | bytes 589832 | tf_op jit(solution)/shard_map/ppermute | solution.py:22
  33.4 5.8 %collective-permute-done.12.refs_7_ = bf16[48,2048]{1,0:T(8,128)(2,1)S(1)} collective-permute-done((bf16[48,2048]{1,0:T(8,128)(2,1)}, bf16[48,2048]{1,0:T(8,128)(2,1)S(1)}, u32[]{:S(2)}, u32[]{:S(2)}) %collective-permute-start.12) | collective-permute-done | bytes 196640 | tf_op jit(solution)/shard_map/ppermute | solution.py:22
  43.3 3.9 %collective-permute-start.7 = (bf16[48,2048]{1,0:T(8,128)(2,1)}, bf16[48,2048]{1,0:T(8,128)(2,1)S(1)}, u32[]{:S(2)}, u32[]{:S(2)}) collective-permute-start(bf16[48,2048]{1,0:T(8,128)(2,1)} %get-tuple-element.37), channel_id=1, source_target_pairs={{0,8},{4,12},{8,0},{12,4},{16,24},{20,28},{24,16},{28,20},{1,9},{5... | collective-permute-start | bytes 589832 | tf_op jit(solution)/shard_map/ppermute | solution.py:22
  47.2 3.0 %collective-permute-start.9 = (bf16[48,2048]{1,0:T(8,128)(2,1)}, bf16[48,2048]{1,0:T(8,128)(2,1)S(1)}, u32[]{:S(2)}, u32[]{:S(2)}) collective-permute-start(bf16[48,2048]{1,0:T(8,128)(2,1)} %get-tuple-element.39), channel_id=1, source_target_pairs={{0,16},{4,20},{8,24},{12,28},{16,0},{20,4},{24,8},{28,12},{1,17},{... | collective-permute-start | bytes 589832 | tf_op jit(solution)/shard_map/ppermute | solution.py:22
  51.9 5.4 %collective-permute-done.7.refs_2_ = bf16[48,2048]{1,0:T(8,128)(2,1)S(1)} collective-permute-done((bf16[48,2048]{1,0:T(8,128)(2,1)}, bf16[48,2048]{1,0:T(8,128)(2,1)S(1)}, u32[]{:S(2)}, u32[]{:S(2)}) %collective-permute-start.7) | collective-permute-done | bytes 196640 | tf_op jit(solution)/shard_map/ppermute | solution.py:22
  57.3 2.6 %collective-permute-done.8.refs_3_ = bf16[48,2048]{1,0:T(8,128)(2,1)S(1)} collective-permute-done((bf16[48,2048]{1,0:T(8,128)(2,1)}, bf16[48,2048]{1,0:T(8,128)(2,1)S(1)}, u32[]{:S(2)}, u32[]{:S(2)}) %collective-permute-start.8) | collective-permute-done | bytes 196640 | tf_op jit(solution)/shard_map/ppermute | solution.py:22
  61.2 5.1 %first_hidden.1.first_ref.refs_0_ = bf16[384,512]{1,0:T(8,128)(2,1)} custom-call(bf16[48,2048]{1,0:T(8,128)(2,1)} %get-tuple-element.35.refs_0_, bf16[48,2048]{1,0:T(8,128)(2,1)} %copy-done.13, bf16[48,2048]{1,0:T(8,128)(2,1)} %copy-done.14, bf16[48,2048]{1,0:T(8,128)(2,1)} %copy-done.15, bf16[48,2048]{1,0:T(8,128)(2,1)} %copy-done.16, ...), custom_call_target="tpu_custom_call" | custom-call | flops 1610612736 | bytes 5767168 | tf_op jit(solution)/shard_map/first_hidden/pallas_call | solution.py:193
  67.1 2.0 %collective-permute-done.13.refs_11_ = bf16[2048,256]{1,0:T(8,128)(2,1)S(1)} collective-permute-done((bf16[2048,256]{1,0:T(8,128)(2,1)S(1)}, bf16[2048,256]{1,0:T(8,128)(2,1)S(1)}, u32[]{:S(2)}, u32[]{:S(2)}) %collective-permute-start.13) | collective-permute-done | bytes 1048608 | tf_op jit(solution)/shard_map/ppermute | solution.py:22
  70.1 7.3 %second_hidden.1 = (bf16[384,512]{1,0:T(8,128)(2,1)}, bf16[48,1024]{1,0:T(8,128)(2,1)}, bf16[48,1024]{1,0:T(8,128)(2,1)}, bf16[48,1024]{1,0:T(8,128)(2,1)}, bf16[48,1024]{1,0:T(8,128)(2,1)}) custom-call(s32[2]{0:T(128)} %compare_select_fusion.2.place_ref, bf16[384,512]{1,0:T(8,128)(2,1)} %first_hidden.1.first_ref.refs_0_, ...), custom_call_target="tpu_custom_call" | custom-call | flops 1048576 | bytes 1048576 | tf_op jit(solution)/shard_map/second_hidden/pallas_call | solution.py:251
  84.6 5.1 %mixer_front.1 = (bf16[384,512]{1,0:T(8,128)(2,1)S(1)}, f32[384,512]{1,0:T(8,128)S(1)}) custom-call(s32[2]{0:T(128)S(1)} %copy-done.1, bf16[96,2048]{1,0:T(8,128)(2,1)S(1)} %fusion.4.refs_0_, bf16[96,2048]{1,0:T(8,128)(2,1)S(1)} %collective-permute-done.14.refs_1_, bf16[96,2048]{1,0:T(8,128)(2,1)S(1)} %collective-permute-done.15.refs_2_, ...), custom_call_target="tpu_custom_call" | custom-call | flops 2415919104 | bytes 8388608 | tf_op jit(solution)/shard_map/mixer_front/pallas_call | solution.py:351
  89.7 3.6 %collective-permute-start.17 = (bf16[2,512]{1,0:T(2,128)(2,1)S(1)}, bf16[2,512]{1,0:T(2,128)(2,1)S(1)}, u32[]{:S(2)}, u32[]{:S(2)}) collective-permute-start(bf16[2,512]{1,0:T(2,128)(2,1)S(1)} %slice.61), channel_id=1, source_target_pairs={{0,4},{4,8},{8,12},{12,16},{16,20},{20,24},{24,28},{1,5},{5,9},{9,... | collective-permute-start | bytes 6152 | tf_op jit(solution)/shard_map/ppermute | solution.py:480
  97.4 3.3 %collective-permute-start.26 = (bf16[48,1024]{1,0:T(8,128)(2,1)}, bf16[48,1024]{1,0:T(8,128)(2,1)S(1)}, u32[]{:S(2)}, u32[]{:S(2)}) collective-permute-start(bf16[48,1024]{1,0:T(8,128)(2,1)} %get-tuple-element.58), channel_id=1, source_target_pairs={{0,16},{4,20},{8,24},{12,28},{16,0},{20,4},{24,8},{28,12},{1,17},{... | collective-permute-start | bytes 294920 | tf_op jit(solution)/shard_map/ppermute | solution.py:22
  100.7 5.9 %collective-permute-done.21.refs_2_ = bf16[384,512]{1,0:T(8,128)(2,1)} collective-permute-done((bf16[384,512]{1,0:T(8,128)(2,1)}, bf16[384,512]{1,0:T(8,128)(2,1)}, u32[]{:S(2)}, u32[]{:S(2)}) %collective-permute-start.21) | collective-permute-done | bytes 393248 | tf_op jit(solution)/shard_map/ppermute | solution.py:22
  106.6 2.3 %collective-permute-start.27 = (bf16[48,1024]{1,0:T(8,128)(2,1)S(1)}, bf16[48,1024]{1,0:T(8,128)(2,1)S(1)}, u32[]{:S(2)}, u32[]{:S(2)}) collective-permute-start(bf16[48,1024]{1,0:T(8,128)(2,1)S(1)} %copy-done.28), channel_id=1, source_target_pairs={{0,20},{4,16},{8,28},{12,24},{16,4},{20,0},{24,12},{28,8},{1,21},{... | collective-permute-start | bytes 294920 | tf_op jit(solution)/shard_map/ppermute | solution.py:22
  108.9 6.1 %collective-permute-done.22.refs_3_ = bf16[384,512]{1,0:T(8,128)(2,1)} collective-permute-done((bf16[384,512]{1,0:T(8,128)(2,1)}, bf16[384,512]{1,0:T(8,128)(2,1)}, u32[]{:S(2)}, u32[]{:S(2)}) %collective-permute-start.22) | collective-permute-done | bytes 393248 | tf_op jit(solution)/shard_map/ppermute | solution.py:22
  115.0 2.5 %collective-permute-start.28 = (bf16[48,1024]{1,0:T(8,128)(2,1)S(1)}, bf16[48,1024]{1,0:T(8,128)(2,1)S(1)}, u32[]{:S(2)}, u32[]{:S(2)}) collective-permute-start(bf16[48,1024]{1,0:T(8,128)(2,1)S(1)} %copy-done.27), channel_id=1, source_target_pairs={{0,24},{4,28},{8,16},{12,20},{16,8},{20,12},{24,0},{28,4},{1,25},{... | collective-permute-start | bytes 294920 | tf_op jit(solution)/shard_map/ppermute | solution.py:22
  117.5 5.0 %late_down.1 = (bf16[96,1024]{1,0:T(8,128)(2,1)}, bf16[96,1024]{1,0:T(8,128)(2,1)}, bf16[96,1024]{1,0:T(8,128)(2,1)}, bf16[96,1024]{1,0:T(8,128)(2,1)}, bf16[48,...) custom-call(s32[2]{0:T(128)} %compare_select_fusion.2.place_ref, ...), custom_call_target="tpu_custom_call" | custom-call | flops 1207959552 | bytes 4194304 | tf_op jit(solution)/shard_map/late_down/pallas_call | solution.py:303
  122.5 3.0 %collective-permute-start.29 = (bf16[48,1024]{1,0:T(8,128)(2,1)S(1)}, bf16[48,1024]{1,0:T(8,128)(2,1)S(1)}, u32[]{:S(2)}, u32[]{:S(2)}) collective-permute-start(bf16[48,1024]{1,0:T(8,128)(2,1)S(1)} %copy-done.26), channel_id=1, source_target_pairs={{0,28},{4,24},{8,20},{12,16},{16,12},{20,8},{24,4},{28,0},{1,29},{... | collective-permute-start | bytes 294920 | tf_op jit(solution)/shard_map/ppermute | solution.py:22
  128.4 5.8 %collective-permute-done.23 = bf16[96,1024]{1,0:T(8,128)(2,1)S(1)} collective-permute-done((bf16[96,1024]{1,0:T(8,128)(2,1)S(1)}, bf16[96,1024]{1,0:T(8,128)(2,1)S(1)}, u32[]{:S(2)}, u32[]{:S(2)}) %collective-permute-start.23) | collective-permute-done | bytes 196640 | tf_op jit(solution)/shard_map/ppermute | solution.py:22
  134.2 6.1 %collective-permute-done.24 = bf16[96,1024]{1,0:T(8,128)(2,1)S(1)} collective-permute-done((bf16[96,1024]{1,0:T(8,128)(2,1)S(1)}, bf16[96,1024]{1,0:T(8,128)(2,1)S(1)}, u32[]{:S(2)}, u32[]{:S(2)}) %collective-permute-start.24) | collective-permute-done | bytes 196640 | tf_op jit(solution)/shard_map/ppermute | solution.py:22
  140.6 6.3 %collective-permute-done.25 = bf16[96,1024]{1,0:T(8,128)(2,1)S(1)} collective-permute-done((bf16[96,1024]{1,0:T(8,128)(2,1)S(1)}, bf16[96,1024]{1,0:T(8,128)(2,1)S(1)}, u32[]{:S(2)}, u32[]{:S(2)}) %collective-permute-start.25) | collective-permute-done | bytes 196640 | tf_op jit(solution)/shard_map/ppermute | solution.py:22
  148.7 4.4 %collective-permute-done.30 = bf16[48,1024]{1,0:T(8,128)(2,1)S(1)} collective-permute-done((bf16[48,1024]{1,0:T(8,128)(2,1)S(1)}, bf16[48,1024]{1,0:T(8,128)(2,1)S(1)}, u32[]{:S(2)}, u32[]{:S(2)}) %collective-permute-start.30) | collective-permute-done | bytes 98336 | tf_op jit(solution)/shard_map/ppermute | solution.py:22
  153.1 2.3 %collective-permute-start.31 = (bf16[48,1024]{1,0:T(8,128)(2,1)S(1)}, bf16[48,1024]{1,0:T(8,128)(2,1)S(1)}, u32[]{:S(2)}, u32[]{:S(2)}) collective-permute-start(bf16[48,1024]{1,0:T(8,128)(2,1)S(1)} %copy-done.31), channel_id=1, source_target_pairs={{0,20},{4,16},{8,28},{12,24},{16,4},{20,0},{24,12},{28,8},{1,21},{... | collective-permute-start | bytes 294920 | tf_op jit(solution)/shard_map/ppermute | solution.py:22
  155.5 4.2 %collective-permute-done.31 = bf16[48,1024]{1,0:T(8,128)(2,1)S(1)} collective-permute-done((bf16[48,1024]{1,0:T(8,128)(2,1)S(1)}, bf16[48,1024]{1,0:T(8,128)(2,1)S(1)}, u32[]{:S(2)}, u32[]{:S(2)}) %collective-permute-start.31) | collective-permute-done | bytes 98336 | tf_op jit(solution)/shard_map/ppermute | solution.py:22
  159.7 3.9 %collective-permute-start.32 = (bf16[48,1024]{1,0:T(8,128)(2,1)S(1)}, bf16[48,1024]{1,0:T(8,128)(2,1)S(1)}, u32[]{:S(2)}, u32[]{:S(2)}) collective-permute-start(bf16[48,1024]{1,0:T(8,128)(2,1)S(1)} %copy-done.30), channel_id=1, source_target_pairs={{0,24},{4,28},{8,16},{12,20},{16,8},{20,12},{24,0},{28,4},{1,25},{... | collective-permute-start | bytes 294920 | tf_op jit(solution)/shard_map/ppermute | solution.py:22
  163.6 2.7 %collective-permute-done.32 = bf16[48,1024]{1,0:T(8,128)(2,1)S(1)} collective-permute-done((bf16[48,1024]{1,0:T(8,128)(2,1)S(1)}, bf16[48,1024]{1,0:T(8,128)(2,1)S(1)}, u32[]{:S(2)}, u32[]{:S(2)}) %collective-permute-start.32) | collective-permute-done | bytes 98336 | tf_op jit(solution)/shard_map/ppermute | solution.py:22
  166.3 6.1 %collective-permute-start.33 = (bf16[48,1024]{1,0:T(8,128)(2,1)S(1)}, bf16[48,1024]{1,0:T(8,128)(2,1)S(1)}, u32[]{:S(2)}, u32[]{:S(2)}) collective-permute-start(bf16[48,1024]{1,0:T(8,128)(2,1)S(1)} %copy-done.29), channel_id=1, source_target_pairs={{0,28},{4,24},{8,20},{12,16},{16,12},{20,8},{24,4},{28,0},{1,29},{... | collective-permute-start | bytes 294920 | tf_op jit(solution)/shard_map/ppermute | solution.py:22
  172.5 2.6 %collective-permute-done.33 = bf16[48,1024]{1,0:T(8,128)(2,1)S(1)} collective-permute-done((bf16[48,1024]{1,0:T(8,128)(2,1)S(1)}, bf16[48,1024]{1,0:T(8,128)(2,1)S(1)}, u32[]{:S(2)}, u32[]{:S(2)}) %collective-permute-start.33) | collective-permute-done | bytes 98336 | tf_op jit(solution)/shard_map/ppermute | solution.py:22
  (157 shorter events, 35.5 us)
Async XLA Ops:
  0.6 26.5 %collective-permute-start.1 = (bf16[2048,256]{1,0:T(8,128)(2,1)}, bf16[2048,256]{1,0:T(8,128)(2,1)}, u32[]{:S(2)}, u32[]{:S(2)}) collective-permute-start(bf16[2048,256]{1,0:T(8,128)(2,1)} %bitcast.66), channel_id=1, source_target_pairs={{0,2},{1,3},{2,0},{3,1},{4,6},{5,7},{6,4},{7,5},{8,10},{9,11},{10,... | collective-permute-start | bytes 3145736 | tf_op jit(solution)/shard_map/ppermute | solution.py:22
  3.7 39.6 %collective-permute-start.3 = (bf16[2048,256]{1,0:T(8,128)(2,1)}, bf16[2048,256]{1,0:T(8,128)(2,1)S(1)}, u32[]{:S(2)}, u32[]{:S(2)}) collective-permute-start(bf16[2048,256]{1,0:T(8,128)(2,1)} %bitcast.67), channel_id=1, source_target_pairs={{0,1},{1,0},{2,3},{3,2},{4,5},{5,4},{6,7},{7,6},{8,9},{9,8},{10,11... | collective-permute-start | bytes 3145736 | tf_op jit(solution)/shard_map/ppermute | solution.py:22
  3.7 38.1 %collective-permute-start.5 = (bf16[1024,512]{1,0:T(8,128)(2,1)}, bf16[1024,512]{1,0:T(8,128)(2,1)}, u32[]{:S(2)}, u32[]{:S(2)}) collective-permute-start(bf16[1024,512]{1,0:T(8,128)(2,1)} %bitcast.72), channel_id=1, source_target_pairs={{0,1},{1,0},{2,3},{3,2},{4,5},{5,4},{6,7},{7,6},{8,9},{9,8},{10,11... | collective-permute-start | bytes 3145736 | tf_op jit(solution)/shard_map/ppermute | solution.py:22
  8.2 18.3 %collective-permute-start.10 = (bf16[48,2048]{1,0:T(8,128)(2,1)}, bf16[48,2048]{1,0:T(8,128)(2,1)S(1)}, u32[]{:S(2)}, u32[]{:S(2)}) collective-permute-start(bf16[48,2048]{1,0:T(8,128)(2,1)} %get-tuple-element.40), channel_id=1, source_target_pairs={{0,20},{4,16},{8,28},{12,24},{16,4},{20,0},{24,12},{28,8},{1,21},{... | collective-permute-start | bytes 589832 | tf_op jit(solution)/shard_map/ppermute | solution.py:22
  11.8 16.5 %collective-permute-start.11 = (bf16[48,2048]{1,0:T(8,128)(2,1)}, bf16[48,2048]{1,0:T(8,128)(2,1)S(1)}, u32[]{:S(2)}, u32[]{:S(2)}) collective-permute-start(bf16[48,2048]{1,0:T(8,128)(2,1)} %get-tuple-element.41), channel_id=1, source_target_pairs={{0,24},{4,28},{8,16},{12,20},{16,8},{20,12},{24,0},{28,4},{1,25},{... | collective-permute-start | bytes 589832 | tf_op jit(solution)/shard_map/ppermute | solution.py:22
  26.5 20.7 %collective-permute-start.4 = (bf16[2048,256]{1,0:T(8,128)(2,1)}, bf16[2048,256]{1,0:T(8,128)(2,1)S(1)}, u32[]{:S(2)}, u32[]{:S(2)}) collective-permute-start(bf16[2048,256]{1,0:T(8,128)(2,1)} %bitcast.69), channel_id=1, source_target_pairs={{0,1},{1,0},{2,3},{3,2},{4,5},{5,4},{6,7},{7,6},{8,9},{9,8},{10,11... | collective-permute-start | bytes 3145736 | tf_op jit(solution)/shard_map/ppermute | solution.py:22
  27.2 20.0 %collective-permute-start.2 = (bf16[2048,256]{1,0:T(8,128)(2,1)}, bf16[2048,256]{1,0:T(8,128)(2,1)S(1)}, u32[]{:S(2)}, u32[]{:S(2)}) collective-permute-start(bf16[2048,256]{1,0:T(8,128)(2,1)} %collective-permute-done.1.refs_8_), channel_id=1, source_target_pairs={{0,1},{1,0},{2,3},{3,2},{4,5},{5,4},{6,7},{7,6},{8,9},{9,8},{10,11... | collective-permute-start | bytes 3145736 | tf_op jit(solution)/shard_map/ppermute | solution.py:22
  28.4 10.8 %collective-permute-start.12 = (bf16[48,2048]{1,0:T(8,128)(2,1)}, bf16[48,2048]{1,0:T(8,128)(2,1)S(1)}, u32[]{:S(2)}, u32[]{:S(2)}) collective-permute-start(bf16[48,2048]{1,0:T(8,128)(2,1)} %get-tuple-element.42), channel_id=1, source_target_pairs={{0,28},{4,24},{8,20},{12,16},{16,12},{20,8},{24,4},{28,0},{1,29},{... | collective-permute-start | bytes 589832 | tf_op jit(solution)/shard_map/ppermute | solution.py:22
  39.1 27.3 %collective-permute-start = (bf16[2048,256]{1,0:T(8,128)(2,1)}, bf16[2048,256]{1,0:T(8,128)(2,1)S(1)}, u32[]{:S(2)}, u32[]{:S(2)}) collective-permute-start(bf16[2048,256]{1,0:T(8,128)(2,1)} %bitcast.70), channel_id=1, source_target_pairs={{0,2},{1,3},{2,0},{3,1},{4,6},{5,7},{6,4},{7,5},{8,10},{9,11},{10,... | collective-permute-start | bytes 3145736 | tf_op jit(solution)/shard_map/ppermute | solution.py:22
  41.8 10.1 %collective-permute-start.6 = (bf16[48,2048]{1,0:T(8,128)(2,1)}, bf16[48,2048]{1,0:T(8,128)(2,1)S(1)}, u32[]{:S(2)}, u32[]{:S(2)}) collective-permute-start(bf16[48,2048]{1,0:T(8,128)(2,1)} %get-tuple-element.36), channel_id=1, source_target_pairs={{0,4},{4,0},{8,12},{12,8},{16,20},{20,16},{24,28},{28,24},{1,5},{5... | collective-permute-start | bytes 589832 | tf_op jit(solution)/shard_map/ppermute | solution.py:22
  43.3 14.1 %collective-permute-start.7 = (bf16[48,2048]{1,0:T(8,128)(2,1)}, bf16[48,2048]{1,0:T(8,128)(2,1)S(1)}, u32[]{:S(2)}, u32[]{:S(2)}) collective-permute-start(bf16[48,2048]{1,0:T(8,128)(2,1)} %get-tuple-element.37), channel_id=1, source_target_pairs={{0,8},{4,12},{8,0},{12,4},{16,24},{20,28},{24,16},{28,20},{1,9},{5... | collective-permute-start | bytes 589832 | tf_op jit(solution)/shard_map/ppermute | solution.py:22
  47.2 12.7 %collective-permute-start.8 = (bf16[48,2048]{1,0:T(8,128)(2,1)}, bf16[48,2048]{1,0:T(8,128)(2,1)S(1)}, u32[]{:S(2)}, u32[]{:S(2)}) collective-permute-start(bf16[48,2048]{1,0:T(8,128)(2,1)} %get-tuple-element.38), channel_id=1, source_target_pairs={{0,12},{4,8},{8,4},{12,0},{16,28},{20,24},{24,20},{28,16},{1,13},{... | collective-permute-start | bytes 589832 | tf_op jit(solution)/shard_map/ppermute | solution.py:22
  47.2 12.7 %collective-permute-start.9 = (bf16[48,2048]{1,0:T(8,128)(2,1)}, bf16[48,2048]{1,0:T(8,128)(2,1)S(1)}, u32[]{:S(2)}, u32[]{:S(2)}) collective-permute-start(bf16[48,2048]{1,0:T(8,128)(2,1)} %get-tuple-element.39), channel_id=1, source_target_pairs={{0,16},{4,20},{8,24},{12,28},{16,0},{20,4},{24,8},{28,12},{1,17},{... | collective-permute-start | bytes 589832 | tf_op jit(solution)/shard_map/ppermute | solution.py:22
  66.4 2.7 %collective-permute-start.13 = (bf16[2048,256]{1,0:T(8,128)(2,1)S(1)}, bf16[2048,256]{1,0:T(8,128)(2,1)S(1)}, u32[]{:S(2)}, u32[]{:S(2)}) collective-permute-start(bf16[2048,256]{1,0:T(8,128)(2,1)S(1)} %collective-permute-done.refs_9_), channel_id=1, source_target_pairs={{0,1},{1,0},{2,3},{3,2},{4,5},{5,4},{6,7},{7,6},{8,9},{9,8},{10,11... | collective-permute-start | bytes 3145736 | tf_op jit(solution)/shard_map/ppermute | solution.py:22
  66.5 11.5 %collective-permute-start.15 = (bf16[96,2048]{1,0:T(8,128)(2,1)S(1)}, bf16[96,2048]{1,0:T(8,128)(2,1)S(1)}, u32[]{:S(2)}, u32[]{:S(2)}) collective-permute-start(bf16[96,2048]{1,0:T(8,128)(2,1)S(1)} %fusion.4.refs_0_), channel_id=1, source_target_pairs={{0,2},{1,3},{2,0},{3,1},{4,6},{5,7},{6,4},{7,5},{8,10},{9,11},{10,... | collective-permute-start | bytes 1179656 | tf_op jit(solution)/shard_map/ppermute | solution.py:22
  66.9 11.1 %collective-permute-start.14 = (bf16[96,2048]{1,0:T(8,128)(2,1)S(1)}, bf16[96,2048]{1,0:T(8,128)(2,1)S(1)}, u32[]{:S(2)}, u32[]{:S(2)}) collective-permute-start(bf16[96,2048]{1,0:T(8,128)(2,1)S(1)} %fusion.4.refs_0_), channel_id=1, source_target_pairs={{0,1},{1,0},{2,3},{3,2},{4,5},{5,4},{6,7},{7,6},{8,9},{9,8},{10,11... | collective-permute-start | bytes 1179656 | tf_op jit(solution)/shard_map/ppermute | solution.py:22
  89.7 6.5 %collective-permute-start.17 = (bf16[2,512]{1,0:T(2,128)(2,1)S(1)}, bf16[2,512]{1,0:T(2,128)(2,1)S(1)}, u32[]{:S(2)}, u32[]{:S(2)}) collective-permute-start(bf16[2,512]{1,0:T(2,128)(2,1)S(1)} %slice.61), channel_id=1, source_target_pairs={{0,4},{4,8},{8,12},{12,16},{16,20},{20,24},{24,28},{1,5},{5,9},{9,... | collective-permute-start | bytes 6152 | tf_op jit(solution)/shard_map/ppermute | solution.py:480
  94.2 12.3 %collective-permute-start.21 = (bf16[384,512]{1,0:T(8,128)(2,1)}, bf16[384,512]{1,0:T(8,128)(2,1)}, u32[]{:S(2)}, u32[]{:S(2)}) collective-permute-start(bf16[384,512]{1,0:T(8,128)(2,1)} %first_hidden.1.first_ref.refs_0_), channel_id=1, source_target_pairs={{0,2},{1,3},{2,0},{3,1},{4,6},{5,7},{6,4},{7,5},{8,10},{9,11},{10,... | collective-permute-start | bytes 1179656 | tf_op jit(solution)/shard_map/ppermute | solution.py:22
  94.8 20.2 %collective-permute-start.22 = (bf16[384,512]{1,0:T(8,128)(2,1)}, bf16[384,512]{1,0:T(8,128)(2,1)}, u32[]{:S(2)}, u32[]{:S(2)}) collective-permute-start(bf16[384,512]{1,0:T(8,128)(2,1)} %get-tuple-element.45.refs_1_), channel_id=1, source_target_pairs={{0,2},{1,3},{2,0},{3,1},{4,6},{5,7},{6,4},{7,5},{8,10},{9,11},{10,... | collective-permute-start | bytes 1179656 | tf_op jit(solution)/shard_map/ppermute | solution.py:22
  96.7 25.8 %collective-permute-start.18 = (bf16[384,512]{1,0:T(8,128)(2,1)S(1)}, bf16[384,512]{1,0:T(8,128)(2,1)S(1)}, u32[]{:S(2)}, u32[]{:S(2)}) collective-permute-start(bf16[384,512]{1,0:T(8,128)(2,1)S(1)} %fusion.7), channel_id=1, source_target_pairs={{0,1},{1,0},{2,3},{3,2},{4,5},{5,4},{6,7},{7,6},{8,9},{9,8},{10,11... | collective-permute-start | bytes 1179656 | tf_op jit(solution)/shard_map/ppermute | solution.py:22
  96.8 28.7 %collective-permute-start.19 = (bf16[384,512]{1,0:T(8,128)(2,1)S(1)}, bf16[384,512]{1,0:T(8,128)(2,1)S(1)}, u32[]{:S(2)}, u32[]{:S(2)}) collective-permute-start(bf16[384,512]{1,0:T(8,128)(2,1)S(1)} %fusion.7), channel_id=1, source_target_pairs={{0,2},{1,3},{2,0},{3,1},{4,6},{5,7},{6,4},{7,5},{8,10},{9,11},{10,... | collective-permute-start | bytes 1179656 | tf_op jit(solution)/shard_map/ppermute | solution.py:22
  97.4 78.3 %collective-permute-start.26 = (bf16[48,1024]{1,0:T(8,128)(2,1)}, bf16[48,1024]{1,0:T(8,128)(2,1)S(1)}, u32[]{:S(2)}, u32[]{:S(2)}) collective-permute-start(bf16[48,1024]{1,0:T(8,128)(2,1)} %get-tuple-element.58), channel_id=1, source_target_pairs={{0,16},{4,20},{8,24},{12,28},{16,0},{20,4},{24,8},{28,12},{1,17},{... | collective-permute-start | bytes 294920 | tf_op jit(solution)/shard_map/ppermute | solution.py:22
  106.6 69.2 %collective-permute-start.27 = (bf16[48,1024]{1,0:T(8,128)(2,1)S(1)}, bf16[48,1024]{1,0:T(8,128)(2,1)S(1)}, u32[]{:S(2)}, u32[]{:S(2)}) collective-permute-start(bf16[48,1024]{1,0:T(8,128)(2,1)S(1)} %copy-done.28), channel_id=1, source_target_pairs={{0,20},{4,16},{8,28},{12,24},{16,4},{20,0},{24,12},{28,8},{1,21},{... | collective-permute-start | bytes 294920 | tf_op jit(solution)/shard_map/ppermute | solution.py:22
  115.0 60.8 %collective-permute-start.28 = (bf16[48,1024]{1,0:T(8,128)(2,1)S(1)}, bf16[48,1024]{1,0:T(8,128)(2,1)S(1)}, u32[]{:S(2)}, u32[]{:S(2)}) collective-permute-start(bf16[48,1024]{1,0:T(8,128)(2,1)S(1)} %copy-done.27), channel_id=1, source_target_pairs={{0,24},{4,28},{8,16},{12,20},{16,8},{20,12},{24,0},{28,4},{1,25},{... | collective-permute-start | bytes 294920 | tf_op jit(solution)/shard_map/ppermute | solution.py:22
  122.5 53.2 %collective-permute-start.29 = (bf16[48,1024]{1,0:T(8,128)(2,1)S(1)}, bf16[48,1024]{1,0:T(8,128)(2,1)S(1)}, u32[]{:S(2)}, u32[]{:S(2)}) collective-permute-start(bf16[48,1024]{1,0:T(8,128)(2,1)S(1)} %copy-done.26), channel_id=1, source_target_pairs={{0,28},{4,24},{8,20},{12,16},{16,12},{20,8},{24,4},{28,0},{1,29},{... | collective-permute-start | bytes 294920 | tf_op jit(solution)/shard_map/ppermute | solution.py:22
  127.2 6.9 %collective-permute-start.23 = (bf16[96,1024]{1,0:T(8,128)(2,1)S(1)}, bf16[96,1024]{1,0:T(8,128)(2,1)S(1)}, u32[]{:S(2)}, u32[]{:S(2)}) collective-permute-start(bf16[96,1024]{1,0:T(8,128)(2,1)S(1)} %copy-done.25), channel_id=1, source_target_pairs={{0,4},{4,0},{8,12},{12,8},{16,20},{20,16},{24,28},{28,24},{1,5},{5... | collective-permute-start | bytes 589832 | tf_op jit(solution)/shard_map/ppermute | solution.py:22
  134.2 6.1 %collective-permute-start.24 = (bf16[96,1024]{1,0:T(8,128)(2,1)S(1)}, bf16[96,1024]{1,0:T(8,128)(2,1)S(1)}, u32[]{:S(2)}, u32[]{:S(2)}) collective-permute-start(bf16[96,1024]{1,0:T(8,128)(2,1)S(1)} %copy-done.24), channel_id=1, source_target_pairs={{0,8},{4,12},{8,0},{12,4},{16,24},{20,28},{24,16},{28,20},{1,9},{5... | collective-permute-start | bytes 589832 | tf_op jit(solution)/shard_map/ppermute | solution.py:22
  140.3 6.6 %collective-permute-start.25 = (bf16[96,1024]{1,0:T(8,128)(2,1)S(1)}, bf16[96,1024]{1,0:T(8,128)(2,1)S(1)}, u32[]{:S(2)}, u32[]{:S(2)}) collective-permute-start(bf16[96,1024]{1,0:T(8,128)(2,1)S(1)} %copy-done.23), channel_id=1, source_target_pairs={{0,12},{4,8},{8,4},{12,0},{16,28},{20,24},{24,20},{28,16},{1,13},{... | collective-permute-start | bytes 589832 | tf_op jit(solution)/shard_map/ppermute | solution.py:22
  146.9 6.3 %collective-permute-start.30 = (bf16[48,1024]{1,0:T(8,128)(2,1)S(1)}, bf16[48,1024]{1,0:T(8,128)(2,1)S(1)}, u32[]{:S(2)}, u32[]{:S(2)}) collective-permute-start(bf16[48,1024]{1,0:T(8,128)(2,1)S(1)} %copy-done.32), channel_id=1, source_target_pairs={{0,16},{4,20},{8,24},{12,28},{16,0},{20,4},{24,8},{28,12},{1,17},{... | collective-permute-start | bytes 294920 | tf_op jit(solution)/shard_map/ppermute | solution.py:22
  153.1 6.6 %collective-permute-start.31 = (bf16[48,1024]{1,0:T(8,128)(2,1)S(1)}, bf16[48,1024]{1,0:T(8,128)(2,1)S(1)}, u32[]{:S(2)}, u32[]{:S(2)}) collective-permute-start(bf16[48,1024]{1,0:T(8,128)(2,1)S(1)} %copy-done.31), channel_id=1, source_target_pairs={{0,20},{4,16},{8,28},{12,24},{16,4},{20,0},{24,12},{28,8},{1,21},{... | collective-permute-start | bytes 294920 | tf_op jit(solution)/shard_map/ppermute | solution.py:22
  159.7 6.6 %collective-permute-start.32 = (bf16[48,1024]{1,0:T(8,128)(2,1)S(1)}, bf16[48,1024]{1,0:T(8,128)(2,1)S(1)}, u32[]{:S(2)}, u32[]{:S(2)}) collective-permute-start(bf16[48,1024]{1,0:T(8,128)(2,1)S(1)} %copy-done.30), channel_id=1, source_target_pairs={{0,24},{4,28},{8,16},{12,20},{16,8},{20,12},{24,0},{28,4},{1,25},{... | collective-permute-start | bytes 294920 | tf_op jit(solution)/shard_map/ppermute | solution.py:22
  166.3 8.7 %collective-permute-start.33 = (bf16[48,1024]{1,0:T(8,128)(2,1)S(1)}, bf16[48,1024]{1,0:T(8,128)(2,1)S(1)}, u32[]{:S(2)}, u32[]{:S(2)}) collective-permute-start(bf16[48,1024]{1,0:T(8,128)(2,1)S(1)} %copy-done.29), channel_id=1, source_target_pairs={{0,28},{4,24},{8,20},{12,16},{16,12},{20,8},{24,4},{28,0},{1,29},{... | collective-permute-start | bytes 294920 | tf_op jit(solution)/shard_map/ppermute | solution.py:22
  (36 other events, 557.3 us)

commit v2 on v1

--- a/solution.py
+++ b/solution.py
@@ -42,14 +42,17 @@
     return count <= 16 and count & (count - 1) == 0
 
 
-def far_first(count):
-    return sorted(range(1, count), key=lambda k: (-k.bit_length(), k))
+def start_order(count):
+    across = [k for k in range(1, count) if k & (count // 2)]
+    nearer = [k for k in range(2, count // 2)]
+    half = len(across) // 2
+    return across[:half] + nearer + across[half:] + [1] * (count > 2)
 
 
 def exchange(chunks, axis, direct):
     if direct:
         moved = dict(chunks)
-        for k in far_first(lax.axis_size(axis)):
+        for k in start_order(lax.axis_size(axis)):
             if k in chunks:
                 moved[k] = swapped(chunks[k], axis, k)
         return moved
@@ -127,7 +130,7 @@
     )(place, ids, rows, gain)
 
 
-def stream_hidden(row_refs, weight_refs, rows, weights, row_sems, weight_sems):
+def stream_hidden(row_refs, weight_refs, rows, weights, row_sems, weight_sems, later=()):
     chunks = row_sems.shape[0]
     depth = rows.shape[1] // chunks
     plan = []
@@ -151,6 +154,9 @@
     for chunk in range(chunks):
         for copy in plan[chunk]:
             copy.wait()
+        if chunk == 0:
+            for copy in later:
+                copy.start()
         part = slice(chunk * depth, (chunk + 1) * depth)
         here = rows[:, part]
         gate_term = jnp.dot(here, weights[0, part, :], preferred_element_type=jnp.float32)
@@ -224,10 +230,7 @@
         pltpu.make_async_copy(ref, target, down_sems.at[index])
         for index, (ref, target) in enumerate(zip(sources, targets))
     ]
-    hidden = stream_hidden(row_refs, weight_refs, *scratch)
-    for load in loads:
-        load.start()
-    hidden_ref[...] = hidden
+    hidden_ref[...] = stream_hidden(row_refs, weight_refs, *scratch, later=loads)
     loads[0].wait()
     first = first_rows[early_rows:]
     second = hidden_ref[early_rows:]
@@ -310,7 +313,7 @@
             pltpu.VMEM(downs[1].shape, jnp.bfloat16),
             pltpu.SemaphoreType.DMA((2,)),
         ],
-        compiler_params=pltpu.CompilerParams(vmem_limit_bytes=56 * MIB),
+        compiler_params=pltpu.CompilerParams(vmem_limit_bytes=24 * MIB),
         cost_estimate=pl.CostEstimate(
             flops=2 * sum(rows) * downs[0].shape[0] * out_width,
             bytes_accessed=4 * MIB,
@@ -362,7 +365,7 @@
             pltpu.SemaphoreType.DMA((4,)),
             pltpu.SemaphoreType.DMA((3,)),
         ],
-        compiler_params=pltpu.CompilerParams(vmem_limit_bytes=40 * MIB),
+        compiler_params=pltpu.CompilerParams(vmem_limit_bytes=56 * MIB),
         cost_estimate=pl.CostEstimate(
             flops=6 * rows * depth * width, bytes_accessed=8 * MIB, transcendentals=0
         ),
@@ -494,7 +497,7 @@
             gated[j], rows_of(mixer_proj, j, chan_width), preferred_element_type=jnp.float32
         )
         mixer_sum = term if mixer_sum is None else mixer_sum + term
-    first_far = after(first_far, gated[0])
+    first_far = after(first_far, product)
     late = late_results(place, far, (first, second, first_far, second_far), downs, sizes, early)
     back_late = exchange(dict(enumerate(late)), "ep", direct)
     back_late[0] = after(back_late[0], mixer_sum)

time: 179 us -> 181 us (1.011)
  starting transfers between devices: 55.8 us -> 44.2 us
  waiting for transfers between devices: 75.5 us -> 86 us
  other arithmetic: 6.42 us -> 10.1 us
  matrix products: 3.66 us -> 6.65 us
  local copies, waits for them, and re-layouts: 10 us -> 7.15 us
    ppermute x34, starting transfers between devices: 52.2 us -> 40.6 us  [swapped(): lax.ppermute(value, axis, [(source, source ^ mask) for source in range(co...]
    ppermute x34, waiting for transfers between devices: 75.5 us -> 86 us  [swapped(): lax.ppermute(value, axis, [(source, source ^ mask) for source in range(co...]
    unnamed x76 -> x60, local copies, waits for them, and re-layouts: 8.03 us -> 4.45 us
    dot_general x4, matrix products: 2.24 us -> 5.22 us  [on_device(): jnp.dot(gated[j], rows_of(mixer_proj, j, chan_width), preferred_element_t...]
    pallas_call x1, Pallas kernels: 5.1 us -> 7.15 us  [mixer_front(): pl.pallas_call(front_kernel, out_shape=[jax.ShapeDtypeStruct((rows, width...]
    pallas_call x1, Pallas kernels: 5.04 us -> 2.99 us  [late_results(): pl.pallas_call(functools.partial(late_kernel, far, tuple(sizes), tuple(ea...]
    convert_element_type x1, other arithmetic: 0.28 us -> 2.24 us  [on_device(): gated = {0: (out_gate * conv_sum).astype(jnp.bfloat16)}]
  transfers between devices with their start and end apart: 35 -> 35, of which waited for: 19 -> 18; matrix products, arithmetic and copies ran while one was open for 6% -> 10% of each run, Pallas kernels for 12% -> 10%
where the time goes in v2:
time: 181 us
  waiting for transfers between devices  86 us (48%)
  starting transfers between devices  44.2 us (24%)
  Pallas kernels  25.4 us (14%)
  other arithmetic  10.1 us (6%)
  local copies, waits for them, and re-layouts  7.15 us (4%)
  matrix products  6.65 us (4%)
    ppermute x34, waiting for transfers between devices, swapped(): lax.ppermute(value, axis, [(source, source ^ mask) for source in range(co...  86 us
    ppermute x34, starting transfers between devices, swapped(): lax.ppermute(value, axis, [(source, source ^ mask) for source in range(co...  40.6 us
    pallas_call x1, Pallas kernels, mixer_front(): pl.pallas_call(front_kernel, out_shape=[jax.ShapeDtypeStruct((rows, width...  7.15 us
    pallas_call x1, Pallas kernels, second_hidden(): pl.pallas_call(functools.partial(second_kernel, len(row_parts), len(weigh...  6.59 us
    dot_general x4, matrix products, on_device(): jnp.dot(gated[j], rows_of(mixer_proj, j, chan_width), preferred_element_t...  5.22 us
    pallas_call x1, Pallas kernels, first_hidden(): pl.pallas_call(functools.partial(first_kernel, len(row_parts)), out_shape...  5.15 us
    unnamed x60, local copies, waits for them, and re-layouts  4.45 us
  transfers between devices with their start and end apart: 35, of which 18 were waited for; matrix products, arithmetic and copies ran while one was open for 10% of the time, Pallas kernels for 10%

profile of v2, /device:TPU:0, one launch (start us, length us, event | category | flops | bytes accessed | tf_op | source)
XLA Modules:
  0.0 180.6 jit_solution(11061350968374323471)
XLA Ops:
  0.6 3.0 %collective-permute-start.1 = (bf16[2048,256]{1,0:T(8,128)(2,1)}, bf16[2048,256]{1,0:T(8,128)(2,1)}, u32[]{:S(2)}, u32[]{:S(2)}) collective-permute-start(bf16[2048,256]{1,0:T(8,128)(2,1)} %bitcast.69), channel_id=1, source_target_pairs={{0,2},{1,3},{2,0},{3,1},{4,6},{5,7},{6,4},{7,5},{8,10},{9,11},{10,... | collective-permute-start | bytes 3145736 | tf_op jit(solution)/shard_map/ppermute | solution.py:22
  4.7 3.5 %dispatch.1 = (bf16[48,2048]{1,0:T(8,128)(2,1)}, bf16[48,2048]{1,0:T(8,128)(2,1)}, bf16[48,2048]{1,0:T(8,128)(2,1)}, bf16[48,2048]{1,0:T(8,128)(2,1)}, bf16[48,2...) custom-call(s32[2]{0:T(128)} %compare_select_fusion.2.place_ref, ...), custom_call_target="tpu_custom_call" | custom-call | flops 150994944 | bytes 2097152 | tf_op jit(solution)/shard_map/dispatch/pallas_call | solution.py:119
  8.2 3.6 %collective-permute-start.10 = (bf16[48,2048]{1,0:T(8,128)(2,1)}, bf16[48,2048]{1,0:T(8,128)(2,1)S(1)}, u32[]{:S(2)}, u32[]{:S(2)}) collective-permute-start(bf16[48,2048]{1,0:T(8,128)(2,1)} %get-tuple-element.40), channel_id=1, source_target_pairs={{0,20},{4,16},{8,28},{12,24},{16,4},{20,0},{24,12},{28,8},{1,21},{... | collective-permute-start | bytes 589832 | tf_op jit(solution)/shard_map/ppermute | solution.py:22
  15.7 10.8 %collective-permute-done.10.refs_5_ = bf16[48,2048]{1,0:T(8,128)(2,1)S(1)} collective-permute-done((bf16[48,2048]{1,0:T(8,128)(2,1)}, bf16[48,2048]{1,0:T(8,128)(2,1)S(1)}, u32[]{:S(2)}, u32[]{:S(2)}) %collective-permute-start.10) | collective-permute-done | bytes 196640 | tf_op jit(solution)/shard_map/ppermute | solution.py:22
  28.4 4.9 %collective-permute-start.12 = (bf16[48,2048]{1,0:T(8,128)(2,1)}, bf16[48,2048]{1,0:T(8,128)(2,1)S(1)}, u32[]{:S(2)}, u32[]{:S(2)}) collective-permute-start(bf16[48,2048]{1,0:T(8,128)(2,1)} %get-tuple-element.42), channel_id=1, source_target_pairs={{0,28},{4,24},{8,20},{12,16},{16,12},{20,8},{24,4},{28,0},{1,29},{... | collective-permute-start | bytes 589832 | tf_op jit(solution)/shard_map/ppermute | solution.py:22
  33.4 5.8 %collective-permute-done.12.refs_7_ = bf16[48,2048]{1,0:T(8,128)(2,1)S(1)} collective-permute-done((bf16[48,2048]{1,0:T(8,128)(2,1)}, bf16[48,2048]{1,0:T(8,128)(2,1)S(1)}, u32[]{:S(2)}, u32[]{:S(2)}) %collective-permute-start.12) | collective-permute-done | bytes 196640 | tf_op jit(solution)/shard_map/ppermute | solution.py:22
  40.6 1.9 %fusion.4.refs_0_ = bf16[96,2048]{1,0:T(8,128)(2,1)} fusion(bf16[96,2048]{1,0:T(8,128)(2,1)} %param.14, f32[2048]{0:T(1024)} %param.16, f32[96]{0:T(128)S(1)} %add_rsqrt_fusion), kind=kLoop, calls=%fused_computation.13 | loop fusion | flops 786432 | bytes 795008 | tf_op jit(solution)/shard_map/convert_element_type | solution.py:17
  43.9 3.9 %collective-permute-start.7 = (bf16[48,2048]{1,0:T(8,128)(2,1)}, bf16[48,2048]{1,0:T(8,128)(2,1)S(1)}, u32[]{:S(2)}, u32[]{:S(2)}) collective-permute-start(bf16[48,2048]{1,0:T(8,128)(2,1)} %get-tuple-element.37), channel_id=1, source_target_pairs={{0,8},{4,12},{8,0},{12,4},{16,24},{20,28},{24,16},{28,20},{1,9},{5... | collective-permute-start | bytes 589832 | tf_op jit(solution)/shard_map/ppermute | solution.py:22
  47.8 3.0 %collective-permute-start.9 = (bf16[48,2048]{1,0:T(8,128)(2,1)}, bf16[48,2048]{1,0:T(8,128)(2,1)S(1)}, u32[]{:S(2)}, u32[]{:S(2)}) collective-permute-start(bf16[48,2048]{1,0:T(8,128)(2,1)} %get-tuple-element.39), channel_id=1, source_target_pairs={{0,16},{4,20},{8,24},{12,28},{16,0},{20,4},{24,8},{28,12},{1,17},{... | collective-permute-start | bytes 589832 | tf_op jit(solution)/shard_map/ppermute | solution.py:22
  52.6 5.4 %collective-permute-done.7.refs_2_ = bf16[48,2048]{1,0:T(8,128)(2,1)S(1)} collective-permute-done((bf16[48,2048]{1,0:T(8,128)(2,1)}, bf16[48,2048]{1,0:T(8,128)(2,1)S(1)}, u32[]{:S(2)}, u32[]{:S(2)}) %collective-permute-start.7) | collective-permute-done | bytes 196640 | tf_op jit(solution)/shard_map/ppermute | solution.py:22
  58.0 2.6 %collective-permute-done.8.refs_3_ = bf16[48,2048]{1,0:T(8,128)(2,1)S(1)} collective-permute-done((bf16[48,2048]{1,0:T(8,128)(2,1)}, bf16[48,2048]{1,0:T(8,128)(2,1)S(1)}, u32[]{:S(2)}, u32[]{:S(2)}) %collective-permute-start.8) | collective-permute-done | bytes 196640 | tf_op jit(solution)/shard_map/ppermute | solution.py:22
  61.9 5.1 %first_hidden.1.first_ref.refs_0_ = bf16[384,512]{1,0:T(8,128)(2,1)} custom-call(bf16[48,2048]{1,0:T(8,128)(2,1)} %get-tuple-element.35.refs_0_, bf16[48,2048]{1,0:T(8,128)(2,1)} %copy-done.13, bf16[48,2048]{1,0:T(8,128)(2,1)} %copy-done.14, bf16[48,2048]{1,0:T(8,128)(2,1)} %copy-done.15, bf16[48,2048]{1,0:T(8,128)(2,1)} %copy-done.16, ...), custom_call_target="tpu_custom_call" | custom-call | flops 1610612736 | bytes 5767168 | tf_op jit(solution)/shard_map/first_hidden/pallas_call | solution.py:199
  67.8 2.0 %collective-permute-done.13.refs_11_ = bf16[2048,256]{1,0:T(8,128)(2,1)S(1)} collective-permute-done((bf16[2048,256]{1,0:T(8,128)(2,1)S(1)}, bf16[2048,256]{1,0:T(8,128)(2,1)S(1)}, u32[]{:S(2)}, u32[]{:S(2)}) %collective-permute-start.13) | collective-permute-done | bytes 1048608 | tf_op jit(solution)/shard_map/ppermute | solution.py:22
  70.8 6.6 %second_hidden.1 = (bf16[384,512]{1,0:T(8,128)(2,1)}, bf16[48,1024]{1,0:T(8,128)(2,1)}, bf16[48,1024]{1,0:T(8,128)(2,1)}, bf16[48,1024]{1,0:T(8,128)(2,1)}, bf16[48,1024]{1,0:T(8,128)(2,1)}) custom-call(s32[2]{0:T(128)} %compare_select_fusion.2.place_ref, bf16[384,512]{1,0:T(8,128)(2,1)} %first_hidden.1.first_ref.refs_0_, ...), custom_call_target="tpu_custom_call" | custom-call | flops 1048576 | bytes 1048576 | tf_op jit(solution)/shard_map/second_hidden/pallas_call | solution.py:254
  78.9 1.8 %collective-permute-done.16.refs_3_ = bf16[96,2048]{1,0:T(8,128)(2,1)} collective-permute-done((bf16[96,2048]{1,0:T(8,128)(2,1)S(1)}, bf16[96,2048]{1,0:T(8,128)(2,1)}, u32[]{:S(2)}, u32[]{:S(2)}) %collective-permute-start.16) | collective-permute-done | bytes 393248 | tf_op jit(solution)/shard_map/ppermute | solution.py:22
  80.8 7.2 %mixer_front.1 = (bf16[384,512]{1,0:T(8,128)(2,1)}, f32[384,512]{1,0:T(8,128)}) custom-call(s32[2]{0:T(128)} %compare_select_fusion.2.place_ref, bf16[96,2048]{1,0:T(8,128)(2,1)} %fusion.4.refs_0_, bf16[96,2048]{1,0:T(8,128)(2,1)} %copy-done.23, bf16[96,2048]{1,0:T(8,128)(2,1)} %copy-done.22, bf16[96,2048]{1,0:T(8,128)(2,1)} %collective-permute-done.16.refs_3_, ...), custom_call_target="tpu_custom_call" | custom-call | flops 2415919104 | bytes 8388608 | tf_op jit(solution)/shard_map/mixer_front/pallas_call | solution.py:354
  88.6 3.6 %collective-permute-start.17 = (bf16[2,512]{1,0:T(2,128)(2,1)S(1)}, bf16[2,512]{1,0:T(2,128)(2,1)S(1)}, u32[]{:S(2)}, u32[]{:S(2)}) collective-permute-start(bf16[2,512]{1,0:T(2,128)(2,1)S(1)} %slice.61), channel_id=1, source_target_pairs={{0,4},{4,8},{8,12},{12,16},{16,20},{20,24},{24,28},{1,5},{5,9},{9,... | collective-permute-start | bytes 6152 | tf_op jit(solution)/shard_map/ppermute | solution.py:483
  96.3 2.2 %fusion.7 = bf16[384,512]{1,0:T(8,128)(2,1)} fusion(f32[384,512]{1,0:T(8,128)} %get-tuple-element.49, f32[386,512]{1,0:T(8,128)S(1)} %maximum_convert_fusion, f32[512]{0:T(512)S(1)} %bitcast.77, f32[512]{0:T(512)S(1)} %bitcast.76, f32[512]{0:T(512)S(1)} %bitcast.75), kind=kLoop, calls=%fused_computation.17 | loop fusion | flops 1376256 | bytes 3545088 | tf_op jit(solution)/shard_map/convert_element_type | solution.py:490
  99.1 2.6 %collective-permute-start.26 = (bf16[48,1024]{1,0:T(8,128)(2,1)}, bf16[48,1024]{1,0:T(8,128)(2,1)S(1)}, u32[]{:S(2)}, u32[]{:S(2)}) collective-permute-start(bf16[48,1024]{1,0:T(8,128)(2,1)} %get-tuple-element.58), channel_id=1, source_target_pairs={{0,16},{4,20},{8,24},{12,28},{16,0},{20,4},{24,8},{28,12},{1,17},{... | collective-permute-start | bytes 294920 | tf_op jit(solution)/shard_map/ppermute | solution.py:22
  101.7 3.5 %collective-permute-done.21.refs_2_ = bf16[384,512]{1,0:T(8,128)(2,1)} collective-permute-done((bf16[384,512]{1,0:T(8,128)(2,1)S(1)}, bf16[384,512]{1,0:T(8,128)(2,1)}, u32[]{:S(2)}, u32[]{:S(2)}) %collective-permute-start.21) | collective-permute-done | bytes 393248 | tf_op jit(solution)/shard_map/ppermute | solution.py:22
  105.3 2.3 %collective-permute-start.27 = (bf16[48,1024]{1,0:T(8,128)(2,1)}, bf16[48,1024]{1,0:T(8,128)(2,1)S(1)}, u32[]{:S(2)}, u32[]{:S(2)}) collective-permute-start(bf16[48,1024]{1,0:T(8,128)(2,1)} %get-tuple-element.59), channel_id=1, source_target_pairs={{0,20},{4,16},{8,28},{12,24},{16,4},{20,0},{24,12},{28,8},{1,21},{... | collective-permute-start | bytes 294920 | tf_op jit(solution)/shard_map/ppermute | solution.py:22
  107.6 6.1 %collective-permute-done.22.refs_3_ = bf16[384,512]{1,0:T(8,128)(2,1)} collective-permute-done((bf16[384,512]{1,0:T(8,128)(2,1)}, bf16[384,512]{1,0:T(8,128)(2,1)}, u32[]{:S(2)}, u32[]{:S(2)}) %collective-permute-start.22) | collective-permute-done | bytes 393248 | tf_op jit(solution)/shard_map/ppermute | solution.py:22
  113.7 2.5 %collective-permute-start.28 = (bf16[48,1024]{1,0:T(8,128)(2,1)}, bf16[48,1024]{1,0:T(8,128)(2,1)S(1)}, u32[]{:S(2)}, u32[]{:S(2)}) collective-permute-start(bf16[48,1024]{1,0:T(8,128)(2,1)} %get-tuple-element.60), channel_id=1, source_target_pairs={{0,24},{4,28},{8,16},{12,20},{16,8},{20,12},{24,0},{28,4},{1,25},{... | collective-permute-start | bytes 294920 | tf_op jit(solution)/shard_map/ppermute | solution.py:22
  117.4 3.0 %late_down.1 = (bf16[96,1024]{1,0:T(8,128)(2,1)S(1)}, bf16[96,1024]{1,0:T(8,128)(2,1)S(1)}, bf16[96,1024]{1,0:T(8,128)(2,1)S(1)}, bf16[96,1024]{1,0:T(8,128)(2,1...) custom-call(s32[2]{0:T(128)S(1)} %copy-done.5, ...), custom_call_target="tpu_custom_call" | custom-call | flops 1207959552 | bytes 4194304 | tf_op jit(solution)/shard_map/late_down/pallas_call | solution.py:306
  120.4 3.0 %collective-permute-start.29 = (bf16[48,1024]{1,0:T(8,128)(2,1)S(1)}, bf16[48,1024]{1,0:T(8,128)(2,1)S(1)}, u32[]{:S(2)}, u32[]{:S(2)}) collective-permute-start(bf16[48,1024]{1,0:T(8,128)(2,1)S(1)} %copy-done.24), channel_id=1, source_target_pairs={{0,28},{4,24},{8,20},{12,16},{16,12},{20,8},{24,4},{28,0},{1,29},{... | collective-permute-start | bytes 294920 | tf_op jit(solution)/shard_map/ppermute | solution.py:22
  128.8 6.1 %collective-permute-done.23 = bf16[96,1024]{1,0:T(8,128)(2,1)S(1)} collective-permute-done((bf16[96,1024]{1,0:T(8,128)(2,1)S(1)}, bf16[96,1024]{1,0:T(8,128)(2,1)S(1)}, u32[]{:S(2)}, u32[]{:S(2)}) %collective-permute-start.23) | collective-permute-done | bytes 196640 | tf_op jit(solution)/shard_map/ppermute | solution.py:22
  134.9 6.4 %collective-permute-done.24 = bf16[96,1024]{1,0:T(8,128)(2,1)S(1)} collective-permute-done((bf16[96,1024]{1,0:T(8,128)(2,1)S(1)}, bf16[96,1024]{1,0:T(8,128)(2,1)S(1)}, u32[]{:S(2)}, u32[]{:S(2)}) %collective-permute-start.24) | collective-permute-done | bytes 196640 | tf_op jit(solution)/shard_map/ppermute | solution.py:22
  141.7 6.3 %collective-permute-done.25 = bf16[96,1024]{1,0:T(8,128)(2,1)S(1)} collective-permute-done((bf16[96,1024]{1,0:T(8,128)(2,1)S(1)}, bf16[96,1024]{1,0:T(8,128)(2,1)S(1)}, u32[]{:S(2)}, u32[]{:S(2)}) %collective-permute-start.25) | collective-permute-done | bytes 196640 | tf_op jit(solution)/shard_map/ppermute | solution.py:22
  148.1 6.3 %collective-permute-done.30 = bf16[48,1024]{1,0:T(8,128)(2,1)S(1)} collective-permute-done((bf16[48,1024]{1,0:T(8,128)(2,1)S(1)}, bf16[48,1024]{1,0:T(8,128)(2,1)S(1)}, u32[]{:S(2)}, u32[]{:S(2)}) %collective-permute-start.30) | collective-permute-done | bytes 98336 | tf_op jit(solution)/shard_map/ppermute | solution.py:22
  154.5 8.6 %collective-permute-done.31 = bf16[48,1024]{1,0:T(8,128)(2,1)S(1)} collective-permute-done((bf16[48,1024]{1,0:T(8,128)(2,1)S(1)}, bf16[48,1024]{1,0:T(8,128)(2,1)S(1)}, u32[]{:S(2)}, u32[]{:S(2)}) %collective-permute-start.31) | collective-permute-done | bytes 98336 | tf_op jit(solution)/shard_map/ppermute | solution.py:22
  164.5 5.2 %collective-permute-done.32 = bf16[48,1024]{1,0:T(8,128)(2,1)S(1)} collective-permute-done((bf16[48,1024]{1,0:T(8,128)(2,1)S(1)}, bf16[48,1024]{1,0:T(8,128)(2,1)S(1)}, u32[]{:S(2)}, u32[]{:S(2)}) %collective-permute-start.32) | collective-permute-done | bytes 98336 | tf_op jit(solution)/shard_map/ppermute | solution.py:22
  171.4 5.5 %collective-permute-done.33 = bf16[48,1024]{1,0:T(8,128)(2,1)S(1)} collective-permute-done((bf16[48,1024]{1,0:T(8,128)(2,1)S(1)}, bf16[48,1024]{1,0:T(8,128)(2,1)S(1)}, u32[]{:S(2)}, u32[]{:S(2)}) %collective-permute-start.33) | collective-permute-done | bytes 98336 | tf_op jit(solution)/shard_map/ppermute | solution.py:22
  (141 shorter events, 35.2 us)
Async XLA Ops:
  0.6 26.5 %collective-permute-start.1 = (bf16[2048,256]{1,0:T(8,128)(2,1)}, bf16[2048,256]{1,0:T(8,128)(2,1)}, u32[]{:S(2)}, u32[]{:S(2)}) collective-permute-start(bf16[2048,256]{1,0:T(8,128)(2,1)} %bitcast.69), channel_id=1, source_target_pairs={{0,2},{1,3},{2,0},{3,1},{4,6},{5,7},{6,4},{7,5},{8,10},{9,11},{10,... | collective-permute-start | bytes 3145736 | tf_op jit(solution)/shard_map/ppermute | solution.py:22
  3.7 40.2 %collective-permute-start.3 = (bf16[2048,256]{1,0:T(8,128)(2,1)}, bf16[2048,256]{1,0:T(8,128)(2,1)}, u32[]{:S(2)}, u32[]{:S(2)}) collective-permute-start(bf16[2048,256]{1,0:T(8,128)(2,1)} %bitcast.70), channel_id=1, source_target_pairs={{0,1},{1,0},{2,3},{3,2},{4,5},{5,4},{6,7},{7,6},{8,9},{9,8},{10,11... | collective-permute-start | bytes 3145736 | tf_op jit(solution)/shard_map/ppermute | solution.py:22
  3.7 38.8 %collective-permute-start.5 = (bf16[1024,512]{1,0:T(8,128)(2,1)}, bf16[1024,512]{1,0:T(8,128)(2,1)S(1)}, u32[]{:S(2)}, u32[]{:S(2)}) collective-permute-start(bf16[1024,512]{1,0:T(8,128)(2,1)} %bitcast.66), channel_id=1, source_target_pairs={{0,1},{1,0},{2,3},{3,2},{4,5},{5,4},{6,7},{7,6},{8,9},{9,8},{10,11... | collective-permute-start | bytes 3145736 | tf_op jit(solution)/shard_map/ppermute | solution.py:22
  8.2 18.3 %collective-permute-start.10 = (bf16[48,2048]{1,0:T(8,128)(2,1)}, bf16[48,2048]{1,0:T(8,128)(2,1)S(1)}, u32[]{:S(2)}, u32[]{:S(2)}) collective-permute-start(bf16[48,2048]{1,0:T(8,128)(2,1)} %get-tuple-element.40), channel_id=1, source_target_pairs={{0,20},{4,16},{8,28},{12,24},{16,4},{20,0},{24,12},{28,8},{1,21},{... | collective-permute-start | bytes 589832 | tf_op jit(solution)/shard_map/ppermute | solution.py:22
  11.8 16.6 %collective-permute-start.11 = (bf16[48,2048]{1,0:T(8,128)(2,1)}, bf16[48,2048]{1,0:T(8,128)(2,1)S(1)}, u32[]{:S(2)}, u32[]{:S(2)}) collective-permute-start(bf16[48,2048]{1,0:T(8,128)(2,1)} %get-tuple-element.41), channel_id=1, source_target_pairs={{0,24},{4,28},{8,16},{12,20},{16,8},{20,12},{24,0},{28,4},{1,25},{... | collective-permute-start | bytes 589832 | tf_op jit(solution)/shard_map/ppermute | solution.py:22
  26.4 21.4 %collective-permute-start.4 = (bf16[2048,256]{1,0:T(8,128)(2,1)}, bf16[2048,256]{1,0:T(8,128)(2,1)S(1)}, u32[]{:S(2)}, u32[]{:S(2)}) collective-permute-start(bf16[2048,256]{1,0:T(8,128)(2,1)} %bitcast.72), channel_id=1, source_target_pairs={{0,1},{1,0},{2,3},{3,2},{4,5},{5,4},{6,7},{7,6},{8,9},{9,8},{10,11... | collective-permute-start | bytes 3145736 | tf_op jit(solution)/shard_map/ppermute | solution.py:22
  27.2 20.7 %collective-permute-start.2 = (bf16[2048,256]{1,0:T(8,128)(2,1)}, bf16[2048,256]{1,0:T(8,128)(2,1)S(1)}, u32[]{:S(2)}, u32[]{:S(2)}) collective-permute-start(bf16[2048,256]{1,0:T(8,128)(2,1)} %collective-permute-done.1.refs_8_), channel_id=1, source_target_pairs={{0,1},{1,0},{2,3},{3,2},{4,5},{5,4},{6,7},{7,6},{8,9},{9,8},{10,11... | collective-permute-start | bytes 3145736 | tf_op jit(solution)/shard_map/ppermute | solution.py:22
  28.4 10.8 %collective-permute-start.12 = (bf16[48,2048]{1,0:T(8,128)(2,1)}, bf16[48,2048]{1,0:T(8,128)(2,1)S(1)}, u32[]{:S(2)}, u32[]{:S(2)}) collective-permute-start(bf16[48,2048]{1,0:T(8,128)(2,1)} %get-tuple-element.42), channel_id=1, source_target_pairs={{0,28},{4,24},{8,20},{12,16},{16,12},{20,8},{24,4},{28,0},{1,29},{... | collective-permute-start | bytes 589832 | tf_op jit(solution)/shard_map/ppermute | solution.py:22
  39.1 28.0 %collective-permute-start = (bf16[2048,256]{1,0:T(8,128)(2,1)}, bf16[2048,256]{1,0:T(8,128)(2,1)S(1)}, u32[]{:S(2)}, u32[]{:S(2)}) collective-permute-start(bf16[2048,256]{1,0:T(8,128)(2,1)} %bitcast.73), channel_id=1, source_target_pairs={{0,2},{1,3},{2,0},{3,1},{4,6},{5,7},{6,4},{7,5},{8,10},{9,11},{10,... | collective-permute-start | bytes 3145736 | tf_op jit(solution)/shard_map/ppermute | solution.py:22
  42.5 10.1 %collective-permute-start.6 = (bf16[48,2048]{1,0:T(8,128)(2,1)}, bf16[48,2048]{1,0:T(8,128)(2,1)S(1)}, u32[]{:S(2)}, u32[]{:S(2)}) collective-permute-start(bf16[48,2048]{1,0:T(8,128)(2,1)} %get-tuple-element.36), channel_id=1, source_target_pairs={{0,4},{4,0},{8,12},{12,8},{16,20},{20,16},{24,28},{28,24},{1,5},{5... | collective-permute-start | bytes 589832 | tf_op jit(solution)/shard_map/ppermute | solution.py:22
  43.9 14.1 %collective-permute-start.7 = (bf16[48,2048]{1,0:T(8,128)(2,1)}, bf16[48,2048]{1,0:T(8,128)(2,1)S(1)}, u32[]{:S(2)}, u32[]{:S(2)}) collective-permute-start(bf16[48,2048]{1,0:T(8,128)(2,1)} %get-tuple-element.37), channel_id=1, source_target_pairs={{0,8},{4,12},{8,0},{12,4},{16,24},{20,28},{24,16},{28,20},{1,9},{5... | collective-permute-start | bytes 589832 | tf_op jit(solution)/shard_map/ppermute | solution.py:22
  47.8 12.7 %collective-permute-start.8 = (bf16[48,2048]{1,0:T(8,128)(2,1)}, bf16[48,2048]{1,0:T(8,128)(2,1)S(1)}, u32[]{:S(2)}, u32[]{:S(2)}) collective-permute-start(bf16[48,2048]{1,0:T(8,128)(2,1)} %get-tuple-element.38), channel_id=1, source_target_pairs={{0,12},{4,8},{8,4},{12,0},{16,28},{20,24},{24,20},{28,16},{1,13},{... | collective-permute-start | bytes 589832 | tf_op jit(solution)/shard_map/ppermute | solution.py:22
  47.8 12.7 %collective-permute-start.9 = (bf16[48,2048]{1,0:T(8,128)(2,1)}, bf16[48,2048]{1,0:T(8,128)(2,1)S(1)}, u32[]{:S(2)}, u32[]{:S(2)}) collective-permute-start(bf16[48,2048]{1,0:T(8,128)(2,1)} %get-tuple-element.39), channel_id=1, source_target_pairs={{0,16},{4,20},{8,24},{12,28},{16,0},{20,4},{24,8},{28,12},{1,17},{... | collective-permute-start | bytes 589832 | tf_op jit(solution)/shard_map/ppermute | solution.py:22
  67.2 11.7 %collective-permute-start.15 = (bf16[96,2048]{1,0:T(8,128)(2,1)}, bf16[96,2048]{1,0:T(8,128)(2,1)S(1)}, u32[]{:S(2)}, u32[]{:S(2)}) collective-permute-start(bf16[96,2048]{1,0:T(8,128)(2,1)} %fusion.4.refs_0_), channel_id=1, source_target_pairs={{0,2},{1,3},{2,0},{3,1},{4,6},{5,7},{6,4},{7,5},{8,10},{9,11},{10,... | collective-permute-start | bytes 1179656 | tf_op jit(solution)/shard_map/ppermute | solution.py:22
  67.6 11.3 %collective-permute-start.14 = (bf16[96,2048]{1,0:T(8,128)(2,1)}, bf16[96,2048]{1,0:T(8,128)(2,1)S(1)}, u32[]{:S(2)}, u32[]{:S(2)}) collective-permute-start(bf16[96,2048]{1,0:T(8,128)(2,1)} %fusion.4.refs_0_), channel_id=1, source_target_pairs={{0,1},{1,0},{2,3},{3,2},{4,5},{5,4},{6,7},{7,6},{8,9},{9,8},{10,11... | collective-permute-start | bytes 1179656 | tf_op jit(solution)/shard_map/ppermute | solution.py:22
  88.6 6.6 %collective-permute-start.17 = (bf16[2,512]{1,0:T(2,128)(2,1)S(1)}, bf16[2,512]{1,0:T(2,128)(2,1)S(1)}, u32[]{:S(2)}, u32[]{:S(2)}) collective-permute-start(bf16[2,512]{1,0:T(2,128)(2,1)S(1)} %slice.61), channel_id=1, source_target_pairs={{0,4},{4,8},{8,12},{12,16},{16,20},{20,24},{24,28},{1,5},{5,9},{9,... | collective-permute-start | bytes 6152 | tf_op jit(solution)/shard_map/ppermute | solution.py:483
  93.1 12.1 %collective-permute-start.21 = (bf16[384,512]{1,0:T(8,128)(2,1)S(1)}, bf16[384,512]{1,0:T(8,128)(2,1)}, u32[]{:S(2)}, u32[]{:S(2)}) collective-permute-start(bf16[384,512]{1,0:T(8,128)(2,1)S(1)} %copy-done.1), channel_id=1, source_target_pairs={{0,2},{1,3},{2,0},{3,1},{4,6},{5,7},{6,4},{7,5},{8,10},{9,11},{10,... | collective-permute-start | bytes 1179656 | tf_op jit(solution)/shard_map/ppermute | solution.py:22
  93.7 20.0 %collective-permute-start.22 = (bf16[384,512]{1,0:T(8,128)(2,1)}, bf16[384,512]{1,0:T(8,128)(2,1)}, u32[]{:S(2)}, u32[]{:S(2)}) collective-permute-start(bf16[384,512]{1,0:T(8,128)(2,1)} %get-tuple-element.45.refs_1_), channel_id=1, source_target_pairs={{0,2},{1,3},{2,0},{3,1},{4,6},{5,7},{6,4},{7,5},{8,10},{9,11},{10,... | collective-permute-start | bytes 1179656 | tf_op jit(solution)/shard_map/ppermute | solution.py:22
  98.6 21.8 %collective-permute-start.18 = (bf16[384,512]{1,0:T(8,128)(2,1)}, bf16[384,512]{1,0:T(8,128)(2,1)}, u32[]{:S(2)}, u32[]{:S(2)}) collective-permute-start(bf16[384,512]{1,0:T(8,128)(2,1)} %fusion.7), channel_id=1, source_target_pairs={{0,1},{1,0},{2,3},{3,2},{4,5},{5,4},{6,7},{7,6},{8,9},{9,8},{10,11... | collective-permute-start | bytes 1179656 | tf_op jit(solution)/shard_map/ppermute | solution.py:22
  98.6 24.8 %collective-permute-start.19 = (bf16[384,512]{1,0:T(8,128)(2,1)}, bf16[384,512]{1,0:T(8,128)(2,1)}, u32[]{:S(2)}, u32[]{:S(2)}) collective-permute-start(bf16[384,512]{1,0:T(8,128)(2,1)} %fusion.7), channel_id=1, source_target_pairs={{0,2},{1,3},{2,0},{3,1},{4,6},{5,7},{6,4},{7,5},{8,10},{9,11},{10,... | collective-permute-start | bytes 1179656 | tf_op jit(solution)/shard_map/ppermute | solution.py:22
  99.1 78.5 %collective-permute-start.26 = (bf16[48,1024]{1,0:T(8,128)(2,1)}, bf16[48,1024]{1,0:T(8,128)(2,1)S(1)}, u32[]{:S(2)}, u32[]{:S(2)}) collective-permute-start(bf16[48,1024]{1,0:T(8,128)(2,1)} %get-tuple-element.58), channel_id=1, source_target_pairs={{0,16},{4,20},{8,24},{12,28},{16,0},{20,4},{24,8},{28,12},{1,17},{... | collective-permute-start | bytes 294920 | tf_op jit(solution)/shard_map/ppermute | solution.py:22
  105.3 72.3 %collective-permute-start.27 = (bf16[48,1024]{1,0:T(8,128)(2,1)}, bf16[48,1024]{1,0:T(8,128)(2,1)S(1)}, u32[]{:S(2)}, u32[]{:S(2)}) collective-permute-start(bf16[48,1024]{1,0:T(8,128)(2,1)} %get-tuple-element.59), channel_id=1, source_target_pairs={{0,20},{4,16},{8,28},{12,24},{16,4},{20,0},{24,12},{28,8},{1,21},{... | collective-permute-start | bytes 294920 | tf_op jit(solution)/shard_map/ppermute | solution.py:22
  113.7 63.9 %collective-permute-start.28 = (bf16[48,1024]{1,0:T(8,128)(2,1)}, bf16[48,1024]{1,0:T(8,128)(2,1)S(1)}, u32[]{:S(2)}, u32[]{:S(2)}) collective-permute-start(bf16[48,1024]{1,0:T(8,128)(2,1)} %get-tuple-element.60), channel_id=1, source_target_pairs={{0,24},{4,28},{8,16},{12,20},{16,8},{20,12},{24,0},{28,4},{1,25},{... | collective-permute-start | bytes 294920 | tf_op jit(solution)/shard_map/ppermute | solution.py:22
  120.4 57.2 %collective-permute-start.29 = (bf16[48,1024]{1,0:T(8,128)(2,1)S(1)}, bf16[48,1024]{1,0:T(8,128)(2,1)S(1)}, u32[]{:S(2)}, u32[]{:S(2)}) collective-permute-start(bf16[48,1024]{1,0:T(8,128)(2,1)S(1)} %copy-done.24), channel_id=1, source_target_pairs={{0,28},{4,24},{8,20},{12,16},{16,12},{20,8},{24,4},{28,0},{1,29},{... | collective-permute-start | bytes 294920 | tf_op jit(solution)/shard_map/ppermute | solution.py:22
  123.4 4.1 %collective-permute-start.20 = (bf16[384,512]{1,0:T(8,128)(2,1)}, bf16[384,512]{1,0:T(8,128)(2,1)S(1)}, u32[]{:S(2)}, u32[]{:S(2)}) collective-permute-start(bf16[384,512]{1,0:T(8,128)(2,1)} %collective-permute-done.19), channel_id=1, source_target_pairs={{0,1},{1,0},{2,3},{3,2},{4,5},{5,4},{6,7},{7,6},{8,9},{9,8},{10,11... | collective-permute-start | bytes 1179656 | tf_op jit(solution)/shard_map/ppermute | solution.py:22
  127.5 7.4 %collective-permute-start.23 = (bf16[96,1024]{1,0:T(8,128)(2,1)S(1)}, bf16[96,1024]{1,0:T(8,128)(2,1)S(1)}, u32[]{:S(2)}, u32[]{:S(2)}) collective-permute-start(bf16[96,1024]{1,0:T(8,128)(2,1)S(1)} %get-tuple-element.55), channel_id=1, source_target_pairs={{0,4},{4,0},{8,12},{12,8},{16,20},{20,16},{24,28},{28,24},{1,5},{5... | collective-permute-start | bytes 589832 | tf_op jit(solution)/shard_map/ppermute | solution.py:22
  134.9 6.5 %collective-permute-start.24 = (bf16[96,1024]{1,0:T(8,128)(2,1)S(1)}, bf16[96,1024]{1,0:T(8,128)(2,1)S(1)}, u32[]{:S(2)}, u32[]{:S(2)}) collective-permute-start(bf16[96,1024]{1,0:T(8,128)(2,1)S(1)} %get-tuple-element.56), channel_id=1, source_target_pairs={{0,8},{4,12},{8,0},{12,4},{16,24},{20,28},{24,16},{28,20},{1,9},{5... | collective-permute-start | bytes 589832 | tf_op jit(solution)/shard_map/ppermute | solution.py:22
  141.4 6.6 %collective-permute-start.25 = (bf16[96,1024]{1,0:T(8,128)(2,1)S(1)}, bf16[96,1024]{1,0:T(8,128)(2,1)S(1)}, u32[]{:S(2)}, u32[]{:S(2)}) collective-permute-start(bf16[96,1024]{1,0:T(8,128)(2,1)S(1)} %get-tuple-element.57), channel_id=1, source_target_pairs={{0,12},{4,8},{8,4},{12,0},{16,28},{20,24},{24,20},{28,16},{1,13},{... | collective-permute-start | bytes 589832 | tf_op jit(solution)/shard_map/ppermute | solution.py:22
  147.9 6.5 %collective-permute-start.30 = (bf16[48,1024]{1,0:T(8,128)(2,1)S(1)}, bf16[48,1024]{1,0:T(8,128)(2,1)S(1)}, u32[]{:S(2)}, u32[]{:S(2)}) collective-permute-start(bf16[48,1024]{1,0:T(8,128)(2,1)S(1)} %get-tuple-element.62), channel_id=1, source_target_pairs={{0,16},{4,20},{8,24},{12,28},{16,0},{20,4},{24,8},{28,12},{1,17},{... | collective-permute-start | bytes 294920 | tf_op jit(solution)/shard_map/ppermute | solution.py:22
  154.4 8.6 %collective-permute-start.31 = (bf16[48,1024]{1,0:T(8,128)(2,1)S(1)}, bf16[48,1024]{1,0:T(8,128)(2,1)S(1)}, u32[]{:S(2)}, u32[]{:S(2)}) collective-permute-start(bf16[48,1024]{1,0:T(8,128)(2,1)S(1)} %get-tuple-element.63), channel_id=1, source_target_pairs={{0,20},{4,16},{8,28},{12,24},{16,4},{20,0},{24,12},{28,8},{1,21},{... | collective-permute-start | bytes 294920 | tf_op jit(solution)/shard_map/ppermute | solution.py:22
  163.0 6.6 %collective-permute-start.32 = (bf16[48,1024]{1,0:T(8,128)(2,1)S(1)}, bf16[48,1024]{1,0:T(8,128)(2,1)S(1)}, u32[]{:S(2)}, u32[]{:S(2)}) collective-permute-start(bf16[48,1024]{1,0:T(8,128)(2,1)S(1)} %get-tuple-element.64), channel_id=1, source_target_pairs={{0,24},{4,28},{8,16},{12,20},{16,8},{20,12},{24,0},{28,4},{1,25},{... | collective-permute-start | bytes 294920 | tf_op jit(solution)/shard_map/ppermute | solution.py:22
  169.6 7.3 %collective-permute-start.33 = (bf16[48,1024]{1,0:T(8,128)(2,1)S(1)}, bf16[48,1024]{1,0:T(8,128)(2,1)S(1)}, u32[]{:S(2)}, u32[]{:S(2)}) collective-permute-start(bf16[48,1024]{1,0:T(8,128)(2,1)S(1)} %get-tuple-element.65), channel_id=1, source_target_pairs={{0,28},{4,24},{8,20},{12,16},{16,12},{20,8},{24,4},{28,0},{1,29},{... | collective-permute-start | bytes 294920 | tf_op jit(solution)/shard_map/ppermute | solution.py:22
  (28 other events, 473.7 us)

commit v3 on v2

--- a/solution.py
+++ b/solution.py
@@ -46,7 +46,7 @@
     across = [k for k in range(1, count) if k & (count // 2)]
     nearer = [k for k in range(2, count // 2)]
     half = len(across) // 2
-    return across[:half] + nearer + across[half:] + [1] * (count > 2)
+    return across[:half] + [1] * (count > 2) + nearer + across[half:]
 
 
 def exchange(chunks, axis, direct):
@@ -305,7 +305,7 @@
     rows = [sizes[k] if k in early else 2 * sizes[k] for k in range(len(sizes))]
     return pl.pallas_call(
         functools.partial(late_kernel, far, tuple(sizes), tuple(early)),
-        out_shape=[jax.ShapeDtypeStruct((count, out_width), jnp.bfloat16) for count in rows],
+        out_shape=[pltpu.HBM((count, out_width), jnp.bfloat16) for count in rows],
         in_specs=[SMEM] + [VMEM] * 4 + [ANY] * 2,
         out_specs=[VMEM] * len(rows),
         scratch_shapes=[
@@ -335,11 +335,13 @@
         pltpu.make_async_copy(ref, weights.at[index], weight_sems.at[index])
         for index, ref in enumerate(weight_refs)
     ]
-    for copy in copies + loads:
+    for copy in copies + loads[:1]:
         copy.start()
     for copy in copies:
         copy.wait()
+    loads[1].start()
     loads[0].wait()
+    loads[2].start()
     in_gate = jnp.dot(rows[...], weights[0], preferred_element_type=jnp.float32)
     loads[1].wait()
     values = jnp.dot(rows[...], weights[1], preferred_element_type=jnp.float32)
@@ -384,7 +386,7 @@
     dims = (((0,), (0,)), ((), ()))
     total = lax.dot_general(masks[0], returned, dims, preferred_element_type=jnp.float32)
     total = total + lax.dot_general(masks[1], returned, dims, preferred_element_type=jnp.float32)
-    return total.astype(jnp.bfloat16)
+    return total
 
 
 def on_device(
@@ -500,11 +502,21 @@
     first_far = after(first_far, product)
     late = late_results(place, far, (first, second, first_far, second_far), downs, sizes, early)
     back_late = exchange(dict(enumerate(late)), "ep", direct)
-    back_late[0] = after(back_late[0], mixer_sum)
-    own_rows = [back_own[k] if k in early else back_late[k][: sizes[k]] for k in range(len(sizes))]
+    width = slot_cap if direct else sizes[0]
+    later = [k for k in range(len(sizes)) if k not in early]
+    own_early = combine_rows(
+        [mask[early[0] * width :] for mask in masks_own],
+        jnp.concatenate([back_own[k] for k in early], axis=0),
+    )
+    back_late[0] = after(back_late[0], mixer_sum, own_early)
     far_rows = [back_late[k][-sizes[k] :] for k in range(len(sizes))]
-    mixed_own = combine_rows(masks_own, jnp.concatenate(own_rows, axis=0))
-    mixed_far = combine_rows(masks_far, jnp.concatenate(far_rows, axis=0))
+    mixed_own = own_early
+    if later:
+        own_rows = [back_late[k][: sizes[k]] for k in later]
+        masks_later = [mask[: len(later) * width] for mask in masks_own]
+        mixed_own = mixed_own + combine_rows(masks_later, jnp.concatenate(own_rows, axis=0))
+    mixed_own = mixed_own.astype(jnp.bfloat16)
+    mixed_far = combine_rows(masks_far, jnp.concatenate(far_rows, axis=0)).astype(jnp.bfloat16)
     mixed = jnp.concatenate([mixed_own, mixed_far], axis=0)
     col_width = down_own.shape[1]
     mixed_near = swapped(mixed[:, col_width:], "tp", near)

time: 181 us -> 148 us (0.82)
  the two profiles are of different devices: /device:TPU:0 before, /device:TPU:17 now
where the time goes in v3:
time: 148 us
  waiting for transfers between devices  60 us (41%)
  starting transfers between devices  41.7 us (28%)
  Pallas kernels  25.4 us (17%)
  other arithmetic  9.52 us (6%)
  local copies, waits for them, and re-layouts  5.93 us (4%)
  matrix products  3.99 us (3%)
    ppermute x34, waiting for transfers between devices, swapped(): lax.ppermute(value, axis, [(source, source ^ mask) for source in range(co...  56.9 us
    ppermute x34, starting transfers between devices, swapped(): lax.ppermute(value, axis, [(source, source ^ mask) for source in range(co...  39.6 us
    pallas_call x1, Pallas kernels, mixer_front(): pl.pallas_call(front_kernel, out_shape=[jax.ShapeDtypeStruct((rows, width...  7.15 us
    pallas_call x1, Pallas kernels, second_hidden(): pl.pallas_call(functools.partial(second_kernel, len(row_parts), len(weigh...  6.57 us
    pallas_call x1, Pallas kernels, first_hidden(): pl.pallas_call(functools.partial(first_kernel, len(row_parts)), out_shape...  5.12 us
    pallas_call x1, Pallas kernels, dispatched(): pl.pallas_call(functools.partial(dispatch_kernel, direct, slot_cap), out_...  3.48 us
    unnamed x64, local copies, waits for them, and re-layouts  3.31 us
    pallas_call x1, Pallas kernels, late_results(): pl.pallas_call(functools.partial(late_kernel, far, tuple(sizes), tuple(ea...  3.11 us
  transfers between devices with their start and end apart: 35, of which 21 were waited for; matrix products, arithmetic and copies ran while one was open for 10% of the time, Pallas kernels for 17%

profile of v3, /device:TPU:17, one launch (start us, length us, event | category | flops | bytes accessed | tf_op | source)
XLA Modules:
  0.0 147.8 jit_solution(9564530259065614224)
XLA Ops:
  3.5 3.5 %dispatch.1 = (bf16[48,2048]{1,0:T(8,128)(2,1)}, bf16[48,2048]{1,0:T(8,128)(2,1)}, bf16[48,2048]{1,0:T(8,128)(2,1)}, bf16[48,2048]{1,0:T(8,128)(2,1)}, bf16[48,2...) custom-call(s32[2]{0:T(128)} %compare_select_fusion.2.place_ref, ...), custom_call_target="tpu_custom_call" | custom-call | flops 150994944 | bytes 2097152 | tf_op jit(solution)/shard_map/dispatch/pallas_call | solution.py:119
  8.0 2.4 %collective-permute-start.11 = (bf16[48,2048]{1,0:T(8,128)(2,1)}, bf16[48,2048]{1,0:T(8,128)(2,1)S(1)}, u32[]{:S(2)}, u32[]{:S(2)}) collective-permute-start(bf16[48,2048]{1,0:T(8,128)(2,1)} %get-tuple-element.41), channel_id=1, source_target_pairs={{0,24},{4,28},{8,16},{12,20},{16,8},{20,12},{24,0},{28,4},{1,25},{... | collective-permute-start | bytes 589832 | tf_op jit(solution)/shard_map/ppermute | solution.py:22
  13.0 7.6 %collective-permute-done.10.refs_5_ = bf16[48,2048]{1,0:T(8,128)(2,1)S(1)} collective-permute-done((bf16[48,2048]{1,0:T(8,128)(2,1)}, bf16[48,2048]{1,0:T(8,128)(2,1)S(1)}, u32[]{:S(2)}, u32[]{:S(2)}) %collective-permute-start.10) | collective-permute-done | bytes 196640 | tf_op jit(solution)/shard_map/ppermute | solution.py:22
  20.5 2.3 %collective-permute-start.4 = (bf16[2048,256]{1,0:T(8,128)(2,1)}, bf16[2048,256]{1,0:T(8,128)(2,1)S(1)}, u32[]{:S(2)}, u32[]{:S(2)}) collective-permute-start(bf16[2048,256]{1,0:T(8,128)(2,1)} %bitcast.70), channel_id=1, source_target_pairs={{0,1},{1,0},{2,3},{3,2},{4,5},{5,4},{6,7},{7,6},{8,9},{9,8},{10,11... | collective-permute-start | bytes 3145736 | tf_op jit(solution)/shard_map/ppermute | solution.py:22
  22.9 2.2 %collective-permute-done.1.refs_8_ = bf16[2048,256]{1,0:T(8,128)(2,1)} collective-permute-done((bf16[2048,256]{1,0:T(8,128)(2,1)}, bf16[2048,256]{1,0:T(8,128)(2,1)}, u32[]{:S(2)}, u32[]{:S(2)}) %collective-permute-start.1) | collective-permute-done | bytes 1048608 | tf_op jit(solution)/shard_map/ppermute | solution.py:22
  25.1 1.5 %collective-permute-start.2 = (bf16[2048,256]{1,0:T(8,128)(2,1)}, bf16[2048,256]{1,0:T(8,128)(2,1)S(1)}, u32[]{:S(2)}, u32[]{:S(2)}) collective-permute-start(bf16[2048,256]{1,0:T(8,128)(2,1)} %collective-permute-done.1.refs_8_), channel_id=1, source_target_pairs={{0,1},{1,0},{2,3},{3,2},{4,5},{5,4},{6,7},{7,6},{8,9},{9,8},{10,11... | collective-permute-start | bytes 3145736 | tf_op jit(solution)/shard_map/ppermute | solution.py:22
  29.1 10.7 %collective-permute-done.12.refs_7_ = bf16[48,2048]{1,0:T(8,128)(2,1)S(1)} collective-permute-done((bf16[48,2048]{1,0:T(8,128)(2,1)}, bf16[48,2048]{1,0:T(8,128)(2,1)S(1)}, u32[]{:S(2)}, u32[]{:S(2)}) %collective-permute-start.12) | collective-permute-done | bytes 196640 | tf_op jit(solution)/shard_map/ppermute | solution.py:22
  40.6 1.9 %fusion.5.refs_0_ = bf16[96,2048]{1,0:T(8,128)(2,1)} fusion(bf16[96,2048]{1,0:T(8,128)(2,1)} %param.14, f32[2048]{0:T(1024)} %param.16, f32[96]{0:T(128)S(1)} %add_rsqrt_fusion), kind=kLoop, calls=%fused_computation.15 | loop fusion | flops 786432 | bytes 795008 | tf_op jit(solution)/shard_map/convert_element_type | solution.py:17
  42.5 1.5 collective-permute-start.6
  49.4 6.5 %collective-permute-done.8.refs_3_ = bf16[48,2048]{1,0:T(8,128)(2,1)S(1)} collective-permute-done((bf16[48,2048]{1,0:T(8,128)(2,1)}, bf16[48,2048]{1,0:T(8,128)(2,1)S(1)}, u32[]{:S(2)}, u32[]{:S(2)}) %collective-permute-start.8) | collective-permute-done | bytes 196640 | tf_op jit(solution)/shard_map/ppermute | solution.py:22
  55.9 1.7 %collective-permute-done.9.refs_4_ = bf16[48,2048]{1,0:T(8,128)(2,1)S(1)} collective-permute-done((bf16[48,2048]{1,0:T(8,128)(2,1)}, bf16[48,2048]{1,0:T(8,128)(2,1)S(1)}, u32[]{:S(2)}, u32[]{:S(2)}) %collective-permute-start.9) | collective-permute-done | bytes 196640 | tf_op jit(solution)/shard_map/ppermute | solution.py:22
  58.3 5.1 %first_hidden.1.first_ref.refs_0_ = bf16[384,512]{1,0:T(8,128)(2,1)} custom-call(bf16[48,2048]{1,0:T(8,128)(2,1)} %get-tuple-element.35.refs_0_, bf16[48,2048]{1,0:T(8,128)(2,1)} %copy-done.13, bf16[48,2048]{1,0:T(8,128)(2,1)} %copy-done.14, bf16[48,2048]{1,0:T(8,128)(2,1)} %copy-done.15, bf16[48,2048]{1,0:T(8,128)(2,1)} %copy-done.16, ...), custom_call_target="tpu_custom_call" | custom-call | flops 1610612736 | bytes 5767168 | tf_op jit(solution)/shard_map/first_hidden/pallas_call | solution.py:199
  63.5 2.3 %collective-permute-start.13 = (bf16[2048,256]{1,0:T(8,128)(2,1)}, bf16[2048,256]{1,0:T(8,128)(2,1)S(1)}, u32[]{:S(2)}, u32[]{:S(2)}) collective-permute-start(bf16[2048,256]{1,0:T(8,128)(2,1)} %collective-permute-done.refs_9_), channel_id=1, source_target_pairs={{0,1},{1,0},{2,3},{3,2},{4,5},{5,4},{6,7},{7,6},{8,9},{9,8},{10,11... | collective-permute-start | bytes 3145736 | tf_op jit(solution)/shard_map/ppermute | solution.py:22
  66.8 1.5 %collective-permute-done.13.refs_11_ = bf16[2048,256]{1,0:T(8,128)(2,1)S(1)} collective-permute-done((bf16[2048,256]{1,0:T(8,128)(2,1)}, bf16[2048,256]{1,0:T(8,128)(2,1)S(1)}, u32[]{:S(2)}, u32[]{:S(2)}) %collective-permute-start.13) | collective-permute-done | bytes 1048608 | tf_op jit(solution)/shard_map/ppermute | solution.py:22
  69.3 6.6 %second_hidden.1 = (bf16[384,512]{1,0:T(8,128)(2,1)}, bf16[48,1024]{1,0:T(8,128)(2,1)}, bf16[48,1024]{1,0:T(8,128)(2,1)}, bf16[48,1024]{1,0:T(8,128)(2,1)}, bf16[48,1024]{1,0:T(8,128)(2,1)}) custom-call(s32[2]{0:T(128)} %compare_select_fusion.2.place_ref, bf16[384,512]{1,0:T(8,128)(2,1)} %first_hidden.1.first_ref.refs_0_, ...), custom_call_target="tpu_custom_call" | custom-call | flops 1048576 | bytes 1048576 | tf_op jit(solution)/shard_map/second_hidden/pallas_call | solution.py:254
  80.6 2.3 %collective-permute-start.22 = (bf16[48,1024]{1,0:T(8,128)(2,1)}, bf16[48,1024]{1,0:T(8,128)(2,1)S(1)}, u32[]{:S(2)}, u32[]{:S(2)}) collective-permute-start(bf16[48,1024]{1,0:T(8,128)(2,1)} %get-tuple-element.52), channel_id=1, source_target_pairs={{0,20},{4,16},{8,28},{12,24},{16,4},{20,0},{24,12},{28,8},{1,21},{... | collective-permute-start | bytes 294920 | tf_op jit(solution)/shard_map/ppermute | solution.py:22
  84.5 1.8 %collective-permute-done.22 = bf16[48,1024]{1,0:T(8,128)(2,1)S(1)} collective-permute-done((bf16[48,1024]{1,0:T(8,128)(2,1)}, bf16[48,1024]{1,0:T(8,128)(2,1)S(1)}, u32[]{:S(2)}, u32[]{:S(2)}) %collective-permute-start.22) | collective-permute-done | bytes 98336 | tf_op jit(solution)/shard_map/ppermute | solution.py:22
  86.2 3.4 %collective-permute-start.24 = (bf16[48,1024]{1,0:T(8,128)(2,1)}, bf16[48,1024]{1,0:T(8,128)(2,1)S(1)}, u32[]{:S(2)}, u32[]{:S(2)}) collective-permute-start(bf16[48,1024]{1,0:T(8,128)(2,1)} %get-tuple-element.54), channel_id=1, source_target_pairs={{0,28},{4,24},{8,20},{12,16},{16,12},{20,8},{24,4},{28,0},{1,29},{... | collective-permute-start | bytes 294920 | tf_op jit(solution)/shard_map/ppermute | solution.py:22
  89.6 3.4 %collective-permute-done.23 = bf16[48,1024]{1,0:T(8,128)(2,1)S(1)} collective-permute-done((bf16[48,1024]{1,0:T(8,128)(2,1)}, bf16[48,1024]{1,0:T(8,128)(2,1)S(1)}, u32[]{:S(2)}, u32[]{:S(2)}) %collective-permute-start.23) | collective-permute-done | bytes 98336 | tf_op jit(solution)/shard_map/ppermute | solution.py:22
  93.8 7.1 %mixer_front.1 = (bf16[384,512]{1,0:T(8,128)(2,1)}, f32[384,512]{1,0:T(8,128)}) custom-call(s32[2]{0:T(128)} %compare_select_fusion.2.place_ref, bf16[96,2048]{1,0:T(8,128)(2,1)} %fusion.5.refs_0_, bf16[96,2048]{1,0:T(8,128)(2,1)} %collective-permute-done.14.refs_1_, bf16[96,2048]{1,0:T(8,128)(2,1)} %collective-permute-done.15.refs_2_, ...), custom_call_target="tpu_custom_call" | custom-call | flops 2415919104 | bytes 8388608 | tf_op jit(solution)/shard_map/mixer_front/pallas_call | solution.py:356
  101.6 2.1 %collective-permute-start.17 = (bf16[2,512]{1,0:T(2,128)(2,1)S(1)}, bf16[2,512]{1,0:T(2,128)(2,1)S(1)}, u32[]{:S(2)}, u32[]{:S(2)}) collective-permute-start(bf16[2,512]{1,0:T(2,128)(2,1)S(1)} %slice.73), channel_id=1, source_target_pairs={{0,4},{4,8},{8,12},{12,16},{16,20},{20,24},{24,28},{1,5},{5,9},{9,... | collective-permute-start | bytes 6152 | tf_op jit(solution)/shard_map/ppermute | solution.py:485
  103.8 3.1 %collective-permute-done.17 = bf16[2,512]{1,0:T(2,128)(2,1)S(1)} collective-permute-done((bf16[2,512]{1,0:T(2,128)(2,1)S(1)}, bf16[2,512]{1,0:T(2,128)(2,1)S(1)}, u32[]{:S(2)}, u32[]{:S(2)}) %collective-permute-start.17) | collective-permute-done | bytes 2080 | tf_op jit(solution)/shard_map/ppermute | solution.py:485
  108.0 1.6 %fusion.8 = bf16[384,512]{1,0:T(8,128)(2,1)S(1)} fusion(f32[384,512]{1,0:T(8,128)} %get-tuple-element.49, f32[386,512]{1,0:T(8,128)S(1)} %maximum_convert_fusion, f32[512]{0:T(512)S(1)} %bitcast.75, f32[512]{0:T(512)S(1)} %bitcast.74, f32[512]{0:T(512)S(1)} %bitcast.73), kind=kLoop, calls=%fused_computation.19 | loop fusion | flops 1376256 | bytes 3545088 | tf_op jit(solution)/shard_map/convert_element_type | solution.py:492
  109.6 2.5 %collective-permute-start.18 = (bf16[384,512]{1,0:T(8,128)(2,1)S(1)}, bf16[384,512]{1,0:T(8,128)(2,1)S(1)}, u32[]{:S(2)}, u32[]{:S(2)}) collective-permute-start(bf16[384,512]{1,0:T(8,128)(2,1)S(1)} %fusion.8), channel_id=1, source_target_pairs={{0,1},{1,0},{2,3},{3,2},{4,5},{5,4},{6,7},{7,6},{8,9},{9,8},{10,11... | collective-permute-start | bytes 1179656 | tf_op jit(solution)/shard_map/ppermute | solution.py:22
  113.1 3.1 %late_down.1 = (bf16[96,1024]{1,0:T(8,128)(2,1)}, bf16[96,1024]{1,0:T(8,128)(2,1)}, bf16[96,1024]{1,0:T(8,128)(2,1)}, bf16[96,1024]{1,0:T(8,128)(2,1)}, bf16[48,...) custom-call(s32[2]{0:T(128)S(1)} %copy-done.5, ...), custom_call_target="tpu_custom_call" | custom-call | flops 1207959552 | bytes 4194304 | tf_op jit(solution)/shard_map/late_down/pallas_call | solution.py:306
  116.8 1.8 %collective-permute-start.28 = (bf16[96,1024]{1,0:T(8,128)(2,1)}, bf16[96,1024]{1,0:T(8,128)(2,1)S(1)}, u32[]{:S(2)}, u32[]{:S(2)}) collective-permute-start(bf16[96,1024]{1,0:T(8,128)(2,1)} %get-tuple-element.60), channel_id=1, source_target_pairs={{0,8},{4,12},{8,0},{12,4},{16,24},{20,28},{24,16},{28,20},{1,9},{5... | collective-permute-start | bytes 589832 | tf_op jit(solution)/shard_map/ppermute | solution.py:22
  119.8 3.0 %collective-permute-done.19 = bf16[384,512]{1,0:T(8,128)(2,1)S(1)} collective-permute-done((bf16[384,512]{1,0:T(8,128)(2,1)S(1)}, bf16[384,512]{1,0:T(8,128)(2,1)S(1)}, u32[]{:S(2)}, u32[]{:S(2)}) %collective-permute-start.19) | collective-permute-done | bytes 393248 | tf_op jit(solution)/shard_map/ppermute | solution.py:22
  126.6 2.1 %collective-permute-start.32 = (bf16[48,1024]{1,0:T(8,128)(2,1)S(1)}, bf16[48,1024]{1,0:T(8,128)(2,1)S(1)}, u32[]{:S(2)}, u32[]{:S(2)}) collective-permute-start(bf16[48,1024]{1,0:T(8,128)(2,1)S(1)} %copy-done.25), channel_id=1, source_target_pairs={{0,24},{4,28},{8,16},{12,20},{16,8},{20,12},{24,0},{28,4},{1,25},{... | collective-permute-start | bytes 294920 | tf_op jit(solution)/shard_map/ppermute | solution.py:22
  128.8 2.1 %collective-permute-start.33 = (bf16[48,1024]{1,0:T(8,128)(2,1)S(1)}, bf16[48,1024]{1,0:T(8,128)(2,1)S(1)}, u32[]{:S(2)}, u32[]{:S(2)}) collective-permute-start(bf16[48,1024]{1,0:T(8,128)(2,1)S(1)} %copy-done.24), channel_id=1, source_target_pairs={{0,28},{4,24},{8,20},{12,16},{16,12},{20,8},{24,4},{28,0},{1,29},{... | collective-permute-start | bytes 294920 | tf_op jit(solution)/shard_map/ppermute | solution.py:22
  131.0 1.6 %collective-permute-done.31 = bf16[48,1024]{1,0:T(8,128)(2,1)S(1)} collective-permute-done((bf16[48,1024]{1,0:T(8,128)(2,1)S(1)}, bf16[48,1024]{1,0:T(8,128)(2,1)S(1)}, u32[]{:S(2)}, u32[]{:S(2)}) %collective-permute-start.31) | collective-permute-done | bytes 98336 | tf_op jit(solution)/shard_map/ppermute | solution.py:22
  132.6 8.0 %collective-permute-done.32 = bf16[48,1024]{1,0:T(8,128)(2,1)S(1)} collective-permute-done((bf16[48,1024]{1,0:T(8,128)(2,1)S(1)}, bf16[48,1024]{1,0:T(8,128)(2,1)S(1)}, u32[]{:S(2)}, u32[]{:S(2)}) %collective-permute-start.32) | collective-permute-done | bytes 98336 | tf_op jit(solution)/shard_map/ppermute | solution.py:22
  140.5 3.7 %collective-permute-done.33 = bf16[48,1024]{1,0:T(8,128)(2,1)S(1)} collective-permute-done((bf16[48,1024]{1,0:T(8,128)(2,1)S(1)}, bf16[48,1024]{1,0:T(8,128)(2,1)S(1)}, u32[]{:S(2)}, u32[]{:S(2)}) %collective-permute-start.33) | collective-permute-done | bytes 98336 | tf_op jit(solution)/shard_map/ppermute | solution.py:22
  (147 shorter events, 36.7 us)
Async XLA Ops:
  0.6 24.4 %collective-permute-start.1 = (bf16[2048,256]{1,0:T(8,128)(2,1)}, bf16[2048,256]{1,0:T(8,128)(2,1)}, u32[]{:S(2)}, u32[]{:S(2)}) collective-permute-start(bf16[2048,256]{1,0:T(8,128)(2,1)} %bitcast.67), channel_id=1, source_target_pairs={{0,2},{1,3},{2,0},{3,1},{4,6},{5,7},{6,4},{7,5},{8,10},{9,11},{10,... | collective-permute-start | bytes 3145736 | tf_op jit(solution)/shard_map/ppermute | solution.py:22
  1.9 42.1 %collective-permute-start.3 = (bf16[2048,256]{1,0:T(8,128)(2,1)}, bf16[2048,256]{1,0:T(8,128)(2,1)}, u32[]{:S(2)}, u32[]{:S(2)}) collective-permute-start(bf16[2048,256]{1,0:T(8,128)(2,1)} %bitcast.68), channel_id=1, source_target_pairs={{0,1},{1,0},{2,3},{3,2},{4,5},{5,4},{6,7},{7,6},{8,9},{9,8},{10,11... | collective-permute-start | bytes 3145736 | tf_op jit(solution)/shard_map/ppermute | solution.py:22
  2.9 39.7 %collective-permute-start.5 = (bf16[1024,512]{1,0:T(8,128)(2,1)}, bf16[1024,512]{1,0:T(8,128)(2,1)S(1)}, u32[]{:S(2)}, u32[]{:S(2)}) collective-permute-start(bf16[1024,512]{1,0:T(8,128)(2,1)} %bitcast.64), channel_id=1, source_target_pairs={{0,1},{1,0},{2,3},{3,2},{4,5},{5,4},{6,7},{7,6},{8,9},{9,8},{10,11... | collective-permute-start | bytes 3145736 | tf_op jit(solution)/shard_map/ppermute | solution.py:22
  7.0 13.6 %collective-permute-start.10 = (bf16[48,2048]{1,0:T(8,128)(2,1)}, bf16[48,2048]{1,0:T(8,128)(2,1)S(1)}, u32[]{:S(2)}, u32[]{:S(2)}) collective-permute-start(bf16[48,2048]{1,0:T(8,128)(2,1)} %get-tuple-element.40), channel_id=1, source_target_pairs={{0,20},{4,16},{8,28},{12,24},{16,4},{20,0},{24,12},{28,8},{1,21},{... | collective-permute-start | bytes 589832 | tf_op jit(solution)/shard_map/ppermute | solution.py:22
  8.0 20.5 %collective-permute-start.11 = (bf16[48,2048]{1,0:T(8,128)(2,1)}, bf16[48,2048]{1,0:T(8,128)(2,1)S(1)}, u32[]{:S(2)}, u32[]{:S(2)}) collective-permute-start(bf16[48,2048]{1,0:T(8,128)(2,1)} %get-tuple-element.41), channel_id=1, source_target_pairs={{0,24},{4,28},{8,16},{12,20},{16,8},{20,12},{24,0},{28,4},{1,25},{... | collective-permute-start | bytes 589832 | tf_op jit(solution)/shard_map/ppermute | solution.py:22
  20.5 23.5 %collective-permute-start.4 = (bf16[2048,256]{1,0:T(8,128)(2,1)}, bf16[2048,256]{1,0:T(8,128)(2,1)S(1)}, u32[]{:S(2)}, u32[]{:S(2)}) collective-permute-start(bf16[2048,256]{1,0:T(8,128)(2,1)} %bitcast.70), channel_id=1, source_target_pairs={{0,1},{1,0},{2,3},{3,2},{4,5},{5,4},{6,7},{7,6},{8,9},{9,8},{10,11... | collective-permute-start | bytes 3145736 | tf_op jit(solution)/shard_map/ppermute | solution.py:22
  25.1 20.2 %collective-permute-start.2 = (bf16[2048,256]{1,0:T(8,128)(2,1)}, bf16[2048,256]{1,0:T(8,128)(2,1)S(1)}, u32[]{:S(2)}, u32[]{:S(2)}) collective-permute-start(bf16[2048,256]{1,0:T(8,128)(2,1)} %collective-permute-done.1.refs_8_), channel_id=1, source_target_pairs={{0,1},{1,0},{2,3},{3,2},{4,5},{5,4},{6,7},{7,6},{8,9},{9,8},{10,11... | collective-permute-start | bytes 3145736 | tf_op jit(solution)/shard_map/ppermute | solution.py:22
  28.6 11.3 %collective-permute-start.12 = (bf16[48,2048]{1,0:T(8,128)(2,1)}, bf16[48,2048]{1,0:T(8,128)(2,1)S(1)}, u32[]{:S(2)}, u32[]{:S(2)}) collective-permute-start(bf16[48,2048]{1,0:T(8,128)(2,1)} %get-tuple-element.42), channel_id=1, source_target_pairs={{0,28},{4,24},{8,20},{12,16},{16,12},{20,8},{24,4},{28,0},{1,29},{... | collective-permute-start | bytes 589832 | tf_op jit(solution)/shard_map/ppermute | solution.py:22
  39.9 23.7 %collective-permute-start = (bf16[2048,256]{1,0:T(8,128)(2,1)}, bf16[2048,256]{1,0:T(8,128)(2,1)}, u32[]{:S(2)}, u32[]{:S(2)}) collective-permute-start(bf16[2048,256]{1,0:T(8,128)(2,1)} %bitcast.71), channel_id=1, source_target_pairs={{0,2},{1,3},{2,0},{3,1},{4,6},{5,7},{6,4},{7,5},{8,10},{9,11},{10,... | collective-permute-start | bytes 3145736 | tf_op jit(solution)/shard_map/ppermute | solution.py:22
  42.5 5.4 %collective-permute-start.6 = (bf16[48,2048]{1,0:T(8,128)(2,1)}, bf16[48,2048]{1,0:T(8,128)(2,1)S(1)}, u32[]{:S(2)}, u32[]{:S(2)}) collective-permute-start(bf16[48,2048]{1,0:T(8,128)(2,1)} %get-tuple-element.36), channel_id=1, source_target_pairs={{0,4},{4,0},{8,12},{12,8},{16,20},{20,16},{24,28},{28,24},{1,5},{5... | collective-permute-start | bytes 589832 | tf_op jit(solution)/shard_map/ppermute | solution.py:22
  44.0 5.4 %collective-permute-start.7 = (bf16[48,2048]{1,0:T(8,128)(2,1)}, bf16[48,2048]{1,0:T(8,128)(2,1)S(1)}, u32[]{:S(2)}, u32[]{:S(2)}) collective-permute-start(bf16[48,2048]{1,0:T(8,128)(2,1)} %get-tuple-element.37), channel_id=1, source_target_pairs={{0,8},{4,12},{8,0},{12,4},{16,24},{20,28},{24,16},{28,20},{1,9},{5... | collective-permute-start | bytes 589832 | tf_op jit(solution)/shard_map/ppermute | solution.py:22
  44.0 11.8 %collective-permute-start.8 = (bf16[48,2048]{1,0:T(8,128)(2,1)}, bf16[48,2048]{1,0:T(8,128)(2,1)S(1)}, u32[]{:S(2)}, u32[]{:S(2)}) collective-permute-start(bf16[48,2048]{1,0:T(8,128)(2,1)} %get-tuple-element.38), channel_id=1, source_target_pairs={{0,12},{4,8},{8,4},{12,0},{16,28},{20,24},{24,20},{28,16},{1,13},{... | collective-permute-start | bytes 589832 | tf_op jit(solution)/shard_map/ppermute | solution.py:22
  45.3 12.3 %collective-permute-start.9 = (bf16[48,2048]{1,0:T(8,128)(2,1)}, bf16[48,2048]{1,0:T(8,128)(2,1)S(1)}, u32[]{:S(2)}, u32[]{:S(2)}) collective-permute-start(bf16[48,2048]{1,0:T(8,128)(2,1)} %get-tuple-element.39), channel_id=1, source_target_pairs={{0,16},{4,20},{8,24},{12,28},{16,0},{20,4},{24,8},{28,12},{1,17},{... | collective-permute-start | bytes 589832 | tf_op jit(solution)/shard_map/ppermute | solution.py:22
  65.8 10.9 %collective-permute-start.15 = (bf16[96,2048]{1,0:T(8,128)(2,1)}, bf16[96,2048]{1,0:T(8,128)(2,1)}, u32[]{:S(2)}, u32[]{:S(2)}) collective-permute-start(bf16[96,2048]{1,0:T(8,128)(2,1)} %fusion.5.refs_0_), channel_id=1, source_target_pairs={{0,2},{1,3},{2,0},{3,1},{4,6},{5,7},{6,4},{7,5},{8,10},{9,11},{10,... | collective-permute-start | bytes 1179656 | tf_op jit(solution)/shard_map/ppermute | solution.py:22
  66.5 14.1 %collective-permute-start.14 = (bf16[96,2048]{1,0:T(8,128)(2,1)}, bf16[96,2048]{1,0:T(8,128)(2,1)}, u32[]{:S(2)}, u32[]{:S(2)}) collective-permute-start(bf16[96,2048]{1,0:T(8,128)(2,1)} %fusion.5.refs_0_), channel_id=1, source_target_pairs={{0,1},{1,0},{2,3},{3,2},{4,5},{5,4},{6,7},{7,6},{8,9},{9,8},{10,11... | collective-permute-start | bytes 1179656 | tf_op jit(solution)/shard_map/ppermute | solution.py:22
  76.7 16.3 %collective-permute-start.16 = (bf16[96,2048]{1,0:T(8,128)(2,1)}, bf16[96,2048]{1,0:T(8,128)(2,1)S(1)}, u32[]{:S(2)}, u32[]{:S(2)}) collective-permute-start(bf16[96,2048]{1,0:T(8,128)(2,1)} %collective-permute-done.15.refs_2_), channel_id=1, source_target_pairs={{0,1},{1,0},{2,3},{3,2},{4,5},{5,4},{6,7},{7,6},{8,9},{9,8},{10,11... | collective-permute-start | bytes 1179656 | tf_op jit(solution)/shard_map/ppermute | solution.py:22
  77.6 5.5 %collective-permute-start.21 = (bf16[48,1024]{1,0:T(8,128)(2,1)}, bf16[48,1024]{1,0:T(8,128)(2,1)S(1)}, u32[]{:S(2)}, u32[]{:S(2)}) collective-permute-start(bf16[48,1024]{1,0:T(8,128)(2,1)} %get-tuple-element.51), channel_id=1, source_target_pairs={{0,16},{4,20},{8,24},{12,28},{16,0},{20,4},{24,8},{28,12},{1,17},{... | collective-permute-start | bytes 294920 | tf_op jit(solution)/shard_map/ppermute | solution.py:22
  79.1 33.9 %collective-permute-start.25 = (bf16[384,512]{1,0:T(8,128)(2,1)S(1)}, bf16[384,512]{1,0:T(8,128)(2,1)S(1)}, u32[]{:S(2)}, u32[]{:S(2)}) collective-permute-start(bf16[384,512]{1,0:T(8,128)(2,1)S(1)} %copy-done.1), channel_id=1, source_target_pairs={{0,2},{1,3},{2,0},{3,1},{4,6},{5,7},{6,4},{7,5},{8,10},{9,11},{10,... | collective-permute-start | bytes 1179656 | tf_op jit(solution)/shard_map/ppermute | solution.py:22
  79.3 33.7 %collective-permute-start.26 = (bf16[384,512]{1,0:T(8,128)(2,1)}, bf16[384,512]{1,0:T(8,128)(2,1)S(1)}, u32[]{:S(2)}, u32[]{:S(2)}) collective-permute-start(bf16[384,512]{1,0:T(8,128)(2,1)} %get-tuple-element.45.refs_1_), channel_id=1, source_target_pairs={{0,2},{1,3},{2,0},{3,1},{4,6},{5,7},{6,4},{7,5},{8,10},{9,11},{10,... | collective-permute-start | bytes 1179656 | tf_op jit(solution)/shard_map/ppermute | solution.py:22
  80.6 5.6 %collective-permute-start.22 = (bf16[48,1024]{1,0:T(8,128)(2,1)}, bf16[48,1024]{1,0:T(8,128)(2,1)S(1)}, u32[]{:S(2)}, u32[]{:S(2)}) collective-permute-start(bf16[48,1024]{1,0:T(8,128)(2,1)} %get-tuple-element.52), channel_id=1, source_target_pairs={{0,20},{4,16},{8,28},{12,24},{16,4},{20,0},{24,12},{28,8},{1,21},{... | collective-permute-start | bytes 294920 | tf_op jit(solution)/shard_map/ppermute | solution.py:22
  83.2 9.9 %collective-permute-start.23 = (bf16[48,1024]{1,0:T(8,128)(2,1)}, bf16[48,1024]{1,0:T(8,128)(2,1)S(1)}, u32[]{:S(2)}, u32[]{:S(2)}) collective-permute-start(bf16[48,1024]{1,0:T(8,128)(2,1)} %get-tuple-element.53), channel_id=1, source_target_pairs={{0,24},{4,28},{8,16},{12,20},{16,8},{20,12},{24,0},{28,4},{1,25},{... | collective-permute-start | bytes 294920 | tf_op jit(solution)/shard_map/ppermute | solution.py:22
  86.2 17.5 %collective-permute-start.24 = (bf16[48,1024]{1,0:T(8,128)(2,1)}, bf16[48,1024]{1,0:T(8,128)(2,1)S(1)}, u32[]{:S(2)}, u32[]{:S(2)}) collective-permute-start(bf16[48,1024]{1,0:T(8,128)(2,1)} %get-tuple-element.54), channel_id=1, source_target_pairs={{0,28},{4,24},{8,20},{12,16},{16,12},{20,8},{24,4},{28,0},{1,29},{... | collective-permute-start | bytes 294920 | tf_op jit(solution)/shard_map/ppermute | solution.py:22
  101.6 5.2 %collective-permute-start.17 = (bf16[2,512]{1,0:T(2,128)(2,1)S(1)}, bf16[2,512]{1,0:T(2,128)(2,1)S(1)}, u32[]{:S(2)}, u32[]{:S(2)}) collective-permute-start(bf16[2,512]{1,0:T(2,128)(2,1)S(1)} %slice.73), channel_id=1, source_target_pairs={{0,4},{4,8},{8,12},{12,16},{16,20},{20,24},{24,28},{1,5},{5,9},{9,... | collective-permute-start | bytes 6152 | tf_op jit(solution)/shard_map/ppermute | solution.py:485
  109.6 10.2 %collective-permute-start.18 = (bf16[384,512]{1,0:T(8,128)(2,1)S(1)}, bf16[384,512]{1,0:T(8,128)(2,1)S(1)}, u32[]{:S(2)}, u32[]{:S(2)}) collective-permute-start(bf16[384,512]{1,0:T(8,128)(2,1)S(1)} %fusion.8), channel_id=1, source_target_pairs={{0,1},{1,0},{2,3},{3,2},{4,5},{5,4},{6,7},{7,6},{8,9},{9,8},{10,11... | collective-permute-start | bytes 1179656 | tf_op jit(solution)/shard_map/ppermute | solution.py:22
  112.1 10.6 %collective-permute-start.19 = (bf16[384,512]{1,0:T(8,128)(2,1)S(1)}, bf16[384,512]{1,0:T(8,128)(2,1)S(1)}, u32[]{:S(2)}, u32[]{:S(2)}) collective-permute-start(bf16[384,512]{1,0:T(8,128)(2,1)S(1)} %fusion.8), channel_id=1, source_target_pairs={{0,2},{1,3},{2,0},{3,1},{4,6},{5,7},{6,4},{7,5},{8,10},{9,11},{10,... | collective-permute-start | bytes 1179656 | tf_op jit(solution)/shard_map/ppermute | solution.py:22
  116.2 10.4 %collective-permute-start.27 = (bf16[96,1024]{1,0:T(8,128)(2,1)}, bf16[96,1024]{1,0:T(8,128)(2,1)S(1)}, u32[]{:S(2)}, u32[]{:S(2)}) collective-permute-start(bf16[96,1024]{1,0:T(8,128)(2,1)} %get-tuple-element.59), channel_id=1, source_target_pairs={{0,4},{4,0},{8,12},{12,8},{16,20},{20,16},{24,28},{28,24},{1,5},{5... | collective-permute-start | bytes 589832 | tf_op jit(solution)/shard_map/ppermute | solution.py:22
  116.8 12.0 %collective-permute-start.28 = (bf16[96,1024]{1,0:T(8,128)(2,1)}, bf16[96,1024]{1,0:T(8,128)(2,1)S(1)}, u32[]{:S(2)}, u32[]{:S(2)}) collective-permute-start(bf16[96,1024]{1,0:T(8,128)(2,1)} %get-tuple-element.60), channel_id=1, source_target_pairs={{0,8},{4,12},{8,0},{12,4},{16,24},{20,28},{24,16},{28,20},{1,9},{5... | collective-permute-start | bytes 589832 | tf_op jit(solution)/shard_map/ppermute | solution.py:22
  118.6 12.3 %collective-permute-start.29 = (bf16[96,1024]{1,0:T(8,128)(2,1)}, bf16[96,1024]{1,0:T(8,128)(2,1)S(1)}, u32[]{:S(2)}, u32[]{:S(2)}) collective-permute-start(bf16[96,1024]{1,0:T(8,128)(2,1)} %get-tuple-element.61), channel_id=1, source_target_pairs={{0,12},{4,8},{8,4},{12,0},{16,28},{20,24},{24,20},{28,16},{1,13},{... | collective-permute-start | bytes 589832 | tf_op jit(solution)/shard_map/ppermute | solution.py:22
  119.7 11.2 %collective-permute-start.30 = (bf16[48,1024]{1,0:T(8,128)(2,1)}, bf16[48,1024]{1,0:T(8,128)(2,1)S(1)}, u32[]{:S(2)}, u32[]{:S(2)}) collective-permute-start(bf16[48,1024]{1,0:T(8,128)(2,1)} %get-tuple-element.62), channel_id=1, source_target_pairs={{0,16},{4,20},{8,24},{12,28},{16,0},{20,4},{24,8},{28,12},{1,17},{... | collective-permute-start | bytes 294920 | tf_op jit(solution)/shard_map/ppermute | solution.py:22
  125.0 7.5 %collective-permute-start.31 = (bf16[48,1024]{1,0:T(8,128)(2,1)S(1)}, bf16[48,1024]{1,0:T(8,128)(2,1)S(1)}, u32[]{:S(2)}, u32[]{:S(2)}) collective-permute-start(bf16[48,1024]{1,0:T(8,128)(2,1)S(1)} %copy-done.26), channel_id=1, source_target_pairs={{0,20},{4,16},{8,28},{12,24},{16,4},{20,0},{24,12},{28,8},{1,21},{... | collective-permute-start | bytes 294920 | tf_op jit(solution)/shard_map/ppermute | solution.py:22
  126.6 13.9 %collective-permute-start.32 = (bf16[48,1024]{1,0:T(8,128)(2,1)S(1)}, bf16[48,1024]{1,0:T(8,128)(2,1)S(1)}, u32[]{:S(2)}, u32[]{:S(2)}) collective-permute-start(bf16[48,1024]{1,0:T(8,128)(2,1)S(1)} %copy-done.25), channel_id=1, source_target_pairs={{0,24},{4,28},{8,16},{12,20},{16,8},{20,12},{24,0},{28,4},{1,25},{... | collective-permute-start | bytes 294920 | tf_op jit(solution)/shard_map/ppermute | solution.py:22
  128.8 15.5 %collective-permute-start.33 = (bf16[48,1024]{1,0:T(8,128)(2,1)S(1)}, bf16[48,1024]{1,0:T(8,128)(2,1)S(1)}, u32[]{:S(2)}, u32[]{:S(2)}) collective-permute-start(bf16[48,1024]{1,0:T(8,128)(2,1)S(1)} %copy-done.24), channel_id=1, source_target_pairs={{0,28},{4,24},{8,20},{12,16},{16,12},{20,8},{24,4},{28,0},{1,29},{... | collective-permute-start | bytes 294920 | tf_op jit(solution)/shard_map/ppermute | solution.py:22
  (30 other events, 384.0 us)

commit v4 on v3

--- a/solution.py
+++ b/solution.py
@@ -325,7 +325,7 @@
 
 def front_kernel(place_ref, *refs):
     part_refs, weight_refs, refs = refs[:4], refs[4:7], refs[7:]
-    product_ref, gate_ref, rows, weights, row_sems, weight_sems = refs
+    product_ref, gate_ref, rim_ref, rows, weights, row_sems, weight_sems = refs
     tok = part_refs[0].shape[0]
     copies = []
     for j, ref in enumerate(part_refs):
@@ -345,12 +345,14 @@
     in_gate = jnp.dot(rows[...], weights[0], preferred_element_type=jnp.float32)
     loads[1].wait()
     values = jnp.dot(rows[...], weights[1], preferred_element_type=jnp.float32)
-    product_ref[...] = (in_gate * values).astype(jnp.bfloat16)
+    product = (in_gate * values).astype(jnp.bfloat16)
+    product_ref[...] = product
+    rim_ref[...] = product[product.shape[0] - rim_ref.shape[0] :]
     loads[2].wait()
     gate_ref[...] = jnp.dot(rows[...], weights[2], preferred_element_type=jnp.float32)
 
 
-def mixer_front(place, parts, weights):
+def mixer_front(place, parts, weights, rim):
     rows = sum(part.shape[0] for part in parts)
     depth, width = weights[0].shape
     return pl.pallas_call(
@@ -358,9 +360,10 @@
         out_shape=[
             jax.ShapeDtypeStruct((rows, width), jnp.bfloat16),
             jax.ShapeDtypeStruct((rows, width), jnp.float32),
+            jax.ShapeDtypeStruct((rim, width), jnp.bfloat16),
         ],
         in_specs=[SMEM] + [ANY] * 7,
-        out_specs=[VMEM, VMEM],
+        out_specs=[VMEM, VMEM, VMEM],
         scratch_shapes=[
             pltpu.VMEM((rows, depth), jnp.bfloat16),
             pltpu.VMEM((3, depth, width), jnp.bfloat16),
@@ -454,6 +457,7 @@
     gates[far ^ near] = swapped(gates[far], "tp", near)
     ready = (masks_own, masks_far, mixer_normed, gates[far ^ near])
     ready += (gates[near], ups[near], down_near)
+    ready += tuple(tap_rows)
     arrived[0] = after(arrived[0], *ready)
     slots_in = [arrived[k] for k in range(len(sizes))]
 
@@ -473,18 +477,18 @@
     second_far = swapped(second, "tp", far)
     back_own = exchange(done_own, "ep", direct)
 
-    normed = {0: after(mixer_normed, ups[far], first)}
+    normed = {0: mixer_normed}
     normed[far] = swapped(normed[0], "tp", far)
     normed[near] = swapped(normed[0], "tp", near)
     normed = {j: after(normed[j], second) for j in normed}
     normed[far ^ near] = swapped(normed[far], "tp", near)
-    product, out_gate = mixer_front(
-        place, [normed[j] for j in order], [in_gate_weight, value_weight, out_gate_weight]
+    front_weights = [in_gate_weight, value_weight, out_gate_weight]
+    product, out_gate, rim_sent = mixer_front(
+        place, [normed[j] for j in order], front_weights, tap_count - 1
     )
     row_count = product.shape[0]
-    rim_rows = lax.ppermute(
-        product[row_count - (tap_count - 1) :], "ep", [(i, i + 1) for i in range(ep_count - 1)]
-    )
+    steps = [(source, source + 1) for source in range(ep_count - 1)]
+    rim_rows = lax.ppermute(rim_sent, "ep", steps)
     extended = jnp.concatenate([rim_rows, product], axis=0).astype(jnp.float32)
     conv_sum = tap_rows[0] * extended[0:row_count]
     for tap_index in range(1, tap_count):

time: 148 us -> 148 us (level)
  starting transfers between devices: 41.7 us -> 43.2 us
  waiting for transfers between devices: 60 us -> 58.5 us
    ppermute x34, waiting for transfers between devices: 56.9 us -> 55.4 us  [swapped(): lax.ppermute(value, axis, [(source, source ^ mask) for source in range(co...]
  transfers between devices with their start and end apart: 35 -> 35, of which waited for: 21 -> 18; matrix products, arithmetic and copies ran while one was open for 10% -> 10% of each run, Pallas kernels for 17% -> 17%
where the time goes in v4:
time: 148 us; the launch traced here: 147 us
  waiting for transfers between devices  58.5 us (40%)
  starting transfers between devices  43.2 us (29%)
  Pallas kernels  25.4 us (17%)
  other arithmetic  9.56 us (6%)
  local copies, waits for them, and re-layouts  5.23 us (4%)
  matrix products  3.98 us (3%)
    ppermute x34, waiting for transfers between devices, swapped(): lax.ppermute(value, axis, [(source, source ^ mask) for source in range(co...  55.4 us
    ppermute x34, starting transfers between devices, swapped(): lax.ppermute(value, axis, [(source, source ^ mask) for source in range(co...  40.9 us
    pallas_call x1, Pallas kernels, mixer_front(): pl.pallas_call(front_kernel, out_shape=[jax.ShapeDtypeStruct((rows, width...  7.15 us
    pallas_call x1, Pallas kernels, second_hidden(): pl.pallas_call(functools.partial(second_kernel, len(row_parts), len(weigh...  6.58 us
    pallas_call x1, Pallas kernels, first_hidden(): pl.pallas_call(functools.partial(first_kernel, len(row_parts)), out_shape...  5.12 us
    pallas_call x1, Pallas kernels, dispatched(): pl.pallas_call(functools.partial(dispatch_kernel, direct, slot_cap), out_...  3.46 us
    unnamed x64, local copies, waits for them, and re-layouts  3.31 us
    pallas_call x1, Pallas kernels, late_results(): pl.pallas_call(functools.partial(late_kernel, far, tuple(sizes), tuple(ea...  3.11 us
  transfers between devices with their start and end apart: 35, of which 18 were waited for; matrix products, arithmetic and copies ran while one was open for 10% of the time, Pallas kernels for 17%

profile of v4, /device:TPU:17, one launch (start us, length us, event | category | flops | bytes accessed | tf_op | source)
XLA Modules:
  0.0 147.1 jit_solution(10416020703636087591)
XLA Ops:
  3.5 3.5 %dispatch.1 = (bf16[48,2048]{1,0:T(8,128)(2,1)}, bf16[48,2048]{1,0:T(8,128)(2,1)}, bf16[48,2048]{1,0:T(8,128)(2,1)}, bf16[48,2048]{1,0:T(8,128)(2,1)}, bf16[48,2...) custom-call(s32[2]{0:T(128)} %compare_select_fusion.2.place_ref, ...), custom_call_target="tpu_custom_call" | custom-call | flops 150994944 | bytes 2097152 | tf_op jit(solution)/shard_map/dispatch/pallas_call | solution.py:119
  7.2 2.3 %collective-permute-start.11 = (bf16[48,2048]{1,0:T(8,128)(2,1)}, bf16[48,2048]{1,0:T(8,128)(2,1)S(1)}, u32[]{:S(2)}, u32[]{:S(2)}) collective-permute-start(bf16[48,2048]{1,0:T(8,128)(2,1)} %get-tuple-element.42), channel_id=1, source_target_pairs={{0,28},{4,24},{8,20},{12,16},{16,12},{20,8},{24,4},{28,0},{1,29},{... | collective-permute-start | bytes 589832 | tf_op jit(solution)/shard_map/ppermute | solution.py:22
  11.9 9.8 %collective-permute-done.10.refs_6_ = bf16[48,2048]{1,0:T(8,128)(2,1)S(1)} collective-permute-done((bf16[48,2048]{1,0:T(8,128)(2,1)}, bf16[48,2048]{1,0:T(8,128)(2,1)S(1)}, u32[]{:S(2)}, u32[]{:S(2)}) %collective-permute-start.10) | collective-permute-done | bytes 196640 | tf_op jit(solution)/shard_map/ppermute | solution.py:22
  21.7 2.2 %collective-permute-start.3 = (bf16[2048,256]{1,0:T(8,128)(2,1)}, bf16[2048,256]{1,0:T(8,128)(2,1)S(1)}, u32[]{:S(2)}, u32[]{:S(2)}) collective-permute-start(bf16[2048,256]{1,0:T(8,128)(2,1)} %bitcast.70), channel_id=1, source_target_pairs={{0,1},{1,0},{2,3},{3,2},{4,5},{5,4},{6,7},{7,6},{8,9},{9,8},{10,11... | collective-permute-start | bytes 3145736 | tf_op jit(solution)/shard_map/ppermute | solution.py:22
  25.1 1.5 %collective-permute-start.1 = (bf16[2048,256]{1,0:T(8,128)(2,1)}, bf16[2048,256]{1,0:T(8,128)(2,1)S(1)}, u32[]{:S(2)}, u32[]{:S(2)}) collective-permute-start(bf16[2048,256]{1,0:T(8,128)(2,1)} %collective-permute-done.refs_8_), channel_id=1, source_target_pairs={{0,1},{1,0},{2,3},{3,2},{4,5},{5,4},{6,7},{7,6},{8,9},{9,8},{10,11... | collective-permute-start | bytes 3145736 | tf_op jit(solution)/shard_map/ppermute | solution.py:22
  29.2 5.0 %collective-permute-done.5.refs_1_ = bf16[48,2048]{1,0:T(8,128)(2,1)S(1)} collective-permute-done((bf16[48,2048]{1,0:T(8,128)(2,1)}, bf16[48,2048]{1,0:T(8,128)(2,1)S(1)}, u32[]{:S(2)}, u32[]{:S(2)}) %collective-permute-start.5) | collective-permute-done | bytes 196640 | tf_op jit(solution)/shard_map/ppermute | solution.py:22
  34.3 1.5 %collective-permute-start.12 = (bf16[2048,256]{1,0:T(8,128)(2,1)}, bf16[2048,256]{1,0:T(8,128)(2,1)}, u32[]{:S(2)}, u32[]{:S(2)}) collective-permute-start(bf16[2048,256]{1,0:T(8,128)(2,1)} %bitcast.71), channel_id=1, source_target_pairs={{0,2},{1,3},{2,0},{3,1},{4,6},{5,7},{6,4},{7,5},{8,10},{9,11},{10,... | collective-permute-start | bytes 3145736 | tf_op jit(solution)/shard_map/ppermute | solution.py:22
  35.7 1.9 %fusion.5.refs_0_ = bf16[96,2048]{1,0:T(8,128)(2,1)} fusion(bf16[96,2048]{1,0:T(8,128)(2,1)} %param.14, f32[2048]{0:T(1024)} %param.16, f32[96]{0:T(128)S(1)} %add_rsqrt_fusion), kind=kLoop, calls=%fused_computation.15 | loop fusion | flops 786432 | bytes 795008 | tf_op jit(solution)/shard_map/convert_element_type | solution.py:17
  40.2 2.3 %collective-permute-start.9 = (bf16[48,2048]{1,0:T(8,128)(2,1)}, bf16[48,2048]{1,0:T(8,128)(2,1)S(1)}, u32[]{:S(2)}, u32[]{:S(2)}) collective-permute-start(bf16[48,2048]{1,0:T(8,128)(2,1)} %get-tuple-element.40), channel_id=1, source_target_pairs={{0,20},{4,16},{8,28},{12,24},{16,4},{20,0},{24,12},{28,8},{1,21},{... | collective-permute-start | bytes 589832 | tf_op jit(solution)/shard_map/ppermute | solution.py:22
  44.2 7.4 %collective-permute-done.7.refs_3_ = bf16[48,2048]{1,0:T(8,128)(2,1)S(1)} collective-permute-done((bf16[48,2048]{1,0:T(8,128)(2,1)}, bf16[48,2048]{1,0:T(8,128)(2,1)S(1)}, u32[]{:S(2)}, u32[]{:S(2)}) %collective-permute-start.7) | collective-permute-done | bytes 196640 | tf_op jit(solution)/shard_map/ppermute | solution.py:22
  51.6 5.2 %collective-permute-done.9.refs_5_ = bf16[48,2048]{1,0:T(8,128)(2,1)S(1)} collective-permute-done((bf16[48,2048]{1,0:T(8,128)(2,1)}, bf16[48,2048]{1,0:T(8,128)(2,1)S(1)}, u32[]{:S(2)}, u32[]{:S(2)}) %collective-permute-start.9) | collective-permute-done | bytes 196640 | tf_op jit(solution)/shard_map/ppermute | solution.py:22
  57.4 5.1 %first_hidden.1.first_ref.refs_0_ = bf16[384,512]{1,0:T(8,128)(2,1)} custom-call(bf16[48,2048]{1,0:T(8,128)(2,1)} %get-tuple-element.35.refs_0_, bf16[48,2048]{1,0:T(8,128)(2,1)} %copy-done.12, bf16[48,2048]{1,0:T(8,128)(2,1)} %copy-done.13, bf16[48,2048]{1,0:T(8,128)(2,1)} %copy-done.14, bf16[48,2048]{1,0:T(8,128)(2,1)} %copy-done.15, ...), custom_call_target="tpu_custom_call" | custom-call | flops 1610612736 | bytes 5767168 | tf_op jit(solution)/shard_map/first_hidden/pallas_call | solution.py:199
  62.6 2.1 %collective-permute-start.13 = (bf16[2048,256]{1,0:T(8,128)(2,1)}, bf16[2048,256]{1,0:T(8,128)(2,1)S(1)}, u32[]{:S(2)}, u32[]{:S(2)}) collective-permute-start(bf16[2048,256]{1,0:T(8,128)(2,1)} %collective-permute-done.12.refs_9_), channel_id=1, source_target_pairs={{0,1},{1,0},{2,3},{3,2},{4,5},{5,4},{6,7},{7,6},{8,9},{9,8},{10,11... | collective-permute-start | bytes 3145736 | tf_op jit(solution)/shard_map/ppermute | solution.py:22
  65.3 1.9 %collective-permute-done.13.refs_11_ = bf16[2048,256]{1,0:T(8,128)(2,1)S(1)} collective-permute-done((bf16[2048,256]{1,0:T(8,128)(2,1)}, bf16[2048,256]{1,0:T(8,128)(2,1)S(1)}, u32[]{:S(2)}, u32[]{:S(2)}) %collective-permute-start.13) | collective-permute-done | bytes 1048608 | tf_op jit(solution)/shard_map/ppermute | solution.py:22
  68.2 6.6 %second_hidden.1 = (bf16[384,512]{1,0:T(8,128)(2,1)}, bf16[48,1024]{1,0:T(8,128)(2,1)}, bf16[48,1024]{1,0:T(8,128)(2,1)}, bf16[48,1024]{1,0:T(8,128)(2,1)}, bf16[48,1024]{1,0:T(8,128)(2,1)}) custom-call(s32[2]{0:T(128)} %compare_select_fusion.2.place_ref, bf16[384,512]{1,0:T(8,128)(2,1)} %first_hidden.1.first_ref.refs_0_, ...), custom_call_target="tpu_custom_call" | custom-call | flops 1048576 | bytes 1048576 | tf_op jit(solution)/shard_map/second_hidden/pallas_call | solution.py:254
  76.6 2.4 %collective-permute-start.21 = (bf16[48,1024]{1,0:T(8,128)(2,1)}, bf16[48,1024]{1,0:T(8,128)(2,1)S(1)}, u32[]{:S(2)}, u32[]{:S(2)}) collective-permute-start(bf16[48,1024]{1,0:T(8,128)(2,1)} %get-tuple-element.51), channel_id=1, source_target_pairs={{0,16},{4,20},{8,24},{12,28},{16,0},{20,4},{24,8},{28,12},{1,17},{... | collective-permute-start | bytes 294920 | tf_op jit(solution)/shard_map/ppermute | solution.py:22
  84.8 2.1 %collective-permute-done.22 = bf16[48,1024]{1,0:T(8,128)(2,1)S(1)} collective-permute-done((bf16[48,1024]{1,0:T(8,128)(2,1)}, bf16[48,1024]{1,0:T(8,128)(2,1)S(1)}, u32[]{:S(2)}, u32[]{:S(2)}) %collective-permute-start.22) | collective-permute-done | bytes 98336 | tf_op jit(solution)/shard_map/ppermute | solution.py:22
  87.0 3.4 %collective-permute-start.24 = (bf16[48,1024]{1,0:T(8,128)(2,1)}, bf16[48,1024]{1,0:T(8,128)(2,1)S(1)}, u32[]{:S(2)}, u32[]{:S(2)}) collective-permute-start(bf16[48,1024]{1,0:T(8,128)(2,1)} %get-tuple-element.54), channel_id=1, source_target_pairs={{0,28},{4,24},{8,20},{12,16},{16,12},{20,8},{24,4},{28,0},{1,29},{... | collective-permute-start | bytes 294920 | tf_op jit(solution)/shard_map/ppermute | solution.py:22
  90.4 4.1 %collective-permute-done.23 = bf16[48,1024]{1,0:T(8,128)(2,1)S(1)} collective-permute-done((bf16[48,1024]{1,0:T(8,128)(2,1)}, bf16[48,1024]{1,0:T(8,128)(2,1)S(1)}, u32[]{:S(2)}, u32[]{:S(2)}) %collective-permute-start.23) | collective-permute-done | bytes 98336 | tf_op jit(solution)/shard_map/ppermute | solution.py:22
  95.3 7.2 %mixer_front.1 = (bf16[384,512]{1,0:T(8,128)(2,1)}, f32[384,512]{1,0:T(8,128)}, bf16[2,512]{1,0:T(2,128)(2,1)}) custom-call(s32[2]{0:T(128)} %compare_select_fusion.2.place_ref, bf16[96,2048]{1,0:T(8,128)(2,1)} %fusion.5.refs_0_, bf16[96,2048]{1,0:T(8,128)(2,1)} %collective-permute-done.14.refs_1_, bf16[96,2048]{1,0:T(8,128)(2,1)} %collective-permute-done.15.refs_2_, ...), custom_call_target="tpu_custom_call" | custom-call | flops 2415919104 | bytes 8388608 | tf_op jit(solution)/shard_map/mixer_front/pallas_call | solution.py:358
  102.4 2.3 %collective-permute-start.17 = (bf16[2,512]{1,0:T(2,128)(2,1)}, bf16[2,512]{1,0:T(2,128)(2,1)S(1)}, u32[]{:S(2)}, u32[]{:S(2)}) collective-permute-start(bf16[2,512]{1,0:T(2,128)(2,1)} %get-tuple-element.49), channel_id=1, source_target_pairs={{0,4},{4,8},{8,12},{12,16},{16,20},{20,24},{24,28},{1,5},{5,9},{9,... | collective-permute-start | bytes 6152 | tf_op jit(solution)/shard_map/ppermute | solution.py:491
  104.8 3.1 %collective-permute-done.17 = bf16[2,512]{1,0:T(2,128)(2,1)S(1)} collective-permute-done((bf16[2,512]{1,0:T(2,128)(2,1)}, bf16[2,512]{1,0:T(2,128)(2,1)S(1)}, u32[]{:S(2)}, u32[]{:S(2)}) %collective-permute-start.17) | collective-permute-done | bytes 2080 | tf_op jit(solution)/shard_map/ppermute | solution.py:491
  109.1 1.6 %fusion.8 = bf16[384,512]{1,0:T(8,128)(2,1)S(1)} fusion(f32[384,512]{1,0:T(8,128)} %get-tuple-element.48, f32[386,512]{1,0:T(8,128)S(1)} %maximum_convert_fusion, f32[512]{0:T(512)S(1)} %bitcast.75, f32[512]{0:T(512)S(1)} %bitcast.74, f32[512]{0:T(512)S(1)} %bitcast.73), kind=kLoop, calls=%fused_computation.19 | loop fusion | flops 1376256 | bytes 3545088 | tf_op jit(solution)/shard_map/convert_element_type | solution.py:496
  110.6 1.8 %collective-permute-start.18 = (bf16[384,512]{1,0:T(8,128)(2,1)S(1)}, bf16[384,512]{1,0:T(8,128)(2,1)S(1)}, u32[]{:S(2)}, u32[]{:S(2)}) collective-permute-start(bf16[384,512]{1,0:T(8,128)(2,1)S(1)} %fusion.8), channel_id=1, source_target_pairs={{0,1},{1,0},{2,3},{3,2},{4,5},{5,4},{6,7},{7,6},{8,9},{9,8},{10,11... | collective-permute-start | bytes 1179656 | tf_op jit(solution)/shard_map/ppermute | solution.py:22
  113.2 3.1 %late_down.1 = (bf16[96,1024]{1,0:T(8,128)(2,1)}, bf16[96,1024]{1,0:T(8,128)(2,1)}, bf16[96,1024]{1,0:T(8,128)(2,1)}, bf16[96,1024]{1,0:T(8,128)(2,1)}, bf16[48,...) custom-call(s32[2]{0:T(128)S(1)} %copy-done.5, ...), custom_call_target="tpu_custom_call" | custom-call | flops 1207959552 | bytes 4194304 | tf_op jit(solution)/shard_map/late_down/pallas_call | solution.py:306
  117.2 1.9 %collective-permute-start.29 = (bf16[96,1024]{1,0:T(8,128)(2,1)}, bf16[96,1024]{1,0:T(8,128)(2,1)S(1)}, u32[]{:S(2)}, u32[]{:S(2)}) collective-permute-start(bf16[96,1024]{1,0:T(8,128)(2,1)} %get-tuple-element.61), channel_id=1, source_target_pairs={{0,12},{4,8},{8,4},{12,0},{16,28},{20,24},{24,20},{28,16},{1,13},{... | collective-permute-start | bytes 589832 | tf_op jit(solution)/shard_map/ppermute | solution.py:22
  119.1 2.1 %collective-permute-start.30 = (bf16[48,1024]{1,0:T(8,128)(2,1)}, bf16[48,1024]{1,0:T(8,128)(2,1)S(1)}, u32[]{:S(2)}, u32[]{:S(2)}) collective-permute-start(bf16[48,1024]{1,0:T(8,128)(2,1)} %get-tuple-element.62), channel_id=1, source_target_pairs={{0,16},{4,20},{8,24},{12,28},{16,0},{20,4},{24,8},{28,12},{1,17},{... | collective-permute-start | bytes 294920 | tf_op jit(solution)/shard_map/ppermute | solution.py:22
  121.2 1.8 %collective-permute-done.19 = bf16[384,512]{1,0:T(8,128)(2,1)S(1)} collective-permute-done((bf16[384,512]{1,0:T(8,128)(2,1)S(1)}, bf16[384,512]{1,0:T(8,128)(2,1)S(1)}, u32[]{:S(2)}, u32[]{:S(2)}) %collective-permute-start.19) | collective-permute-done | bytes 393248 | tf_op jit(solution)/shard_map/ppermute | solution.py:22
  129.0 2.3 %collective-permute-done.30 = bf16[48,1024]{1,0:T(8,128)(2,1)S(1)} collective-permute-done((bf16[48,1024]{1,0:T(8,128)(2,1)}, bf16[48,1024]{1,0:T(8,128)(2,1)S(1)}, u32[]{:S(2)}, u32[]{:S(2)}) %collective-permute-start.30) | collective-permute-done | bytes 98336 | tf_op jit(solution)/shard_map/ppermute | solution.py:22
  131.3 3.8 %collective-permute-done.31 = bf16[48,1024]{1,0:T(8,128)(2,1)S(1)} collective-permute-done((bf16[48,1024]{1,0:T(8,128)(2,1)S(1)}, bf16[48,1024]{1,0:T(8,128)(2,1)S(1)}, u32[]{:S(2)}, u32[]{:S(2)}) %collective-permute-start.31) | collective-permute-done | bytes 98336 | tf_op jit(solution)/shard_map/ppermute | solution.py:22
  135.1 4.9 %collective-permute-done.32 = bf16[48,1024]{1,0:T(8,128)(2,1)S(1)} collective-permute-done((bf16[48,1024]{1,0:T(8,128)(2,1)S(1)}, bf16[48,1024]{1,0:T(8,128)(2,1)S(1)}, u32[]{:S(2)}, u32[]{:S(2)}) %collective-permute-start.32) | collective-permute-done | bytes 98336 | tf_op jit(solution)/shard_map/ppermute | solution.py:22
  140.1 2.7 %collective-permute-done.33 = bf16[48,1024]{1,0:T(8,128)(2,1)S(1)} collective-permute-done((bf16[48,1024]{1,0:T(8,128)(2,1)S(1)}, bf16[48,1024]{1,0:T(8,128)(2,1)S(1)}, u32[]{:S(2)}, u32[]{:S(2)}) %collective-permute-start.33) | collective-permute-done | bytes 98336 | tf_op jit(solution)/shard_map/ppermute | solution.py:22
  (146 shorter events, 37.0 us)
Async XLA Ops:
  0.6 24.4 %collective-permute-start = (bf16[2048,256]{1,0:T(8,128)(2,1)}, bf16[2048,256]{1,0:T(8,128)(2,1)}, u32[]{:S(2)}, u32[]{:S(2)}) collective-permute-start(bf16[2048,256]{1,0:T(8,128)(2,1)} %bitcast.67), channel_id=1, source_target_pairs={{0,2},{1,3},{2,0},{3,1},{4,6},{5,7},{6,4},{7,5},{8,10},{9,11},{10,... | collective-permute-start | bytes 3145736 | tf_op jit(solution)/shard_map/ppermute | solution.py:22
  1.9 37.0 %collective-permute-start.2 = (bf16[2048,256]{1,0:T(8,128)(2,1)}, bf16[2048,256]{1,0:T(8,128)(2,1)}, u32[]{:S(2)}, u32[]{:S(2)}) collective-permute-start(bf16[2048,256]{1,0:T(8,128)(2,1)} %bitcast.68), channel_id=1, source_target_pairs={{0,1},{1,0},{2,3},{3,2},{4,5},{5,4},{6,7},{7,6},{8,9},{9,8},{10,11... | collective-permute-start | bytes 3145736 | tf_op jit(solution)/shard_map/ppermute | solution.py:22
  2.9 34.8 %collective-permute-start.4 = (bf16[1024,512]{1,0:T(8,128)(2,1)}, bf16[1024,512]{1,0:T(8,128)(2,1)S(1)}, u32[]{:S(2)}, u32[]{:S(2)}) collective-permute-start(bf16[1024,512]{1,0:T(8,128)(2,1)} %bitcast.64), channel_id=1, source_target_pairs={{0,1},{1,0},{2,3},{3,2},{4,5},{5,4},{6,7},{7,6},{8,9},{9,8},{10,11... | collective-permute-start | bytes 3145736 | tf_op jit(solution)/shard_map/ppermute | solution.py:22
  6.9 14.8 %collective-permute-start.10 = (bf16[48,2048]{1,0:T(8,128)(2,1)}, bf16[48,2048]{1,0:T(8,128)(2,1)S(1)}, u32[]{:S(2)}, u32[]{:S(2)}) collective-permute-start(bf16[48,2048]{1,0:T(8,128)(2,1)} %get-tuple-element.41), channel_id=1, source_target_pairs={{0,24},{4,28},{8,16},{12,20},{16,8},{20,12},{24,0},{28,4},{1,25},{... | collective-permute-start | bytes 589832 | tf_op jit(solution)/shard_map/ppermute | solution.py:22
  7.2 20.6 %collective-permute-start.11 = (bf16[48,2048]{1,0:T(8,128)(2,1)}, bf16[48,2048]{1,0:T(8,128)(2,1)S(1)}, u32[]{:S(2)}, u32[]{:S(2)}) collective-permute-start(bf16[48,2048]{1,0:T(8,128)(2,1)} %get-tuple-element.42), channel_id=1, source_target_pairs={{0,28},{4,24},{8,20},{12,16},{16,12},{20,8},{24,4},{28,0},{1,29},{... | collective-permute-start | bytes 589832 | tf_op jit(solution)/shard_map/ppermute | solution.py:22
  21.7 18.4 %collective-permute-start.3 = (bf16[2048,256]{1,0:T(8,128)(2,1)}, bf16[2048,256]{1,0:T(8,128)(2,1)S(1)}, u32[]{:S(2)}, u32[]{:S(2)}) collective-permute-start(bf16[2048,256]{1,0:T(8,128)(2,1)} %bitcast.70), channel_id=1, source_target_pairs={{0,1},{1,0},{2,3},{3,2},{4,5},{5,4},{6,7},{7,6},{8,9},{9,8},{10,11... | collective-permute-start | bytes 3145736 | tf_op jit(solution)/shard_map/ppermute | solution.py:22
  25.1 15.1 %collective-permute-start.1 = (bf16[2048,256]{1,0:T(8,128)(2,1)}, bf16[2048,256]{1,0:T(8,128)(2,1)S(1)}, u32[]{:S(2)}, u32[]{:S(2)}) collective-permute-start(bf16[2048,256]{1,0:T(8,128)(2,1)} %collective-permute-done.refs_8_), channel_id=1, source_target_pairs={{0,1},{1,0},{2,3},{3,2},{4,5},{5,4},{6,7},{7,6},{8,9},{9,8},{10,11... | collective-permute-start | bytes 3145736 | tf_op jit(solution)/shard_map/ppermute | solution.py:22
  27.8 6.5 %collective-permute-start.5 = (bf16[48,2048]{1,0:T(8,128)(2,1)}, bf16[48,2048]{1,0:T(8,128)(2,1)S(1)}, u32[]{:S(2)}, u32[]{:S(2)}) collective-permute-start(bf16[48,2048]{1,0:T(8,128)(2,1)} %get-tuple-element.36), channel_id=1, source_target_pairs={{0,4},{4,0},{8,12},{12,8},{16,20},{20,16},{24,28},{28,24},{1,5},{5... | collective-permute-start | bytes 589832 | tf_op jit(solution)/shard_map/ppermute | solution.py:22
  34.3 28.3 %collective-permute-start.12 = (bf16[2048,256]{1,0:T(8,128)(2,1)}, bf16[2048,256]{1,0:T(8,128)(2,1)}, u32[]{:S(2)}, u32[]{:S(2)}) collective-permute-start(bf16[2048,256]{1,0:T(8,128)(2,1)} %bitcast.71), channel_id=1, source_target_pairs={{0,2},{1,3},{2,0},{3,1},{4,6},{5,7},{6,4},{7,5},{8,10},{9,11},{10,... | collective-permute-start | bytes 3145736 | tf_op jit(solution)/shard_map/ppermute | solution.py:22
  37.7 6.5 %collective-permute-start.6 = (bf16[48,2048]{1,0:T(8,128)(2,1)}, bf16[48,2048]{1,0:T(8,128)(2,1)S(1)}, u32[]{:S(2)}, u32[]{:S(2)}) collective-permute-start(bf16[48,2048]{1,0:T(8,128)(2,1)} %get-tuple-element.37), channel_id=1, source_target_pairs={{0,8},{4,12},{8,0},{12,4},{16,24},{20,28},{24,16},{28,20},{1,9},{5... | collective-permute-start | bytes 589832 | tf_op jit(solution)/shard_map/ppermute | solution.py:22
  39.0 12.6 %collective-permute-start.7 = (bf16[48,2048]{1,0:T(8,128)(2,1)}, bf16[48,2048]{1,0:T(8,128)(2,1)S(1)}, u32[]{:S(2)}, u32[]{:S(2)}) collective-permute-start(bf16[48,2048]{1,0:T(8,128)(2,1)} %get-tuple-element.38), channel_id=1, source_target_pairs={{0,12},{4,8},{8,4},{12,0},{16,28},{20,24},{24,20},{28,16},{1,13},{... | collective-permute-start | bytes 589832 | tf_op jit(solution)/shard_map/ppermute | solution.py:22
  40.1 11.5 %collective-permute-start.8 = (bf16[48,2048]{1,0:T(8,128)(2,1)}, bf16[48,2048]{1,0:T(8,128)(2,1)S(1)}, u32[]{:S(2)}, u32[]{:S(2)}) collective-permute-start(bf16[48,2048]{1,0:T(8,128)(2,1)} %get-tuple-element.39), channel_id=1, source_target_pairs={{0,16},{4,20},{8,24},{12,28},{16,0},{20,4},{24,8},{28,12},{1,17},{... | collective-permute-start | bytes 589832 | tf_op jit(solution)/shard_map/ppermute | solution.py:22
  40.2 16.6 %collective-permute-start.9 = (bf16[48,2048]{1,0:T(8,128)(2,1)}, bf16[48,2048]{1,0:T(8,128)(2,1)S(1)}, u32[]{:S(2)}, u32[]{:S(2)}) collective-permute-start(bf16[48,2048]{1,0:T(8,128)(2,1)} %get-tuple-element.40), channel_id=1, source_target_pairs={{0,20},{4,16},{8,28},{12,24},{16,4},{20,0},{24,12},{28,8},{1,21},{... | collective-permute-start | bytes 589832 | tf_op jit(solution)/shard_map/ppermute | solution.py:22
  64.7 10.9 %collective-permute-start.15 = (bf16[96,2048]{1,0:T(8,128)(2,1)}, bf16[96,2048]{1,0:T(8,128)(2,1)}, u32[]{:S(2)}, u32[]{:S(2)}) collective-permute-start(bf16[96,2048]{1,0:T(8,128)(2,1)} %fusion.5.refs_0_), channel_id=1, source_target_pairs={{0,2},{1,3},{2,0},{3,1},{4,6},{5,7},{6,4},{7,5},{8,10},{9,11},{10,... | collective-permute-start | bytes 1179656 | tf_op jit(solution)/shard_map/ppermute | solution.py:22
  65.0 16.4 %collective-permute-start.14 = (bf16[96,2048]{1,0:T(8,128)(2,1)}, bf16[96,2048]{1,0:T(8,128)(2,1)}, u32[]{:S(2)}, u32[]{:S(2)}) collective-permute-start(bf16[96,2048]{1,0:T(8,128)(2,1)} %fusion.5.refs_0_), channel_id=1, source_target_pairs={{0,1},{1,0},{2,3},{3,2},{4,5},{5,4},{6,7},{7,6},{8,9},{9,8},{10,11... | collective-permute-start | bytes 1179656 | tf_op jit(solution)/shard_map/ppermute | solution.py:22
  75.6 18.9 %collective-permute-start.16 = (bf16[96,2048]{1,0:T(8,128)(2,1)}, bf16[96,2048]{1,0:T(8,128)(2,1)S(1)}, u32[]{:S(2)}, u32[]{:S(2)}) collective-permute-start(bf16[96,2048]{1,0:T(8,128)(2,1)} %collective-permute-done.15.refs_2_), channel_id=1, source_target_pairs={{0,1},{1,0},{2,3},{3,2},{4,5},{5,4},{6,7},{7,6},{8,9},{9,8},{10,11... | collective-permute-start | bytes 1179656 | tf_op jit(solution)/shard_map/ppermute | solution.py:22
  76.6 6.9 %collective-permute-start.21 = (bf16[48,1024]{1,0:T(8,128)(2,1)}, bf16[48,1024]{1,0:T(8,128)(2,1)S(1)}, u32[]{:S(2)}, u32[]{:S(2)}) collective-permute-start(bf16[48,1024]{1,0:T(8,128)(2,1)} %get-tuple-element.51), channel_id=1, source_target_pairs={{0,16},{4,20},{8,24},{12,28},{16,0},{20,4},{24,8},{28,12},{1,17},{... | collective-permute-start | bytes 294920 | tf_op jit(solution)/shard_map/ppermute | solution.py:22
  79.9 33.3 %collective-permute-start.25 = (bf16[384,512]{1,0:T(8,128)(2,1)S(1)}, bf16[384,512]{1,0:T(8,128)(2,1)S(1)}, u32[]{:S(2)}, u32[]{:S(2)}) collective-permute-start(bf16[384,512]{1,0:T(8,128)(2,1)S(1)} %copy-done.1), channel_id=1, source_target_pairs={{0,2},{1,3},{2,0},{3,1},{4,6},{5,7},{6,4},{7,5},{8,10},{9,11},{10,... | collective-permute-start | bytes 1179656 | tf_op jit(solution)/shard_map/ppermute | solution.py:22
  80.2 33.0 %collective-permute-start.26 = (bf16[384,512]{1,0:T(8,128)(2,1)}, bf16[384,512]{1,0:T(8,128)(2,1)S(1)}, u32[]{:S(2)}, u32[]{:S(2)}) collective-permute-start(bf16[384,512]{1,0:T(8,128)(2,1)} %get-tuple-element.44.refs_1_), channel_id=1, source_target_pairs={{0,2},{1,3},{2,0},{3,1},{4,6},{5,7},{6,4},{7,5},{8,10},{9,11},{10,... | collective-permute-start | bytes 1179656 | tf_op jit(solution)/shard_map/ppermute | solution.py:22
  81.4 5.6 %collective-permute-start.22 = (bf16[48,1024]{1,0:T(8,128)(2,1)}, bf16[48,1024]{1,0:T(8,128)(2,1)S(1)}, u32[]{:S(2)}, u32[]{:S(2)}) collective-permute-start(bf16[48,1024]{1,0:T(8,128)(2,1)} %get-tuple-element.52), channel_id=1, source_target_pairs={{0,20},{4,16},{8,28},{12,24},{16,4},{20,0},{24,12},{28,8},{1,21},{... | collective-permute-start | bytes 294920 | tf_op jit(solution)/shard_map/ppermute | solution.py:22
  83.4 11.1 %collective-permute-start.23 = (bf16[48,1024]{1,0:T(8,128)(2,1)}, bf16[48,1024]{1,0:T(8,128)(2,1)S(1)}, u32[]{:S(2)}, u32[]{:S(2)}) collective-permute-start(bf16[48,1024]{1,0:T(8,128)(2,1)} %get-tuple-element.53), channel_id=1, source_target_pairs={{0,24},{4,28},{8,16},{12,20},{16,8},{20,12},{24,0},{28,4},{1,25},{... | collective-permute-start | bytes 294920 | tf_op jit(solution)/shard_map/ppermute | solution.py:22
  87.0 17.8 %collective-permute-start.24 = (bf16[48,1024]{1,0:T(8,128)(2,1)}, bf16[48,1024]{1,0:T(8,128)(2,1)S(1)}, u32[]{:S(2)}, u32[]{:S(2)}) collective-permute-start(bf16[48,1024]{1,0:T(8,128)(2,1)} %get-tuple-element.54), channel_id=1, source_target_pairs={{0,28},{4,24},{8,20},{12,16},{16,12},{20,8},{24,4},{28,0},{1,29},{... | collective-permute-start | bytes 294920 | tf_op jit(solution)/shard_map/ppermute | solution.py:22
  102.4 5.4 %collective-permute-start.17 = (bf16[2,512]{1,0:T(2,128)(2,1)}, bf16[2,512]{1,0:T(2,128)(2,1)S(1)}, u32[]{:S(2)}, u32[]{:S(2)}) collective-permute-start(bf16[2,512]{1,0:T(2,128)(2,1)} %get-tuple-element.49), channel_id=1, source_target_pairs={{0,4},{4,8},{8,12},{12,16},{16,20},{20,24},{24,28},{1,5},{5,9},{9,... | collective-permute-start | bytes 6152 | tf_op jit(solution)/shard_map/ppermute | solution.py:491
  110.6 8.4 %collective-permute-start.18 = (bf16[384,512]{1,0:T(8,128)(2,1)S(1)}, bf16[384,512]{1,0:T(8,128)(2,1)S(1)}, u32[]{:S(2)}, u32[]{:S(2)}) collective-permute-start(bf16[384,512]{1,0:T(8,128)(2,1)S(1)} %fusion.8), channel_id=1, source_target_pairs={{0,1},{1,0},{2,3},{3,2},{4,5},{5,4},{6,7},{7,6},{8,9},{9,8},{10,11... | collective-permute-start | bytes 1179656 | tf_op jit(solution)/shard_map/ppermute | solution.py:22
  112.4 10.6 %collective-permute-start.19 = (bf16[384,512]{1,0:T(8,128)(2,1)S(1)}, bf16[384,512]{1,0:T(8,128)(2,1)S(1)}, u32[]{:S(2)}, u32[]{:S(2)}) collective-permute-start(bf16[384,512]{1,0:T(8,128)(2,1)S(1)} %fusion.8), channel_id=1, source_target_pairs={{0,2},{1,3},{2,0},{3,1},{4,6},{5,7},{6,4},{7,5},{8,10},{9,11},{10,... | collective-permute-start | bytes 1179656 | tf_op jit(solution)/shard_map/ppermute | solution.py:22
  116.4 10.7 %collective-permute-start.27 = (bf16[96,1024]{1,0:T(8,128)(2,1)}, bf16[96,1024]{1,0:T(8,128)(2,1)S(1)}, u32[]{:S(2)}, u32[]{:S(2)}) collective-permute-start(bf16[96,1024]{1,0:T(8,128)(2,1)} %get-tuple-element.59), channel_id=1, source_target_pairs={{0,4},{4,0},{8,12},{12,8},{16,20},{20,16},{24,28},{28,24},{1,5},{5... | collective-permute-start | bytes 589832 | tf_op jit(solution)/shard_map/ppermute | solution.py:22
  116.4 11.8 %collective-permute-start.28 = (bf16[96,1024]{1,0:T(8,128)(2,1)}, bf16[96,1024]{1,0:T(8,128)(2,1)S(1)}, u32[]{:S(2)}, u32[]{:S(2)}) collective-permute-start(bf16[96,1024]{1,0:T(8,128)(2,1)} %get-tuple-element.60), channel_id=1, source_target_pairs={{0,8},{4,12},{8,0},{12,4},{16,24},{20,28},{24,16},{28,20},{1,9},{5... | collective-permute-start | bytes 589832 | tf_op jit(solution)/shard_map/ppermute | solution.py:22
  117.2 11.8 %collective-permute-start.29 = (bf16[96,1024]{1,0:T(8,128)(2,1)}, bf16[96,1024]{1,0:T(8,128)(2,1)S(1)}, u32[]{:S(2)}, u32[]{:S(2)}) collective-permute-start(bf16[96,1024]{1,0:T(8,128)(2,1)} %get-tuple-element.61), channel_id=1, source_target_pairs={{0,12},{4,8},{8,4},{12,0},{16,28},{20,24},{24,20},{28,16},{1,13},{... | collective-permute-start | bytes 589832 | tf_op jit(solution)/shard_map/ppermute | solution.py:22
  119.1 12.2 %collective-permute-start.30 = (bf16[48,1024]{1,0:T(8,128)(2,1)}, bf16[48,1024]{1,0:T(8,128)(2,1)S(1)}, u32[]{:S(2)}, u32[]{:S(2)}) collective-permute-start(bf16[48,1024]{1,0:T(8,128)(2,1)} %get-tuple-element.62), channel_id=1, source_target_pairs={{0,16},{4,20},{8,24},{12,28},{16,0},{20,4},{24,8},{28,12},{1,17},{... | collective-permute-start | bytes 294920 | tf_op jit(solution)/shard_map/ppermute | solution.py:22
  125.3 9.8 %collective-permute-start.31 = (bf16[48,1024]{1,0:T(8,128)(2,1)S(1)}, bf16[48,1024]{1,0:T(8,128)(2,1)S(1)}, u32[]{:S(2)}, u32[]{:S(2)}) collective-permute-start(bf16[48,1024]{1,0:T(8,128)(2,1)S(1)} %copy-done.26), channel_id=1, source_target_pairs={{0,20},{4,16},{8,28},{12,24},{16,4},{20,0},{24,12},{28,8},{1,21},{... | collective-permute-start | bytes 294920 | tf_op jit(solution)/shard_map/ppermute | solution.py:22
  127.1 13.0 %collective-permute-start.32 = (bf16[48,1024]{1,0:T(8,128)(2,1)S(1)}, bf16[48,1024]{1,0:T(8,128)(2,1)S(1)}, u32[]{:S(2)}, u32[]{:S(2)}) collective-permute-start(bf16[48,1024]{1,0:T(8,128)(2,1)S(1)} %copy-done.25), channel_id=1, source_target_pairs={{0,24},{4,28},{8,16},{12,20},{16,8},{20,12},{24,0},{28,4},{1,25},{... | collective-permute-start | bytes 294920 | tf_op jit(solution)/shard_map/ppermute | solution.py:22
  128.3 14.5 %collective-permute-start.33 = (bf16[48,1024]{1,0:T(8,128)(2,1)S(1)}, bf16[48,1024]{1,0:T(8,128)(2,1)S(1)}, u32[]{:S(2)}, u32[]{:S(2)}) collective-permute-start(bf16[48,1024]{1,0:T(8,128)(2,1)S(1)} %copy-done.24), channel_id=1, source_target_pairs={{0,28},{4,24},{8,20},{12,16},{16,12},{20,8},{24,4},{28,0},{1,29},{... | collective-permute-start | bytes 294920 | tf_op jit(solution)/shard_map/ppermute | solution.py:22
  (30 other events, 391.8 us)

commit v5 on v4

--- a/solution.py
+++ b/solution.py
@@ -118,7 +118,8 @@
     width = rows.shape[1]
     return pl.pallas_call(
         functools.partial(dispatch_kernel, direct, slot_cap),
-        out_shape=[jax.ShapeDtypeStruct((size, width), jnp.bfloat16) for size in sizes],
+        out_shape=[pltpu.HBM((sizes[0], width), jnp.bfloat16)]
+        + [pltpu.VMEM((size, width), jnp.bfloat16) for size in sizes[1:]],
         in_specs=[SMEM, VMEM, ANY, VMEM],
         out_specs=[VMEM] * len(sizes),
         scratch_shapes=[pltpu.VMEM(rows.shape, rows.dtype), pltpu.SemaphoreType.DMA],
@@ -198,7 +199,7 @@
     width = weights[0].shape[1] * len(weights) // 2
     return pl.pallas_call(
         functools.partial(first_kernel, len(row_parts)),
-        out_shape=jax.ShapeDtypeStruct((rows, width), jnp.bfloat16),
+        out_shape=pltpu.VMEM((rows, width), jnp.bfloat16),
         in_specs=[ANY] * (len(row_parts) + len(weights)),
         out_specs=VMEM,
         scratch_shapes=hidden_scratch(row_parts, weights),
@@ -249,8 +250,8 @@
     rows = sum(sizes)
     width = weights[0].shape[1] * len(weights) // 2
     out_width = 2 * downs[0].shape[1]
-    outs = [jax.ShapeDtypeStruct((rows, width), jnp.bfloat16)]
-    outs += [jax.ShapeDtypeStruct((sizes[k], out_width), jnp.bfloat16) for k in early]
+    outs = [pltpu.VMEM((rows, width), jnp.bfloat16)]
+    outs += [pltpu.VMEM((sizes[k], out_width), jnp.bfloat16) for k in early]
     hidden, *results = pl.pallas_call(
         functools.partial(second_kernel, len(row_parts), len(weights), sum(sizes[: early[0]])),
         out_shape=outs,
@@ -358,9 +359,9 @@
     return pl.pallas_call(
         front_kernel,
         out_shape=[
-            jax.ShapeDtypeStruct((rows, width), jnp.bfloat16),
-            jax.ShapeDtypeStruct((rows, width), jnp.float32),
-            jax.ShapeDtypeStruct((rim, width), jnp.bfloat16),
+            pltpu.VMEM((rows, width), jnp.bfloat16),
+            pltpu.VMEM((rows, width), jnp.float32),
+            pltpu.VMEM((rim, width), jnp.bfloat16),
         ],
         in_specs=[SMEM] + [ANY] * 7,
         out_specs=[VMEM, VMEM, VMEM],

time: 148 us -> 142 us (0.959)
  the two profiles are of different devices: /device:TPU:17 before, /device:TPU:0 now
where the time goes in v5:
time: 142 us; the launch traced here: 141 us
  waiting for transfers between devices  51.2 us (36%)
  starting transfers between devices  47.7 us (34%)
  Pallas kernels  22.8 us (16%)
  other arithmetic  7.2 us (5%)
  local copies, waits for them, and re-layouts  6.41 us (5%)
  matrix products  3.99 us (3%)
    ppermute x34, waiting for transfers between devices, swapped(): lax.ppermute(value, axis, [(source, source ^ mask) for source in range(co...  50.1 us
    ppermute x34, starting transfers between devices, swapped(): lax.ppermute(value, axis, [(source, source ^ mask) for source in range(co...  45.1 us
    pallas_call x1, Pallas kernels, mixer_front(): pl.pallas_call(front_kernel, out_shape=[pltpu.VMEM((rows, width), jnp.bfl...  6.25 us
    pallas_call x1, Pallas kernels, second_hidden(): pl.pallas_call(functools.partial(second_kernel, len(row_parts), len(weigh...  5.85 us
    unnamed x66, local copies, waits for them, and re-layouts  4.43 us
    pallas_call x1, Pallas kernels, first_hidden(): pl.pallas_call(functools.partial(first_kernel, len(row_parts)), out_shape...  4.37 us
    pallas_call x1, Pallas kernels, dispatched(): pl.pallas_call(functools.partial(dispatch_kernel, direct, slot_cap), out_...  3.16 us
    pallas_call x1, Pallas kernels, late_results(): pl.pallas_call(functools.partial(late_kernel, far, tuple(sizes), tuple(ea...  3.13 us
  transfers between devices with their start and end apart: 35, of which 16 were waited for; matrix products, arithmetic and copies ran while one was open for 9% of the time, Pallas kernels for 16%

profile of v5, /device:TPU:0, one launch (start us, length us, event | category | flops | bytes accessed | tf_op | source)
XLA Modules:
  0.0 140.5 jit_solution(5907202354705901841)
XLA Ops:
  0.6 3.0 %collective-permute-start = (bf16[2048,256]{1,0:T(8,128)(2,1)}, bf16[2048,256]{1,0:T(8,128)(2,1)}, u32[]{:S(2)}, u32[]{:S(2)}) collective-permute-start(bf16[2048,256]{1,0:T(8,128)(2,1)} %bitcast.67), channel_id=1, source_target_pairs={{0,2},{1,3},{2,0},{3,1},{4,6},{5,7},{6,4},{7,5},{8,10},{9,11},{10,... | collective-permute-start | bytes 3145736 | tf_op jit(solution)/shard_map/ppermute | solution.py:22
  4.7 3.2 %dispatch.1 = (bf16[48,2048]{1,0:T(8,128)(2,1)}, bf16[48,2048]{1,0:T(8,128)(2,1)S(1)}, bf16[48,2048]{1,0:T(8,128)(2,1)S(1)}, bf16[48,2048]{1,0:T(8,128)(2,1)S(1)...) custom-call(s32[2]{0:T(128)} %compare_select_fusion.2.place_ref, ...), custom_call_target="tpu_custom_call" | custom-call | flops 150994944 | bytes 2097152 | tf_op jit(solution)/shard_map/dispatch/pallas_call | solution.py:119
  10.0 3.6 %collective-permute-start.10 = (bf16[48,2048]{1,0:T(8,128)(2,1)}, bf16[48,2048]{1,0:T(8,128)(2,1)}, u32[]{:S(2)}, u32[]{:S(2)}) collective-permute-start(bf16[48,2048]{1,0:T(8,128)(2,1)} %get-tuple-element.41), channel_id=1, source_target_pairs={{0,24},{4,28},{8,16},{12,20},{16,8},{20,12},{24,0},{28,4},{1,25},{... | collective-permute-start | bytes 589832 | tf_op jit(solution)/shard_map/ppermute | solution.py:22
  17.3 1.9 %collective-permute-done.10.refs_6_ = bf16[48,2048]{1,0:T(8,128)(2,1)} collective-permute-done((bf16[48,2048]{1,0:T(8,128)(2,1)}, bf16[48,2048]{1,0:T(8,128)(2,1)}, u32[]{:S(2)}, u32[]{:S(2)}) %collective-permute-start.10) | collective-permute-done | bytes 196640 | tf_op jit(solution)/shard_map/ppermute | solution.py:22
  19.2 7.9 %collective-permute-done.refs_8_ = bf16[2048,256]{1,0:T(8,128)(2,1)} collective-permute-done((bf16[2048,256]{1,0:T(8,128)(2,1)}, bf16[2048,256]{1,0:T(8,128)(2,1)}, u32[]{:S(2)}, u32[]{:S(2)}) %collective-permute-start) | collective-permute-done | bytes 1048608 | tf_op jit(solution)/shard_map/ppermute | solution.py:22
  28.3 1.8 %collective-permute-start.5 = (bf16[48,2048]{1,0:T(8,128)(2,1)}, bf16[48,2048]{1,0:T(8,128)(2,1)S(1)}, u32[]{:S(2)}, u32[]{:S(2)}) collective-permute-start(bf16[48,2048]{1,0:T(8,128)(2,1)} %copy-done.9), channel_id=1, source_target_pairs={{0,4},{4,0},{8,12},{12,8},{16,20},{20,16},{24,28},{28,24},{1,5},{5... | collective-permute-start | bytes 589832 | tf_op jit(solution)/shard_map/ppermute | solution.py:22
  30.3 5.7 %collective-permute-done.5.refs_1_ = bf16[48,2048]{1,0:T(8,128)(2,1)S(1)} collective-permute-done((bf16[48,2048]{1,0:T(8,128)(2,1)}, bf16[48,2048]{1,0:T(8,128)(2,1)S(1)}, u32[]{:S(2)}, u32[]{:S(2)}) %collective-permute-start.5) | collective-permute-done | bytes 196640 | tf_op jit(solution)/shard_map/ppermute | solution.py:22
  36.0 1.7 %collective-permute-start.12 = (bf16[2048,256]{1,0:T(8,128)(2,1)}, bf16[2048,256]{1,0:T(8,128)(2,1)}, u32[]{:S(2)}, u32[]{:S(2)}) collective-permute-start(bf16[2048,256]{1,0:T(8,128)(2,1)} %bitcast.71), channel_id=1, source_target_pairs={{0,2},{1,3},{2,0},{3,1},{4,6},{5,7},{6,4},{7,5},{8,10},{9,11},{10,... | collective-permute-start | bytes 3145736 | tf_op jit(solution)/shard_map/ppermute | solution.py:22
  37.7 1.9 %fusion.5.refs_0_ = bf16[96,2048]{1,0:T(8,128)(2,1)} fusion(bf16[96,2048]{1,0:T(8,128)(2,1)} %param.14, f32[2048]{0:T(1024)} %param.16, f32[96]{0:T(128)S(1)} %add_rsqrt_fusion), kind=kLoop, calls=%fused_computation.15 | loop fusion | flops 786432 | bytes 795008 | tf_op jit(solution)/shard_map/convert_element_type | solution.py:17
  39.6 1.6 %collective-permute-start.6 = (bf16[48,2048]{1,0:T(8,128)(2,1)}, bf16[48,2048]{1,0:T(8,128)(2,1)S(1)}, u32[]{:S(2)}, u32[]{:S(2)}) collective-permute-start(bf16[48,2048]{1,0:T(8,128)(2,1)} %copy-done.8), channel_id=1, source_target_pairs={{0,8},{4,12},{8,0},{12,4},{16,24},{20,28},{24,16},{28,20},{1,9},{5... | collective-permute-start | bytes 589832 | tf_op jit(solution)/shard_map/ppermute | solution.py:22
  42.6 2.6 %collective-permute-start.8 = (bf16[48,2048]{1,0:T(8,128)(2,1)S(1)}, bf16[48,2048]{1,0:T(8,128)(2,1)S(1)}, u32[]{:S(2)}, u32[]{:S(2)}) collective-permute-start(bf16[48,2048]{1,0:T(8,128)(2,1)S(1)} %get-tuple-element.39), channel_id=1, source_target_pairs={{0,16},{4,20},{8,24},{12,28},{16,0},{20,4},{24,8},{28,12},{1,17},{... | collective-permute-start | bytes 589832 | tf_op jit(solution)/shard_map/ppermute | solution.py:22
  47.2 7.6 %collective-permute-done.6.refs_2_ = bf16[48,2048]{1,0:T(8,128)(2,1)S(1)} collective-permute-done((bf16[48,2048]{1,0:T(8,128)(2,1)}, bf16[48,2048]{1,0:T(8,128)(2,1)S(1)}, u32[]{:S(2)}, u32[]{:S(2)}) %collective-permute-start.6) | collective-permute-done | bytes 196640 | tf_op jit(solution)/shard_map/ppermute | solution.py:22
  54.8 4.7 %collective-permute-done.7.refs_3_ = bf16[48,2048]{1,0:T(8,128)(2,1)S(1)} collective-permute-done((bf16[48,2048]{1,0:T(8,128)(2,1)}, bf16[48,2048]{1,0:T(8,128)(2,1)S(1)}, u32[]{:S(2)}, u32[]{:S(2)}) %collective-permute-start.7) | collective-permute-done | bytes 196640 | tf_op jit(solution)/shard_map/ppermute | solution.py:22
  59.5 2.3 %collective-permute-done.9.refs_5_ = bf16[48,2048]{1,0:T(8,128)(2,1)S(1)} collective-permute-done((bf16[48,2048]{1,0:T(8,128)(2,1)S(1)}, bf16[48,2048]{1,0:T(8,128)(2,1)S(1)}, u32[]{:S(2)}, u32[]{:S(2)}) %collective-permute-start.9) | collective-permute-done | bytes 196640 | tf_op jit(solution)/shard_map/ppermute | solution.py:22
  62.4 4.4 %first_hidden.1.first_ref.refs_0_ = bf16[384,512]{1,0:T(8,128)(2,1)S(1)} custom-call(bf16[48,2048]{1,0:T(8,128)(2,1)} %get-tuple-element.35.refs_0_, bf16[48,2048]{1,0:T(8,128)(2,1)} %copy-done.14, bf16[48,2048]{1,0:T(8,128)(2,1)} %copy-done.15, bf16[48,2048]{1,0:T(8,128)(2,1)} %copy-done.16, bf16[48,2048]{1,0:T(8,128)(2,1)} %copy-done.17, ...), custom_call_target="tpu_custom_call" | custom-call | flops 1610612736 | bytes 5767168 | tf_op jit(solution)/shard_map/first_hidden/pallas_call | solution.py:200
  68.7 1.9 %collective-permute-done.13.refs_11_ = bf16[2048,256]{1,0:T(8,128)(2,1)} collective-permute-done((bf16[2048,256]{1,0:T(8,128)(2,1)}, bf16[2048,256]{1,0:T(8,128)(2,1)}, u32[]{:S(2)}, u32[]{:S(2)}) %collective-permute-start.13) | collective-permute-done | bytes 1048608 | tf_op jit(solution)/shard_map/ppermute | solution.py:22
  70.6 5.8 %second_hidden.1 = (bf16[384,512]{1,0:T(8,128)(2,1)S(1)}, bf16[48,1024]{1,0:T(8,128)(2,1)S(1)}, bf16[48,1024]{1,0:T(8,128)(2,1)S(1)}, bf16[48,1024]{1,0:T(8,128)(2,1)S(1)}, bf16[48,1024]{1,0:T(8,128)(2,1)S(1)}) custom-call(s32[2]{0:T(128)} %compare_select_fusion.2.place_ref, bf16[384,512]{1,0:T(8,128)(2,1)} %copy-done.1, ...), custom_call_target="tpu_custom_call" | custom-call | flops 1048576 | bytes 1048576 | tf_op jit(solution)/shard_map/second_hidden/pallas_call | solution.py:255
  76.5 3.0 %collective-permute-done.15.refs_2_ = bf16[96,2048]{1,0:T(8,128)(2,1)} collective-permute-done((bf16[96,2048]{1,0:T(8,128)(2,1)}, bf16[96,2048]{1,0:T(8,128)(2,1)}, u32[]{:S(2)}, u32[]{:S(2)}) %collective-permute-start.15) | collective-permute-done | bytes 393248 | tf_op jit(solution)/shard_map/ppermute | solution.py:22
  82.8 3.5 %collective-permute-start.22 = (bf16[48,1024]{1,0:T(8,128)(2,1)S(1)}, bf16[48,1024]{1,0:T(8,128)(2,1)S(1)}, u32[]{:S(2)}, u32[]{:S(2)}) collective-permute-start(bf16[48,1024]{1,0:T(8,128)(2,1)S(1)} %get-tuple-element.52), channel_id=1, source_target_pairs={{0,20},{4,16},{8,28},{12,24},{16,4},{20,0},{24,12},{28,8},{1,21},{... | collective-permute-start | bytes 294920 | tf_op jit(solution)/shard_map/ppermute | solution.py:22
  86.3 1.8 %collective-permute-done.21 = bf16[48,1024]{1,0:T(8,128)(2,1)S(1)} collective-permute-done((bf16[48,1024]{1,0:T(8,128)(2,1)S(1)}, bf16[48,1024]{1,0:T(8,128)(2,1)S(1)}, u32[]{:S(2)}, u32[]{:S(2)}) %collective-permute-start.21) | collective-permute-done | bytes 98336 | tf_op jit(solution)/shard_map/ppermute | solution.py:22
  88.1 1.8 %collective-permute-start.23 = (bf16[48,1024]{1,0:T(8,128)(2,1)S(1)}, bf16[48,1024]{1,0:T(8,128)(2,1)S(1)}, u32[]{:S(2)}, u32[]{:S(2)}) collective-permute-start(bf16[48,1024]{1,0:T(8,128)(2,1)S(1)} %get-tuple-element.53), channel_id=1, source_target_pairs={{0,24},{4,28},{8,16},{12,20},{16,8},{20,12},{24,0},{28,4},{1,25},{... | collective-permute-start | bytes 294920 | tf_op jit(solution)/shard_map/ppermute | solution.py:22
  89.9 4.4 %collective-permute-done.22 = bf16[48,1024]{1,0:T(8,128)(2,1)S(1)} collective-permute-done((bf16[48,1024]{1,0:T(8,128)(2,1)S(1)}, bf16[48,1024]{1,0:T(8,128)(2,1)S(1)}, u32[]{:S(2)}, u32[]{:S(2)}) %collective-permute-start.22) | collective-permute-done | bytes 98336 | tf_op jit(solution)/shard_map/ppermute | solution.py:22
  94.3 3.3 %collective-permute-start.24 = (bf16[48,1024]{1,0:T(8,128)(2,1)S(1)}, bf16[48,1024]{1,0:T(8,128)(2,1)S(1)}, u32[]{:S(2)}, u32[]{:S(2)}) collective-permute-start(bf16[48,1024]{1,0:T(8,128)(2,1)S(1)} %get-tuple-element.54), channel_id=1, source_target_pairs={{0,28},{4,24},{8,20},{12,16},{16,12},{20,8},{24,4},{28,0},{1,29},{... | collective-permute-start | bytes 294920 | tf_op jit(solution)/shard_map/ppermute | solution.py:22
  97.7 6.3 %mixer_front.1 = (bf16[384,512]{1,0:T(8,128)(2,1)S(1)}, f32[384,512]{1,0:T(8,128)S(1)}, bf16[2,512]{1,0:T(2,128)(2,1)S(1)}) custom-call(s32[2]{0:T(128)} %compare_select_fusion.2.place_ref, bf16[96,2048]{1,0:T(8,128)(2,1)} %fusion.5.refs_0_, bf16[96,2048]{1,0:T(8,128)(2,1)} %collective-permute-done.14.refs_1_, ...), custom_call_target="tpu_custom_call" | custom-call | flops 2415919104 | bytes 8388608 | tf_op jit(solution)/shard_map/mixer_front/pallas_call | solution.py:359
  104.0 2.6 %collective-permute-start.17 = (bf16[2,512]{1,0:T(2,128)(2,1)S(1)}, bf16[2,512]{1,0:T(2,128)(2,1)S(1)}, u32[]{:S(2)}, u32[]{:S(2)}) collective-permute-start(bf16[2,512]{1,0:T(2,128)(2,1)S(1)} %get-tuple-element.49), channel_id=1, source_target_pairs={{0,4},{4,8},{8,12},{12,16},{16,20},{20,24},{24,28},{1,5},{5,9},{9,... | collective-permute-start | bytes 6152 | tf_op jit(solution)/shard_map/ppermute | solution.py:492
  109.7 3.1 %late_down.1 = (bf16[96,1024]{1,0:T(8,128)(2,1)}, bf16[96,1024]{1,0:T(8,128)(2,1)}, bf16[96,1024]{1,0:T(8,128)(2,1)}, bf16[96,1024]{1,0:T(8,128)(2,1)}, bf16[48,...) custom-call(s32[2]{0:T(128)S(1)} %copy-done.6, ...), custom_call_target="tpu_custom_call" | custom-call | flops 1207959552 | bytes 4194304 | tf_op jit(solution)/shard_map/late_down/pallas_call | solution.py:307
  112.8 2.3 %collective-permute-start.27 = (bf16[96,1024]{1,0:T(8,128)(2,1)}, bf16[96,1024]{1,0:T(8,128)(2,1)S(1)}, u32[]{:S(2)}, u32[]{:S(2)}) collective-permute-start(bf16[96,1024]{1,0:T(8,128)(2,1)} %get-tuple-element.59), channel_id=1, source_target_pairs={{0,4},{4,0},{8,12},{12,8},{16,20},{20,16},{24,28},{28,24},{1,5},{5... | collective-permute-start | bytes 589832 | tf_op jit(solution)/shard_map/ppermute | solution.py:22
  117.5 1.7 %collective-permute-start.30 = (bf16[48,1024]{1,0:T(8,128)(2,1)}, bf16[48,1024]{1,0:T(8,128)(2,1)S(1)}, u32[]{:S(2)}, u32[]{:S(2)}) collective-permute-start(bf16[48,1024]{1,0:T(8,128)(2,1)} %get-tuple-element.62), channel_id=1, source_target_pairs={{0,16},{4,20},{8,24},{12,28},{16,0},{20,4},{24,8},{28,12},{1,17},{... | collective-permute-start | bytes 294920 | tf_op jit(solution)/shard_map/ppermute | solution.py:22
  121.5 2.0 %collective-permute-start.31 = (bf16[48,1024]{1,0:T(8,128)(2,1)S(1)}, bf16[48,1024]{1,0:T(8,128)(2,1)S(1)}, u32[]{:S(2)}, u32[]{:S(2)}) collective-permute-start(bf16[48,1024]{1,0:T(8,128)(2,1)S(1)} %copy-done.27), channel_id=1, source_target_pairs={{0,20},{4,16},{8,28},{12,24},{16,4},{20,0},{24,12},{28,8},{1,21},{... | collective-permute-start | bytes 294920 | tf_op jit(solution)/shard_map/ppermute | solution.py:22
  124.6 2.6 %collective-permute-start.32 = (bf16[48,1024]{1,0:T(8,128)(2,1)S(1)}, bf16[48,1024]{1,0:T(8,128)(2,1)S(1)}, u32[]{:S(2)}, u32[]{:S(2)}) collective-permute-start(bf16[48,1024]{1,0:T(8,128)(2,1)S(1)} %copy-done.26), channel_id=1, source_target_pairs={{0,24},{4,28},{8,16},{12,20},{16,8},{20,12},{24,0},{28,4},{1,25},{... | collective-permute-start | bytes 294920 | tf_op jit(solution)/shard_map/ppermute | solution.py:22
  127.2 3.2 %collective-permute-start.33 = (bf16[48,1024]{1,0:T(8,128)(2,1)S(1)}, bf16[48,1024]{1,0:T(8,128)(2,1)S(1)}, u32[]{:S(2)}, u32[]{:S(2)}) collective-permute-start(bf16[48,1024]{1,0:T(8,128)(2,1)S(1)} %copy-done.25), channel_id=1, source_target_pairs={{0,28},{4,24},{8,20},{12,16},{16,12},{20,8},{24,4},{28,0},{1,29},{... | collective-permute-start | bytes 294920 | tf_op jit(solution)/shard_map/ppermute | solution.py:22
  130.6 6.4 %collective-permute-done.31 = bf16[48,1024]{1,0:T(8,128)(2,1)S(1)} collective-permute-done((bf16[48,1024]{1,0:T(8,128)(2,1)S(1)}, bf16[48,1024]{1,0:T(8,128)(2,1)S(1)}, u32[]{:S(2)}, u32[]{:S(2)}) %collective-permute-start.31) | collective-permute-done | bytes 98336 | tf_op jit(solution)/shard_map/ppermute | solution.py:22
  (148 shorter events, 29.7 us)
Async XLA Ops:
  0.6 26.5 %collective-permute-start = (bf16[2048,256]{1,0:T(8,128)(2,1)}, bf16[2048,256]{1,0:T(8,128)(2,1)}, u32[]{:S(2)}, u32[]{:S(2)}) collective-permute-start(bf16[2048,256]{1,0:T(8,128)(2,1)} %bitcast.67), channel_id=1, source_target_pairs={{0,2},{1,3},{2,0},{3,1},{4,6},{5,7},{6,4},{7,5},{8,10},{9,11},{10,... | collective-permute-start | bytes 3145736 | tf_op jit(solution)/shard_map/ppermute | solution.py:22
  3.7 37.5 %collective-permute-start.2 = (bf16[2048,256]{1,0:T(8,128)(2,1)}, bf16[2048,256]{1,0:T(8,128)(2,1)}, u32[]{:S(2)}, u32[]{:S(2)}) collective-permute-start(bf16[2048,256]{1,0:T(8,128)(2,1)} %bitcast.68), channel_id=1, source_target_pairs={{0,1},{1,0},{2,3},{3,2},{4,5},{5,4},{6,7},{7,6},{8,9},{9,8},{10,11... | collective-permute-start | bytes 3145736 | tf_op jit(solution)/shard_map/ppermute | solution.py:22
  3.7 35.9 %collective-permute-start.4 = (bf16[1024,512]{1,0:T(8,128)(2,1)}, bf16[1024,512]{1,0:T(8,128)(2,1)S(1)}, u32[]{:S(2)}, u32[]{:S(2)}) collective-permute-start(bf16[1024,512]{1,0:T(8,128)(2,1)} %bitcast.64), channel_id=1, source_target_pairs={{0,1},{1,0},{2,3},{3,2},{4,5},{5,4},{6,7},{7,6},{8,9},{9,8},{10,11... | collective-permute-start | bytes 3145736 | tf_op jit(solution)/shard_map/ppermute | solution.py:22
  10.0 9.3 %collective-permute-start.10 = (bf16[48,2048]{1,0:T(8,128)(2,1)}, bf16[48,2048]{1,0:T(8,128)(2,1)}, u32[]{:S(2)}, u32[]{:S(2)}) collective-permute-start(bf16[48,2048]{1,0:T(8,128)(2,1)} %get-tuple-element.41), channel_id=1, source_target_pairs={{0,24},{4,28},{8,16},{12,20},{16,8},{20,12},{24,0},{28,4},{1,25},{... | collective-permute-start | bytes 589832 | tf_op jit(solution)/shard_map/ppermute | solution.py:22
  13.6 14.8 %collective-permute-start.11 = (bf16[48,2048]{1,0:T(8,128)(2,1)}, bf16[48,2048]{1,0:T(8,128)(2,1)}, u32[]{:S(2)}, u32[]{:S(2)}) collective-permute-start(bf16[48,2048]{1,0:T(8,128)(2,1)} %get-tuple-element.42), channel_id=1, source_target_pairs={{0,28},{4,24},{8,20},{12,16},{16,12},{20,8},{24,4},{28,0},{1,29},{... | collective-permute-start | bytes 589832 | tf_op jit(solution)/shard_map/ppermute | solution.py:22
  19.2 23.4 %collective-permute-start.3 = (bf16[2048,256]{1,0:T(8,128)(2,1)}, bf16[2048,256]{1,0:T(8,128)(2,1)S(1)}, u32[]{:S(2)}, u32[]{:S(2)}) collective-permute-start(bf16[2048,256]{1,0:T(8,128)(2,1)} %bitcast.70), channel_id=1, source_target_pairs={{0,1},{1,0},{2,3},{3,2},{4,5},{5,4},{6,7},{7,6},{8,9},{9,8},{10,11... | collective-permute-start | bytes 3145736 | tf_op jit(solution)/shard_map/ppermute | solution.py:22
  27.2 18.0 %collective-permute-start.1 = (bf16[2048,256]{1,0:T(8,128)(2,1)}, bf16[2048,256]{1,0:T(8,128)(2,1)S(1)}, u32[]{:S(2)}, u32[]{:S(2)}) collective-permute-start(bf16[2048,256]{1,0:T(8,128)(2,1)} %collective-permute-done.refs_8_), channel_id=1, source_target_pairs={{0,1},{1,0},{2,3},{3,2},{4,5},{5,4},{6,7},{7,6},{8,9},{9,8},{10,11... | collective-permute-start | bytes 3145736 | tf_op jit(solution)/shard_map/ppermute | solution.py:22
  28.3 7.6 %collective-permute-start.5 = (bf16[48,2048]{1,0:T(8,128)(2,1)}, bf16[48,2048]{1,0:T(8,128)(2,1)S(1)}, u32[]{:S(2)}, u32[]{:S(2)}) collective-permute-start(bf16[48,2048]{1,0:T(8,128)(2,1)} %copy-done.9), channel_id=1, source_target_pairs={{0,4},{4,0},{8,12},{12,8},{16,20},{20,16},{24,28},{28,24},{1,5},{5... | collective-permute-start | bytes 589832 | tf_op jit(solution)/shard_map/ppermute | solution.py:22
  36.0 31.6 %collective-permute-start.12 = (bf16[2048,256]{1,0:T(8,128)(2,1)}, bf16[2048,256]{1,0:T(8,128)(2,1)}, u32[]{:S(2)}, u32[]{:S(2)}) collective-permute-start(bf16[2048,256]{1,0:T(8,128)(2,1)} %bitcast.71), channel_id=1, source_target_pairs={{0,2},{1,3},{2,0},{3,1},{4,6},{5,7},{6,4},{7,5},{8,10},{9,11},{10,... | collective-permute-start | bytes 3145736 | tf_op jit(solution)/shard_map/ppermute | solution.py:22
  39.6 15.2 %collective-permute-start.6 = (bf16[48,2048]{1,0:T(8,128)(2,1)}, bf16[48,2048]{1,0:T(8,128)(2,1)S(1)}, u32[]{:S(2)}, u32[]{:S(2)}) collective-permute-start(bf16[48,2048]{1,0:T(8,128)(2,1)} %copy-done.8), channel_id=1, source_target_pairs={{0,8},{4,12},{8,0},{12,4},{16,24},{20,28},{24,16},{28,20},{1,9},{5... | collective-permute-start | bytes 589832 | tf_op jit(solution)/shard_map/ppermute | solution.py:22
  41.2 18.3 %collective-permute-start.7 = (bf16[48,2048]{1,0:T(8,128)(2,1)}, bf16[48,2048]{1,0:T(8,128)(2,1)S(1)}, u32[]{:S(2)}, u32[]{:S(2)}) collective-permute-start(bf16[48,2048]{1,0:T(8,128)(2,1)} %copy-done.7), channel_id=1, source_target_pairs={{0,12},{4,8},{8,4},{12,0},{16,28},{20,24},{24,20},{28,16},{1,13},{... | collective-permute-start | bytes 589832 | tf_op jit(solution)/shard_map/ppermute | solution.py:22
  42.6 16.9 %collective-permute-start.8 = (bf16[48,2048]{1,0:T(8,128)(2,1)S(1)}, bf16[48,2048]{1,0:T(8,128)(2,1)S(1)}, u32[]{:S(2)}, u32[]{:S(2)}) collective-permute-start(bf16[48,2048]{1,0:T(8,128)(2,1)S(1)} %get-tuple-element.39), channel_id=1, source_target_pairs={{0,16},{4,20},{8,24},{12,28},{16,0},{20,4},{24,8},{28,12},{1,17},{... | collective-permute-start | bytes 589832 | tf_op jit(solution)/shard_map/ppermute | solution.py:22
  45.2 16.6 %collective-permute-start.9 = (bf16[48,2048]{1,0:T(8,128)(2,1)S(1)}, bf16[48,2048]{1,0:T(8,128)(2,1)S(1)}, u32[]{:S(2)}, u32[]{:S(2)}) collective-permute-start(bf16[48,2048]{1,0:T(8,128)(2,1)S(1)} %get-tuple-element.40), channel_id=1, source_target_pairs={{0,20},{4,16},{8,28},{12,24},{16,4},{20,0},{24,12},{28,8},{1,21},{... | collective-permute-start | bytes 589832 | tf_op jit(solution)/shard_map/ppermute | solution.py:22
  67.6 11.8 %collective-permute-start.15 = (bf16[96,2048]{1,0:T(8,128)(2,1)}, bf16[96,2048]{1,0:T(8,128)(2,1)}, u32[]{:S(2)}, u32[]{:S(2)}) collective-permute-start(bf16[96,2048]{1,0:T(8,128)(2,1)} %fusion.5.refs_0_), channel_id=1, source_target_pairs={{0,2},{1,3},{2,0},{3,1},{4,6},{5,7},{6,4},{7,5},{8,10},{9,11},{10,... | collective-permute-start | bytes 1179656 | tf_op jit(solution)/shard_map/ppermute | solution.py:22
  68.5 14.3 %collective-permute-start.14 = (bf16[96,2048]{1,0:T(8,128)(2,1)}, bf16[96,2048]{1,0:T(8,128)(2,1)}, u32[]{:S(2)}, u32[]{:S(2)}) collective-permute-start(bf16[96,2048]{1,0:T(8,128)(2,1)} %fusion.5.refs_0_), channel_id=1, source_target_pairs={{0,1},{1,0},{2,3},{3,2},{4,5},{5,4},{6,7},{7,6},{8,9},{9,8},{10,11... | collective-permute-start | bytes 1179656 | tf_op jit(solution)/shard_map/ppermute | solution.py:22
  79.4 18.3 %collective-permute-start.16 = (bf16[96,2048]{1,0:T(8,128)(2,1)}, bf16[96,2048]{1,0:T(8,128)(2,1)}, u32[]{:S(2)}, u32[]{:S(2)}) collective-permute-start(bf16[96,2048]{1,0:T(8,128)(2,1)} %collective-permute-done.15.refs_2_), channel_id=1, source_target_pairs={{0,1},{1,0},{2,3},{3,2},{4,5},{5,4},{6,7},{7,6},{8,9},{9,8},{10,11... | collective-permute-start | bytes 1179656 | tf_op jit(solution)/shard_map/ppermute | solution.py:22
  79.4 8.7 %collective-permute-start.21 = (bf16[48,1024]{1,0:T(8,128)(2,1)S(1)}, bf16[48,1024]{1,0:T(8,128)(2,1)S(1)}, u32[]{:S(2)}, u32[]{:S(2)}) collective-permute-start(bf16[48,1024]{1,0:T(8,128)(2,1)S(1)} %get-tuple-element.51), channel_id=1, source_target_pairs={{0,16},{4,20},{8,24},{12,28},{16,0},{20,4},{24,8},{28,12},{1,17},{... | collective-permute-start | bytes 294920 | tf_op jit(solution)/shard_map/ppermute | solution.py:22
  80.7 29.0 %collective-permute-start.25 = (bf16[384,512]{1,0:T(8,128)(2,1)S(1)}, bf16[384,512]{1,0:T(8,128)(2,1)S(1)}, u32[]{:S(2)}, u32[]{:S(2)}) collective-permute-start(bf16[384,512]{1,0:T(8,128)(2,1)S(1)} %copy-done.2), channel_id=1, source_target_pairs={{0,2},{1,3},{2,0},{3,1},{4,6},{5,7},{6,4},{7,5},{8,10},{9,11},{10,... | collective-permute-start | bytes 1179656 | tf_op jit(solution)/shard_map/ppermute | solution.py:22
  81.3 28.4 %collective-permute-start.26 = (bf16[384,512]{1,0:T(8,128)(2,1)S(1)}, bf16[384,512]{1,0:T(8,128)(2,1)S(1)}, u32[]{:S(2)}, u32[]{:S(2)}) collective-permute-start(bf16[384,512]{1,0:T(8,128)(2,1)S(1)} %get-tuple-element.44.refs_1_), channel_id=1, source_target_pairs={{0,2},{1,3},{2,0},{3,1},{4,6},{5,7},{6,4},{7,5},{8,10},{9,11},{10,... | collective-permute-start | bytes 1179656 | tf_op jit(solution)/shard_map/ppermute | solution.py:22
  82.8 11.6 %collective-permute-start.22 = (bf16[48,1024]{1,0:T(8,128)(2,1)S(1)}, bf16[48,1024]{1,0:T(8,128)(2,1)S(1)}, u32[]{:S(2)}, u32[]{:S(2)}) collective-permute-start(bf16[48,1024]{1,0:T(8,128)(2,1)S(1)} %get-tuple-element.52), channel_id=1, source_target_pairs={{0,20},{4,16},{8,28},{12,24},{16,4},{20,0},{24,12},{28,8},{1,21},{... | collective-permute-start | bytes 294920 | tf_op jit(solution)/shard_map/ppermute | solution.py:22
  88.1 9.6 %collective-permute-start.23 = (bf16[48,1024]{1,0:T(8,128)(2,1)S(1)}, bf16[48,1024]{1,0:T(8,128)(2,1)S(1)}, u32[]{:S(2)}, u32[]{:S(2)}) collective-permute-start(bf16[48,1024]{1,0:T(8,128)(2,1)S(1)} %get-tuple-element.53), channel_id=1, source_target_pairs={{0,24},{4,28},{8,16},{12,20},{16,8},{20,12},{24,0},{28,4},{1,25},{... | collective-permute-start | bytes 294920 | tf_op jit(solution)/shard_map/ppermute | solution.py:22
  94.3 12.2 %collective-permute-start.24 = (bf16[48,1024]{1,0:T(8,128)(2,1)S(1)}, bf16[48,1024]{1,0:T(8,128)(2,1)S(1)}, u32[]{:S(2)}, u32[]{:S(2)}) collective-permute-start(bf16[48,1024]{1,0:T(8,128)(2,1)S(1)} %get-tuple-element.54), channel_id=1, source_target_pairs={{0,28},{4,24},{8,20},{12,16},{16,12},{20,8},{24,4},{28,0},{1,29},{... | collective-permute-start | bytes 294920 | tf_op jit(solution)/shard_map/ppermute | solution.py:22
  104.0 3.7 %collective-permute-start.17 = (bf16[2,512]{1,0:T(2,128)(2,1)S(1)}, bf16[2,512]{1,0:T(2,128)(2,1)S(1)}, u32[]{:S(2)}, u32[]{:S(2)}) collective-permute-start(bf16[2,512]{1,0:T(2,128)(2,1)S(1)} %get-tuple-element.49), channel_id=1, source_target_pairs={{0,4},{4,8},{8,12},{12,16},{16,20},{20,24},{24,28},{1,5},{5,9},{9,... | collective-permute-start | bytes 6152 | tf_op jit(solution)/shard_map/ppermute | solution.py:492
  108.1 9.4 %collective-permute-start.18 = (bf16[384,512]{1,0:T(8,128)(2,1)S(1)}, bf16[384,512]{1,0:T(8,128)(2,1)S(1)}, u32[]{:S(2)}, u32[]{:S(2)}) collective-permute-start(bf16[384,512]{1,0:T(8,128)(2,1)S(1)} %fusion.8), channel_id=1, source_target_pairs={{0,1},{1,0},{2,3},{3,2},{4,5},{5,4},{6,7},{7,6},{8,9},{9,8},{10,11... | collective-permute-start | bytes 1179656 | tf_op jit(solution)/shard_map/ppermute | solution.py:22
  108.2 11.5 %collective-permute-start.19 = (bf16[384,512]{1,0:T(8,128)(2,1)S(1)}, bf16[384,512]{1,0:T(8,128)(2,1)S(1)}, u32[]{:S(2)}, u32[]{:S(2)}) collective-permute-start(bf16[384,512]{1,0:T(8,128)(2,1)S(1)} %fusion.8), channel_id=1, source_target_pairs={{0,2},{1,3},{2,0},{3,1},{4,6},{5,7},{6,4},{7,5},{8,10},{9,11},{10,... | collective-permute-start | bytes 1179656 | tf_op jit(solution)/shard_map/ppermute | solution.py:22
  112.8 11.8 %collective-permute-start.27 = (bf16[96,1024]{1,0:T(8,128)(2,1)}, bf16[96,1024]{1,0:T(8,128)(2,1)S(1)}, u32[]{:S(2)}, u32[]{:S(2)}) collective-permute-start(bf16[96,1024]{1,0:T(8,128)(2,1)} %get-tuple-element.59), channel_id=1, source_target_pairs={{0,4},{4,0},{8,12},{12,8},{16,20},{20,16},{24,28},{28,24},{1,5},{5... | collective-permute-start | bytes 589832 | tf_op jit(solution)/shard_map/ppermute | solution.py:22
  115.2 12.0 %collective-permute-start.28 = (bf16[96,1024]{1,0:T(8,128)(2,1)}, bf16[96,1024]{1,0:T(8,128)(2,1)S(1)}, u32[]{:S(2)}, u32[]{:S(2)}) collective-permute-start(bf16[96,1024]{1,0:T(8,128)(2,1)} %get-tuple-element.60), channel_id=1, source_target_pairs={{0,8},{4,12},{8,0},{12,4},{16,24},{20,28},{24,16},{28,20},{1,9},{5... | collective-permute-start | bytes 589832 | tf_op jit(solution)/shard_map/ppermute | solution.py:22
  116.1 14.5 %collective-permute-start.29 = (bf16[96,1024]{1,0:T(8,128)(2,1)}, bf16[96,1024]{1,0:T(8,128)(2,1)S(1)}, u32[]{:S(2)}, u32[]{:S(2)}) collective-permute-start(bf16[96,1024]{1,0:T(8,128)(2,1)} %get-tuple-element.61), channel_id=1, source_target_pairs={{0,12},{4,8},{8,4},{12,0},{16,28},{20,24},{24,20},{28,16},{1,13},{... | collective-permute-start | bytes 589832 | tf_op jit(solution)/shard_map/ppermute | solution.py:22
  117.5 13.1 %collective-permute-start.30 = (bf16[48,1024]{1,0:T(8,128)(2,1)}, bf16[48,1024]{1,0:T(8,128)(2,1)S(1)}, u32[]{:S(2)}, u32[]{:S(2)}) collective-permute-start(bf16[48,1024]{1,0:T(8,128)(2,1)} %get-tuple-element.62), channel_id=1, source_target_pairs={{0,16},{4,20},{8,24},{12,28},{16,0},{20,4},{24,8},{28,12},{1,17},{... | collective-permute-start | bytes 294920 | tf_op jit(solution)/shard_map/ppermute | solution.py:22
  121.5 15.6 %collective-permute-start.31 = (bf16[48,1024]{1,0:T(8,128)(2,1)S(1)}, bf16[48,1024]{1,0:T(8,128)(2,1)S(1)}, u32[]{:S(2)}, u32[]{:S(2)}) collective-permute-start(bf16[48,1024]{1,0:T(8,128)(2,1)S(1)} %copy-done.27), channel_id=1, source_target_pairs={{0,20},{4,16},{8,28},{12,24},{16,4},{20,0},{24,12},{28,8},{1,21},{... | collective-permute-start | bytes 294920 | tf_op jit(solution)/shard_map/ppermute | solution.py:22
  124.6 12.4 %collective-permute-start.32 = (bf16[48,1024]{1,0:T(8,128)(2,1)S(1)}, bf16[48,1024]{1,0:T(8,128)(2,1)S(1)}, u32[]{:S(2)}, u32[]{:S(2)}) collective-permute-start(bf16[48,1024]{1,0:T(8,128)(2,1)S(1)} %copy-done.26), channel_id=1, source_target_pairs={{0,24},{4,28},{8,16},{12,20},{16,8},{20,12},{24,0},{28,4},{1,25},{... | collective-permute-start | bytes 294920 | tf_op jit(solution)/shard_map/ppermute | solution.py:22
  127.2 9.9 %collective-permute-start.33 = (bf16[48,1024]{1,0:T(8,128)(2,1)S(1)}, bf16[48,1024]{1,0:T(8,128)(2,1)S(1)}, u32[]{:S(2)}, u32[]{:S(2)}) collective-permute-start(bf16[48,1024]{1,0:T(8,128)(2,1)S(1)} %copy-done.25), channel_id=1, source_target_pairs={{0,28},{4,24},{8,20},{12,16},{16,12},{20,8},{24,4},{28,0},{1,29},{... | collective-permute-start | bytes 294920 | tf_op jit(solution)/shard_map/ppermute | solution.py:22
  (31 other events, 302.8 us)
